TPU v7x, 256 devices: a whole 4x4x8 slice. The times are simulated.
256 devices in a mesh: sp: 32 (over z, x), tp: 8 (over y, core).
Axes of the slice: x: 4, y: 4, z: 8, core: 2. Of those that a mesh axis runs over, the one named last changes fastest.
Arguments:
- tokens: bfloat16 [16384, 2048], P(('sp', 'tp')), may hold values from -6 to 6
- norm_gain: float32 [2048], replicated, may hold values from 0.1 to 1.9
- rec_query: bfloat16 [2048, 1024], P(None, 'tp'), may hold values from -0.125 to 0.125
- fwd_gate: bfloat16 [2048, 1024], P(None, 'tp'), may hold values from -0.125 to 0.125
- bwd_gate: bfloat16 [2048, 1024], P(None, 'tp'), may hold values from -0.125 to 0.125
- rec_value: bfloat16 [2048, 1024], P(None, 'tp'), may hold values from -0.125 to 0.125
- gate_leak: float32 [2, 1024], P(None, 'tp'), may hold values from 0 to 0.08, as said below
- log_decay: float32 [2, 16384, 8], P(None, 'sp', 'tp'), may hold values from -2.2 to 0, as said below
- rec_gain: float32 [128], replicated, may hold values from 0.1 to 1.9
- att_query: bfloat16 [2048, 1024], P(None, 'tp'), as said below
- att_key: bfloat16 [2048, 1024], P(None, 'tp')
- att_value: bfloat16 [2048, 1024], P(None, 'tp'), may hold values from -0.125 to 0.125
- lambdas: float32 [8], P('tp'), may hold values from 0.3 to 0.8
- att_gain: float32 [128], replicated, may hold values from 0.1 to 1.9
- out_rec: bfloat16 [1024, 2048], replicated, may hold values from -0.125 to 0.125
- out_att: bfloat16 [1024, 2048], replicated, may hold values from -0.125 to 0.125
Outputs:
- layer_out: bfloat16 [16384, 2048], P(('sp', 'tp'))
Inputs may be any that keep to these rules, and one draw needn't show every extreme that they name: `gate_leak`: positive, by direction and channel. `log_decay`: never positive. `att_query`: entries of order 2048 to the power -1/2.
All inputs are finite; a program needn't handle non-finite values.
Results may differ from a plain program's by a relative error of at most 0.011.
Values may be sent and summed in bfloat16 or wider, within the bound.
No kernel may reach another device: no remote copies, remote signals or barrier semaphores. Data moves between devices by JAX's collectives and lax.ppermute only.
A program may use at most 128 MiB of HBM per device.

v0:
```python
import math

import jax
import jax.numpy as jnp
from jax import lax
from jax.sharding import Mesh
from jax.sharding import PartitionSpec as P

HK = 128
HV = 128
AK = 64
AV = 128
BLOCK = 64
SP = ("sp_0", "sp_1")
SP_TP = ("sp_0", "sp_1", "tp")


EPS = 1e-06
THETA = 500000.0


def joined_along(pieces, dim):
    dims = list(pieces.shape[1:])
    dims[dim] *= pieces.shape[0]
    return jnp.moveaxis(pieces, 0, dim).reshape(dims)


def copy_for_each(value, axis):
    copies = jnp.broadcast_to(value, (lax.axis_size(axis), *value.shape))
    return lax.all_to_all(copies, axis, split_axis=0, concat_axis=0, tiled=True)


def gathered_copies(value, axis, dim):
    return joined_along(copy_for_each(value, axis), dim)


def nothing_yet(value, identity):
    return jax.tree.map(
        lambda part, zero: jnp.zeros_like(part) + jnp.asarray(zero, part.dtype), value, identity
    )


def all_in_one(value, axis):
    leaves = jax.tree.leaves(value)
    order = sorted(range(len(leaves)), key=lambda k: -leaves[k].size)
    width = (1, *leaves[order[0]].shape)[-1]
    lines = [
        jnp.pad(leaves[k].reshape(-1), (0, -leaves[k].size % width)).reshape(-1, width)
        for k in order
    ]
    both, at, found = (lax.all_gather(jnp.concatenate(lines), axis), 0, {})
    for k, line in zip(order, lines):
        piece = both[:, at : at + len(line)].reshape(len(both), -1)
        found[k] = piece[:, : leaves[k].size].reshape(-1, *leaves[k].shape)
        at += len(line)
    numbers = iter(range(len(leaves)))
    return jax.tree.map(lambda _: found[next(numbers)], value)


def entering(value, axes, combine, identity, reverse):
    before = start = nothing_yet(value, identity)
    subtotal = value
    for axis in reversed(axes):
        size, position = (lax.axis_size(axis), lax.axis_index(axis))
        pieces = all_in_one(
            jax.tree.map(
                lambda part, kind: part.astype(kind), subtotal, (jnp.bfloat16, jnp.bfloat16)
            ),
            axis,
        )
        inside, subtotal = (start, start)
        for k in reversed(range(size)) if reverse else range(size):
            passed = k > position if reverse else k < position
            subtotal = combine(
                subtotal, jax.tree.map(lambda part, own: part[k].astype(own.dtype), pieces, value)
            )
            inside = jax.tree.map(lambda new, old: jnp.where(passed, new, old), subtotal, inside)
        before = combine(inside, before)
    return before


def in_one_piece(arrays, axis, dim, along):
    ends, at = ([], 0)
    for a in arrays[:-1]:
        at += a.shape[along]
        ends.append(at)
    both = jnp.concatenate(arrays, axis=along)
    return tuple(jnp.split(lax.all_gather(both, axis, axis=dim, tiled=True), ends, axis=along))


def rms_scale(values, gain):
    return values * lax.rsqrt(jnp.mean(values * values, axis=-1, keepdims=True) + EPS) * gain


def block_recurrence(queries, keys_in, values, log_forget):
    head_count, length, key_width = queries.shape
    value_width = values.shape[-1]
    block_count = length // BLOCK
    block_shape = (head_count, block_count, BLOCK, key_width)
    query_blocks = queries.reshape(block_shape)
    key_blocks = keys_in.reshape(block_shape)
    value_blocks = values.reshape(head_count, block_count, BLOCK, value_width)
    cumulative = jnp.cumsum(log_forget.reshape(block_shape), axis=2)
    middle = cumulative[:, :, BLOCK // 2 - 1 : BLOCK // 2]
    block_last = cumulative[:, :, BLOCK - 1 :]
    scores = jnp.einsum(
        "hntd,hnsd->hnts",
        query_blocks * jnp.exp(cumulative - middle),
        key_blocks * jnp.exp(middle - cumulative),
    )
    causal_mask = jnp.arange(BLOCK)[:, None] >= jnp.arange(BLOCK)[None, :]
    scores = jnp.where(causal_mask, scores, 0.0)
    within_out = jnp.einsum("hnts,hnsv->hntv", scores, value_blocks)
    per_block_state = jnp.einsum(
        "hnsd,hnsv->hndv", key_blocks * jnp.exp(block_last - cumulative), value_blocks
    )
    block_decay = jnp.exp(block_last[:, :, 0])

    def advance(running, inputs_now):
        factor, added_state = inputs_now
        return (factor[..., None] * running + added_state, running)

    initial = jnp.zeros((head_count, key_width, value_width), jnp.float32)
    end_state, before = lax.scan(
        advance, initial, (jnp.moveaxis(block_decay, 1, 0), jnp.moveaxis(per_block_state, 1, 0))
    )
    before = jnp.moveaxis(before, 0, 1)
    carried = jnp.einsum("hntd,hndv->hntv", query_blocks * jnp.exp(cumulative), before)
    return ((within_out + carried).reshape(head_count, length, value_width), end_state, cumulative)


def local_direction(queries, keys_in, values, log_forget):
    outputs, end_state, cumulative = block_recurrence(queries, keys_in, values, log_forget)
    head_count, length, key_width = queries.shape
    block_totals = cumulative[:, :, BLOCK - 1]
    before_block = jnp.cumsum(block_totals, axis=1) - block_totals
    within = (cumulative + before_block[:, :, None]).reshape(head_count, length, key_width)
    return (outputs, jnp.exp(jnp.sum(block_totals, axis=1)), end_state, queries * jnp.exp(within))


def link(earlier, later):
    return (earlier[0] * later[0], later[0][..., None] * earlier[1] + later[1])


def rotate(vectors, positions):
    half_width = AK // 2
    frequency = THETA ** (-(jnp.arange(half_width, dtype=jnp.float32) * 2.0 / AK))
    angles = positions[:, None] * frequency[None, :]
    cosine = jnp.cos(angles)[:, None, None, :]
    sines = jnp.sin(angles)[:, None, None, :]
    first_half = vectors[..., :half_width]
    second = vectors[..., half_width:]
    return jnp.concatenate(
        [first_half * cosine - second * sines, second * cosine + first_half * sines], axis=-1
    )


def attend(carry, queries, key_rows, value_rows):
    head_count = queries.shape[1]
    row_count = key_rows.shape[0]
    span_rows = math.gcd(row_count, 1024)
    key_blocks = key_rows.reshape(row_count // span_rows, span_rows, head_count, 2, AK)
    value_blocks = value_rows.reshape(row_count // span_rows, span_rows, head_count, AV)

    def absorb(running, inputs_now):
        peak_values, totals, summed = running
        key_block, value_block = inputs_now
        scores = jnp.einsum(
            "qhmd,khmd->hmqk", queries, key_block, preferred_element_type=jnp.float32
        )
        raised = jnp.maximum(peak_values, jnp.max(scores, axis=-1))
        shrink = jnp.exp(peak_values - raised)
        weights_raw = jnp.exp(scores - raised[..., None])
        totals = totals * shrink + jnp.sum(weights_raw, axis=-1)
        summed = summed * shrink[..., None] + jnp.einsum(
            "hmqk,khv->hmqv",
            weights_raw.astype(jnp.bfloat16),
            value_block,
            preferred_element_type=jnp.float32,
        )
        return ((raised, totals, summed), None)

    running, unused = lax.scan(absorb, carry, (key_blocks, value_blocks))
    return running


def on_device(
    tokens,
    norm_gain,
    rec_query,
    fwd_gate,
    bwd_gate,
    rec_value,
    gate_leak,
    log_decay,
    rec_gain,
    att_query,
    att_key,
    att_value,
    lambdas,
    att_gain,
    out_rec,
    out_att,
):
    normed = rms_scale(tokens.astype(jnp.float32), norm_gain).astype(jnp.bfloat16)
    weights_all = (rec_query, fwd_gate, bwd_gate, rec_value, att_query, att_key, att_value)
    joined = jnp.concatenate(weights_all, axis=1)
    projected = jnp.dot(
        gathered_copies(normed, "tp", 0), joined, preferred_element_type=jnp.float32
    ).astype(jnp.bfloat16)
    length = projected.shape[0]
    columns = []
    column_start = 0
    for weight in weights_all:
        columns.append(projected[:, column_start : column_start + weight.shape[1]])
        column_start = column_start + weight.shape[1]
    query_raw, fwd_raw, bwd_raw, value_raw, att_query_raw, att_key_raw, att_value_raw = columns

    def split_heads(table, width):
        return table.astype(jnp.float32).reshape(length, -1, width).transpose(1, 0, 2)

    queries = jax.nn.silu(split_heads(query_raw, HK))
    values = split_heads(value_raw, HV)
    rec_heads = queries.shape[0]
    key_fwd = gate_leak[0].reshape(rec_heads, 1, HK) * jax.nn.sigmoid(-split_heads(fwd_raw, HK))
    key_bwd = gate_leak[1].reshape(rec_heads, 1, HK) * jax.nn.sigmoid(-split_heads(bwd_raw, HK))
    log_fwd = jnp.log1p(-key_fwd) + log_decay[0].T[:, :, None]
    log_bwd = jnp.log1p(-key_bwd) + log_decay[1].T[:, :, None]
    out_fwd, decay_fwd, ending_fwd, read_fwd = local_direction(queries, key_fwd, values, log_fwd)
    out_back, decay_bwd, ending_bwd, read_bwd = local_direction(
        jnp.flip(queries, 1), jnp.flip(key_bwd, 1), jnp.flip(values, 1), jnp.flip(log_bwd, 1)
    )
    positions = (lax.axis_index(SP) * length + jnp.arange(length, dtype=jnp.int32)).astype(
        jnp.float32
    )
    att_queries = (
        rotate(att_query_raw.astype(jnp.float32).reshape(length, -1, 2, AK), positions)
        * AK ** (-0.5)
    ).astype(jnp.bfloat16)
    att_keys = (
        rotate(att_key_raw.astype(jnp.float32).reshape(length, -1, 2, AK), positions)
        .astype(jnp.bfloat16)
        .reshape(length, -1)
    )
    att_heads = att_queries.shape[1]
    initial = (
        jnp.full((att_heads, 2, length), -jnp.inf, jnp.float32),
        jnp.zeros((att_heads, 2, length), jnp.float32),
        jnp.zeros((att_heads, 2, length, AV), jnp.float32),
    )
    identity = (jnp.ones_like(decay_fwd), jnp.zeros_like(ending_fwd))
    entry_fwd = entering((decay_fwd, ending_fwd), SP, link, identity, False)[1]
    entry_bwd = entering((decay_bwd, ending_bwd), SP, link, identity, True)[1]
    piece = in_one_piece((att_keys, att_value_raw), SP, 0, 1)
    running = attend(initial, att_queries, piece[0], piece[1])
    out_fwd = out_fwd + jnp.einsum("hld,hdv->hlv", read_fwd, entry_fwd)
    out_back = out_back + jnp.einsum("hld,hdv->hlv", read_bwd, entry_bwd)
    rec_rows = rms_scale(out_fwd + jnp.flip(out_back, 1), rec_gain)
    rec_rows = rec_rows.transpose(1, 0, 2).reshape(length, -1).astype(jnp.bfloat16)
    peak_values, totals, summed = running
    ratio = summed / totals[..., None]
    mixed_heads = ratio[:, 0] - lambdas[:, None, None] * ratio[:, 1]
    att_rows = (
        rms_scale(mixed_heads, att_gain).transpose(1, 0, 2).reshape(length, -1).astype(jnp.bfloat16)
    )
    rec_all, att_all = (
        lax.all_to_all(rec_rows, "tp", split_axis=0, concat_axis=1, tiled=True),
        lax.all_to_all(att_rows, "tp", split_axis=0, concat_axis=1, tiled=True),
    )
    projected_out = jnp.dot(rec_all, out_rec, preferred_element_type=jnp.float32) + jnp.dot(
        att_all, out_att, preferred_element_type=jnp.float32
    )
    return projected_out.astype(jnp.bfloat16)


def solution(mesh):
    torus = Mesh(mesh.devices.reshape(8, 4, mesh.shape["tp"]), ("sp_0", "sp_1", "tp"))
    in_specs = (
        P(SP_TP, None),
        P(),
        P(None, "tp"),
        P(None, "tp"),
        P(None, "tp"),
        P(None, "tp"),
        P(None, "tp"),
        P(None, SP, "tp"),
        P(),
        P(None, "tp"),
        P(None, "tp"),
        P(None, "tp"),
        P("tp"),
        P(),
        P(),
        P(),
    )
    out_specs = P(SP_TP, None)
    return jax.shard_map(
        on_device, mesh=torus, in_specs=in_specs, out_specs=out_specs, check_vma=False
    )
```

profile of v0, /device:TPU:1, one launch (start us, length us, event | category | flops | bytes accessed | tf_op | source)
XLA Modules:
  0.0 368.9 jit_solution(11481244566510974270)
XLA Ops:
  10.4 6.8 %all-to-all-start = ((bf16[8,64,2048]{2,1,0:T(8,128)(2,1)}), bf16[8,64,2048]{2,1,0:T(8,128)(2,1)S(1)}, u32[]{:S(2)}, u32[]{:S(2)}) async-start(bf16[8,64,2048]{2,1,0:T(8,128)(2,1)} %broadcast_in_dim.32), calls=%async_computation | async-start | bytes 4194304 | tf_op jit(solution)/shard_map/all_to_all | solution.py:30
  26.1 17.4 %all-to-all-done = bf16[8,64,2048]{2,1,0:T(8,128)(2,1)S(1)} async-done(((bf16[8,64,2048]{2,1,0:T(8,128)(2,1)}), bf16[8,64,2048]{2,1,0:T(8,128)(2,1)S(1)}, u32[]{:S(2)}, u32[]{:S(2)}) %all-to-all-start) | async-done | bytes 2097184 | tf_op jit(solution)/shard_map/all_to_all | solution.py:30
  43.5 4.4 %convolution_convert_fusion = bf16[512,896]{1,0:T(8,128)(2,1)S(1)} fusion(bf16[512,2048]{1,0:T(8,128)(2,1)S(1)} %bitcast.374, bf16[2048,896]{1,0:T(8,128)(2,1)} %constant_dynamic-update-slice_fusion), kind=kOutput, calls=%fused_computation.34 | convolution fusion | flops 1879506944 | bytes 6684672 | tf_op jit(solution)/shard_map/dot_general | solution.py:208
  57.0 6.2 %while.42 = (s32[]{:T(128)}, f32[1,128,128]{2,1,0:T(8,128)S(1)}, bf16[8,1,128,128]{3,2,1,0:T(8,128)(2,1)S(1)}, f32[8,1,128]{2,1,0:T(1,128)}, f32[8,1,128,128]{3,2,1,0:T(8,128)S(1)}, /*index=5*/s32[]{:T(128)}, s32[]{:T(128)}) while((s32[]{:T(128)}, f32[1,128,128]{2,1,0:T(8,128)S(1)}, bf16[8,1,128,128]{3,2,1,0:T(8,128)(2,1)S(1)}, ...), condition=%wide.region_8.9_spmd.clone, body=%wide.region_7.8_spmd.clone.sunk | while | flops 65539 | bytes 296556 | solution.py:124
  63.3 9.9 %all-gather.6 = bf16[4,129,128]{2,1,0:T(8,128)(2,1)S(1)} all-gather(bf16[1,129,128]{2,1,0:T(8,128)(2,1)S(1)} %maximum_bitcast_fusion.2), channel_id=4, replica_groups=mesh['sp_0'=8,'sp_1'=4,'tp'=8] {'sp_1'}, dimensions={0}, use_global_device_ids=true | all-gather | bytes 165120 | tf_op jit(solution)/shard_map/all_gather | solution.py:51
  73.3 23.6 %all-gather.7 = bf16[8,129,128]{2,1,0:T(8,128)(2,1)S(1)} all-gather(bf16[1,129,128]{2,1,0:T(8,128)(2,1)S(1)} %maximum_bitcast_fusion.3), channel_id=5, replica_groups=mesh['sp_0'=8,'sp_1'=4,'tp'=8] {'sp_0'}, dimensions={0}, use_global_device_ids=true | all-gather | bytes 297216 | tf_op jit(solution)/shard_map/all_gather | solution.py:51
  100.5 6.2 %while.41 = (s32[]{:T(128)}, f32[1,128,128]{2,1,0:T(8,128)S(1)}, bf16[8,1,128,128]{3,2,1,0:T(8,128)(2,1)S(1)}, f32[8,1,128]{2,1,0:T(1,128)}, f32[8,1,128,128]{3,2,1,0:T(8,128)S(1)}, /*index=5*/s32[]{:T(128)}, s32[]{:T(128)}) while((s32[]{:T(128)}, f32[1,128,128]{2,1,0:T(8,128)S(1)}, bf16[8,1,128,128]{3,2,1,0:T(8,128)(2,1)S(1)}, ...), condition=%wide.region_3.4_spmd.clone, body=%wide.region_2.3_spmd.clone.sunk | while | flops 65539 | bytes 296556 | solution.py:124
  106.8 11.3 %all-gather.4 = bf16[4,129,128]{2,1,0:T(8,128)(2,1)S(1)} all-gather(bf16[1,129,128]{2,1,0:T(8,128)(2,1)S(1)} %maximum_bitcast_fusion), channel_id=2, replica_groups=mesh['sp_0'=8,'sp_1'=4,'tp'=8] {'sp_1'}, dimensions={0}, use_global_device_ids=true | all-gather | bytes 165120 | tf_op jit(solution)/shard_map/all_gather | solution.py:51
  118.3 22.5 %all-gather.5 = bf16[8,129,128]{2,1,0:T(8,128)(2,1)S(1)} all-gather(bf16[1,129,128]{2,1,0:T(8,128)(2,1)S(1)} %maximum_bitcast_fusion.1), channel_id=3, replica_groups=mesh['sp_0'=8,'sp_1'=4,'tp'=8] {'sp_0'}, dimensions={0}, use_global_device_ids=true | all-gather | bytes 297216 | tf_op jit(solution)/shard_map/all_gather | solution.py:51
  142.8 16.7 %all-to-all-start.1 = ((bf16[8,64,128]{2,1,0:T(8,128)(2,1)}), bf16[8,64,128]{2,1,0:T(8,128)(2,1)S(1)}, u32[]{:S(2)}, u32[]{:S(2)}) async-start(bf16[8,64,128]{2,1,0:T(8,128)(2,1)} %bitcast.75), calls=%async_computation.1 | async-start | bytes 262144 | tf_op jit(solution)/shard_map/all_to_all | solution.py:267
  159.5 5.7 %fusion.265 = (bf16[16384,128]{1,0:T(8,128)(2,1)}, bf16[16384,128]{1,0:T(8,128)(2,1)}) fusion(bf16[16384,256]{1,0:T(8,128)(2,1)} %all-gather.10.cloned.1.call-done), kind=kLoop, calls=%fused_computation.394 | loop fusion | bytes 16777216 | tf_op jit(solution)/shard_map/split | solution.py:88
  165.2 14.7 %reshape.1565 = bf16[16,1024,1,2,64]{4,3,1,0,2:T(2,128)(2,1)} reshape(bf16[16384,128]{1,0:T(8,128)(2,1)} %get-tuple-element.274) | data formatting | bytes 8388608 | tf_op jit(solution)/shard_map/reshape | solution.py:162
  180.0 20.1 %copy.138 = bf16[16,1024,1,2,64]{1,4,3,2,0:T(8,128)(2,1)} copy(bf16[16,1024,1,2,64]{4,3,1,0,2:T(2,128)(2,1)} %reshape.1565) | data formatting | bytes 8388608
  200.1 146.9 %while.43 = (s32[]{:T(128)}, f32[1,2,512]{2,1,0:T(2,128)S(1)}, f32[1,2,512]{2,1,0:T(2,128)S(1)}, f32[1,2,512,128]{3,2,1,0:T(8,128)S(1)}, bf16[16,1024,1,2,64]{1,...) while((s32[]{:T(128)}, f32[1,2,512]{2,1,0:T(2,128)S(1)}, ...), condition=%wide.region_15.16_spmd.clone, body=%wide.region_12.15_spmd.clone.sunk | while | flops 408295424 | bytes 31129748 | solution.py:183
  200.1 3.7 bitcast_reduce_fusion.2
  209.3 3.7 bitcast_reduce_fusion.2
  218.4 3.7 bitcast_reduce_fusion.2
  227.6 3.7 bitcast_reduce_fusion.2
  236.8 3.7 bitcast_reduce_fusion.2
  246.0 3.7 bitcast_reduce_fusion.2
  255.2 3.7 bitcast_reduce_fusion.2
  264.3 3.7 bitcast_reduce_fusion.2
  273.5 3.7 bitcast_reduce_fusion.2
  282.7 3.7 bitcast_reduce_fusion.2
  291.9 3.7 bitcast_reduce_fusion.2
  301.1 3.7 bitcast_reduce_fusion.2
  310.3 3.7 bitcast_reduce_fusion.2
  319.4 3.7 bitcast_reduce_fusion.2
  328.6 3.7 bitcast_reduce_fusion.2
  337.8 3.7 bitcast_reduce_fusion.2
  348.2 4.8 %all-to-all-start.2 = ((bf16[8,64,128]{2,1,0:T(8,128)(2,1)}), bf16[8,64,128]{2,1,0:T(8,128)(2,1)S(1)}, u32[]{:S(2)}, u32[]{:S(2)}) async-start(bf16[8,64,128]{2,1,0:T(8,128)(2,1)} %multiply_convert_fusion), calls=%async_computation.2 | async-start | bytes 262144 | tf_op jit(solution)/shard_map/all_to_all | solution.py:268
  358.3 3.7 %fusion.23 = bf16[64,2048]{1,0:T(8,128)(2,1)} fusion(f32[64,2048]{1,0:T(8,128)S(1)} %fusion.73, bf16[1024,2048]{1,0:T(8,128)(2,1)} %param.37, bf16[8,64,128]{2,1,0:T(8,128)(2,1)S(1)} %all-to-all-done.2), kind=kOutput, calls=%fused_computation.33 | convolution fusion | flops 268697600 | bytes 5111808 | tf_op jit(solution)/shard_map/dot_general | solution.py:270
  (275 shorter events, 132.9 us)
Async XLA Ops:
  6.5 10.8 %copy-start.8 = (f32[2,512,1]{1,2,0:T(1,128)S(1)}, f32[2,512,1]{1,2,0:T(1,128)}, u32[]{:S(2)}) copy-start(f32[2,512,1]{1,2,0:T(1,128)} %param.29) | copy-start | bytes 12292
  7.7 10.1 %copy-start.9 = (f32[2,128]{1,0:T(2,128)S(1)}, f32[2,128]{1,0:T(2,128)}, u32[]{:S(2)}) copy-start(f32[2,128]{1,0:T(2,128)} %param.28) | copy-start | bytes 3076
  7.7 10.1 %copy-start.2 = (bf16[2048,128]{1,0:T(8,128)(2,1)S(1)}, bf16[2048,128]{1,0:T(8,128)(2,1)}, u32[]{:S(2)}) copy-start(bf16[2048,128]{1,0:T(8,128)(2,1)} %param.24) | copy-start | bytes 1572868
  10.4 8.3 %copy-start.3 = (bf16[2048,128]{1,0:T(8,128)(2,1)S(1)}, bf16[2048,128]{1,0:T(8,128)(2,1)}, u32[]{:S(2)}) copy-start(bf16[2048,128]{1,0:T(8,128)(2,1)} %param.25) | copy-start | bytes 1572868
  10.4 33.1 %all-to-all-start = ((bf16[8,64,2048]{2,1,0:T(8,128)(2,1)}), bf16[8,64,2048]{2,1,0:T(8,128)(2,1)S(1)}, u32[]{:S(2)}, u32[]{:S(2)}) async-start(bf16[8,64,2048]{2,1,0:T(8,128)(2,1)} %broadcast_in_dim.32), calls=%async_computation | async-start | bytes 4194304 | tf_op jit(solution)/shard_map/all_to_all | solution.py:30
  17.3 142.3 %all-gather.10.cloned.1.call-start = ((), (), s32[]{:S(2)}) async-start(), calls=%async_computation.3 | async-start | bytes 8650752 | tf_op jit(solution)/shard_map/all_gather | solution.py:88
  17.4 6.0 %copy-start.4 = (bf16[2048,128]{1,0:T(8,128)(2,1)S(1)}, bf16[2048,128]{1,0:T(8,128)(2,1)}, u32[]{:S(2)}) copy-start(bf16[2048,128]{1,0:T(8,128)(2,1)} %param.31) | copy-start | bytes 1572868
  17.4 7.0 %copy-start.5 = (bf16[2048,128]{1,0:T(8,128)(2,1)S(1)}, bf16[2048,128]{1,0:T(8,128)(2,1)}, u32[]{:S(2)}) copy-start(bf16[2048,128]{1,0:T(8,128)(2,1)} %param.32) | copy-start | bytes 1572868
  17.4 7.8 %copy-start.6 = (bf16[2048,128]{1,0:T(8,128)(2,1)S(1)}, bf16[2048,128]{1,0:T(8,128)(2,1)}, u32[]{:S(2)}) copy-start(bf16[2048,128]{1,0:T(8,128)(2,1)} %param.33) | copy-start | bytes 1572868
  47.9 0.9 copy-start.1
  57.0 43.4 %copy-start.12 = (f32[128]{0:T(128)S(1)}, f32[128]{0:T(128)}, u32[]{:S(2)}) copy-start(f32[128]{0:T(128)} %get-tuple-element.352) | copy-start | bytes 1540
  97.0 0.7 copy-start.7
  100.2 41.8 %copy-start.10 = (f32[128]{0:T(128)S(1)}, f32[128]{0:T(128)}, u32[]{:S(2)}) copy-start(f32[128]{0:T(128)} %param.30) | copy-start | bytes 1540
  142.8 205.4 %all-to-all-start.1 = ((bf16[8,64,128]{2,1,0:T(8,128)(2,1)}), bf16[8,64,128]{2,1,0:T(8,128)(2,1)S(1)}, u32[]{:S(2)}, u32[]{:S(2)}) async-start(bf16[8,64,128]{2,1,0:T(8,128)(2,1)} %bitcast.75), calls=%async_computation.1 | async-start | bytes 262144 | tf_op jit(solution)/shard_map/all_to_all | solution.py:267
  200.1 147.4 %copy-start.11 = (f32[128]{0:T(128)S(1)}, f32[128]{0:T(128)}, u32[]{:S(2)}) copy-start(f32[128]{0:T(128)} %param.35) | copy-start | bytes 1540
  203.7 3.4 copy-start
  212.9 3.4 copy-start
  222.1 3.4 copy-start
  231.3 3.4 copy-start
  240.5 3.4 copy-start
  249.6 3.4 copy-start
  258.8 3.4 copy-start
  268.0 3.4 copy-start
  277.2 3.4 copy-start
  286.4 3.4 copy-start
  295.6 3.4 copy-start
  304.7 3.4 copy-start
  313.9 3.4 copy-start
  323.1 3.4 copy-start
  332.3 3.4 copy-start
  341.5 3.4 copy-start
  348.2 10.1 %all-to-all-start.2 = ((bf16[8,64,128]{2,1,0:T(8,128)(2,1)}), bf16[8,64,128]{2,1,0:T(8,128)(2,1)S(1)}, u32[]{:S(2)}, u32[]{:S(2)}) async-start(bf16[8,64,128]{2,1,0:T(8,128)(2,1)} %multiply_convert_fusion), calls=%async_computation.2 | async-start | bytes 262144 | tf_op jit(solution)/shard_map/all_to_all | solution.py:268
Sparse Core Ops, SparseCore 0:
  53.2 101.1 all-gather.9
where the time goes:
time: 372 us; the launch traced here: 369 us
  matrix products  106 us (28%)
  local copies, waits for them, and re-layouts  70.9 us (19%)
  blocking collectives  67.4 us (18%)
  other arithmetic  60.9 us (16%)
  starting transfers between devices  28.3 us (8%)
  waiting for transfers between devices  19.6 us (5%)
  between operations  14.7 us (4%)
    all_gather x4, blocking collectives, all_in_one(): both, at, found = (lax.all_gather(jnp.concatenate(lines), axis), 0, {})  67.4 us
    dot_general x16, matrix products, absorb(): jnp.einsum('qhmd,khmd->hmqk', queries, key_block, preferred_element_type=...  58.6 us
    reduce_sum x16, other arithmetic, absorb(): totals = totals * shrink + jnp.sum(weights_raw, axis=-1)  46.8 us
    dot_general x16, matrix products, absorb(): jnp.einsum('hmqk,khv->hmqv', weights_raw.astype(jnp.bfloat16), value_bloc...  32.8 us
    unnamed x31, local copies, waits for them, and re-layouts  28.8 us
    all_to_all x1, waiting for transfers between devices, copy_for_each(): return lax.all_to_all(copies, axis, split_axis=0, concat_axis=0, tiled=True)  17.4 us
    all_to_all x1, starting transfers between devices, on_device(): lax.all_to_all(rec_rows, 'tp', split_axis=0, concat_axis=1, tiled=True)  16.7 us
    reshape x1, local copies, waits for them, and re-layouts, attend(): key_rows.reshape(row_count // span_rows, span_rows, head_count, 2, AK)  14.7 us
  transfers between devices with their start and end apart: 4, of which 2 were waited for; matrix products, arithmetic and copies ran while one was open for 58% of the time, Pallas kernels for 0%

commit v1 on v0

v1 whole, which is shorter than its diff:
```python
import functools

import jax
import jax.numpy as jnp
from jax import lax
from jax.experimental import pallas as pl
from jax.experimental.pallas import tpu as pltpu
from jax.sharding import Mesh
from jax.sharding import PartitionSpec as P

HK = 128
HV = 128
AK = 64
AV = 128
BLOCK = 64
NZ, NX, NY, NC = 8, 4, 4, 2
AXES = ("z", "x", "y", "c")
SP = ("z", "x")
TP = ("y", "c")
TOK = 512
ACC_ROWS = 144
SEND_ROWS = 2 * AV + 16
BF16 = jnp.bfloat16
F32 = jnp.float32

EPS = 1e-06
THETA = 500000.0
LOW = -1e30


def shift(value, axis, by, size):
    return lax.ppermute(value, axis, [(i, (i + by) % size) for i in range(size)])


def gather_rows(rows):
    y, c = lax.axis_index("y"), lax.axis_index("c")
    half = rows.shape[0] // 2
    up = shift(rows, "y", 1, NY)
    down = shift(rows, "y", -1, NY)
    far_low = shift(rows[:half], "y", 2, NY)
    far_high = shift(rows[half:], "y", -2, NY)
    mine = jnp.zeros((NY, *rows.shape), rows.dtype)
    for piece, source in (
        (rows, y),
        (up, (y + 3) % 4),
        (down, (y + 1) % 4),
        (jnp.concatenate([far_low, far_high]), (y + 2) % 4),
    ):
        mine = lax.dynamic_update_slice(mine, piece[None], (source, 0, 0))
    other = shift(mine, "c", 1, NC)
    both = jnp.zeros((NY, NC, *rows.shape), rows.dtype)
    both = lax.dynamic_update_slice(both, mine[:, None], (0, c, 0, 0))
    both = lax.dynamic_update_slice(both, other[:, None], (0, 1 - c, 0, 0))
    return both.reshape(-1, rows.shape[1])


def rms_scale(values, gain):
    return values * lax.rsqrt(jnp.mean(values * values, axis=-1, keepdims=True) + EPS) * gain


def block_recurrence(queries, keys_in, values, log_forget):
    head_count, length, key_width = queries.shape
    value_width = values.shape[-1]
    block_count = length // BLOCK
    block_shape = (head_count, block_count, BLOCK, key_width)
    query_blocks = queries.reshape(block_shape)
    key_blocks = keys_in.reshape(block_shape)
    value_blocks = values.reshape(head_count, block_count, BLOCK, value_width)
    cumulative = jnp.cumsum(log_forget.reshape(block_shape), axis=2)
    middle = cumulative[:, :, BLOCK // 2 - 1 : BLOCK // 2]
    block_last = cumulative[:, :, BLOCK - 1 :]
    scores = jnp.einsum(
        "hntd,hnsd->hnts",
        query_blocks * jnp.exp(cumulative - middle),
        key_blocks * jnp.exp(middle - cumulative),
    )
    causal_mask = jnp.arange(BLOCK)[:, None] >= jnp.arange(BLOCK)[None, :]
    scores = jnp.where(causal_mask, scores, 0.0)
    within_out = jnp.einsum("hnts,hnsv->hntv", scores, value_blocks)
    per_block_state = jnp.einsum(
        "hnsd,hnsv->hndv", key_blocks * jnp.exp(block_last - cumulative), value_blocks
    )
    block_decay = jnp.exp(block_last[:, :, 0])

    def advance(running, inputs_now):
        factor, added_state = inputs_now
        return (factor[..., None] * running + added_state, running)

    initial = jnp.zeros((head_count, key_width, value_width), jnp.float32)
    end_state, before = lax.scan(
        advance, initial, (jnp.moveaxis(block_decay, 1, 0), jnp.moveaxis(per_block_state, 1, 0))
    )
    before = jnp.moveaxis(before, 0, 1)
    carried = jnp.einsum("hntd,hndv->hntv", query_blocks * jnp.exp(cumulative), before)
    return ((within_out + carried).reshape(head_count, length, value_width), end_state, cumulative)


def local_direction(queries, keys_in, values, log_forget):
    outputs, end_state, cumulative = block_recurrence(queries, keys_in, values, log_forget)
    head_count, length, key_width = queries.shape
    block_totals = cumulative[:, :, BLOCK - 1]
    before_block = jnp.cumsum(block_totals, axis=1) - block_totals
    within = (cumulative + before_block[:, :, None]).reshape(head_count, length, key_width)
    return (outputs, jnp.exp(jnp.sum(block_totals, axis=1)), end_state, queries * jnp.exp(within))


def rotate(vectors, positions):
    half_width = AK // 2
    frequency = THETA ** (-(jnp.arange(half_width, dtype=jnp.float32) * 2.0 / AK))
    angles = positions[:, None] * frequency[None, :]
    cosine = jnp.cos(angles)[:, None, :]
    sines = jnp.sin(angles)[:, None, :]
    first_half = vectors[..., :half_width]
    second = vectors[..., half_width:]
    return jnp.concatenate(
        [first_half * cosine - second * sines, second * cosine + first_half * sines], axis=-1
    )


def attend_body(*refs, first, last, chunks, key_block):
    q_ref, *kv_refs = refs[: 1 + chunks]
    rest = refs[1 + chunks :]
    if not first:
        peak_in, acc_in = rest[:2]
        rest = rest[2:]
    if last:
        send_ref, k_all, v_all, peaks, accs = rest
    else:
        peaks, accs, k_all, v_all = rest
    width = q_ref.shape[-1]
    rows = kv_refs[0].shape[0]

    @pl.when(pl.program_id(0) == 0)
    def _():
        for n, kv in enumerate(kv_refs):
            k_all[n * rows : (n + 1) * rows, :] = kv[:, :128]
            v_all[:AV, n * rows : (n + 1) * rows] = kv[:, 128:].T
        v_all[AV:, :] = jnp.ones((ACC_ROWS - AV, chunks * rows), BF16)

    if first:
        peaks[...] = jnp.full(peaks.shape, LOW, F32)
        accs[...] = jnp.zeros(accs.shape, F32)
    else:
        peaks[...] = peak_in[...]
        accs[...] = acc_in[...]
    both = q_ref[...]
    upper = lax.broadcasted_iota(jnp.int32, (2 * AK, width), 0) < AK
    zero = jnp.zeros_like(both)
    maps = (jnp.where(upper, both, zero), jnp.where(upper, zero, both))

    def absorb(i, unused):
        at = pl.multiple_of(i * key_block, key_block)
        keys = k_all[pl.ds(at, key_block), :]
        values = v_all[:, pl.ds(at, key_block)]
        scores = [jnp.dot(keys, q, preferred_element_type=F32) for q in maps]
        for m in range(2):
            old = peaks[m, 0:1, :]
            new = jnp.maximum(old, jnp.max(scores[m], axis=0, keepdims=True))
            weights = jnp.exp(scores[m] - new).astype(BF16)
            accs[m] = accs[m] * jnp.exp(old - new) + jnp.dot(
                values, weights, preferred_element_type=F32
            )
            peaks[m, 0:1, :] = new
        return 0

    lax.fori_loop(0, chunks * rows // key_block, absorb, 0, unroll=2)
    if last:
        for m in range(2):
            acc = accs[m]
            total = acc[AV : AV + 1, :]
            send_ref[0, m * AV : (m + 1) * AV, :] = (acc[:AV] / total).astype(BF16)
            level = peaks[m, 0:1, :] + jnp.log(total)
            high = level.astype(BF16)
            left = level - high.astype(F32)
            middle = left.astype(BF16)
            low = (left - middle.astype(F32)).astype(BF16)
            at = 2 * AV + 8 * m
            send_ref[0, at : at + 8, :] = jnp.concatenate(
                [high.astype(F32), middle.astype(F32), low.astype(F32), jnp.zeros((5, width), F32)]
            ).astype(BF16)


def attend(queries, pieces, state=None, last=False):
    chunks, rows = len(pieces), pieces[0].shape[0]
    count = queries.shape[1]
    tiles = count // TOK
    first = state is None
    kv_spec = pl.BlockSpec((rows, 256), lambda i: (0, 0))
    peak_spec = pl.BlockSpec((2, 8, TOK), lambda i: (0, 0, i))
    acc_spec = pl.BlockSpec((2, ACC_ROWS, TOK), lambda i: (0, 0, i))
    in_specs = [pl.BlockSpec((2 * AK, TOK), lambda i: (0, i))] + [kv_spec] * chunks
    operands = [queries, *pieces]
    if not first:
        in_specs += [peak_spec, acc_spec]
        operands += state
    scratch = [pltpu.VMEM((chunks * rows, 128), BF16), pltpu.VMEM((ACC_ROWS, chunks * rows), BF16)]
    if last:
        out_specs = [pl.BlockSpec((1, SEND_ROWS, TOK), lambda i: (i, 0, 0))]
        out_shape = [jax.ShapeDtypeStruct((tiles, SEND_ROWS, TOK), BF16)]
        scratch += [pltpu.VMEM((2, 8, TOK), F32), pltpu.VMEM((2, ACC_ROWS, TOK), F32)]
    else:
        out_specs = [peak_spec, acc_spec]
        out_shape = [
            jax.ShapeDtypeStruct((2, 8, count), F32),
            jax.ShapeDtypeStruct((2, ACC_ROWS, count), F32),
        ]
    body = functools.partial(attend_body, first=first, last=last, chunks=chunks, key_block=TOK)
    work = 2 * count * chunks * rows
    return pl.pallas_call(
        body,
        grid=(tiles,),
        in_specs=in_specs,
        out_specs=out_specs,
        out_shape=out_shape,
        scratch_shapes=scratch,
        cost_estimate=pl.CostEstimate(
            flops=work * 2 * (AK + AV), transcendentals=work, bytes_accessed=count * 2048
        ),
        compiler_params=pltpu.CompilerParams(vmem_limit_bytes=48 * 1024 * 1024),
        name="attend",
    )(*operands)


def mix_body(a_ref, b_ref, c_ref, d_ref, weight_ref, gain_ref, out_ref):
    refs = (a_ref, b_ref, c_ref, d_ref)
    mixed = None
    for m in range(2):
        at = 2 * AV + 8 * m
        levels = []
        for ref in refs:
            parts = ref[at : at + 8, :].astype(F32)
            levels.append(parts[0:1] + parts[1:2] + parts[2:3])
        peak = functools.reduce(jnp.maximum, levels)
        shares = [jnp.exp(level - peak) for level in levels]
        total = functools.reduce(jnp.add, shares)
        summed = None
        for ref, share in zip(refs, shares):
            term = ref[m * AV : (m + 1) * AV, :].astype(F32) * (share / total)
            summed = term if summed is None else summed + term
        mixed = summed if m == 0 else mixed - weight_ref[0] * summed
    scale = lax.rsqrt(jnp.mean(mixed * mixed, axis=0, keepdims=True) + EPS)
    out_ref[...] = ((mixed * scale).T * gain_ref[...]).astype(BF16)


def mix(partials, weight, gain):
    vmem = pl.BlockSpec(memory_space=pltpu.VMEM)
    return pl.pallas_call(
        mix_body,
        in_specs=[vmem] * 4 + [pl.BlockSpec(memory_space=pltpu.SMEM), vmem],
        out_specs=vmem,
        out_shape=jax.ShapeDtypeStruct((TOK, AV), BF16),
        name="mix",
    )(*partials, weight, gain.reshape(1, AV))


def link(earlier, later):
    return (earlier[0] * later[0], later[0][..., None] * earlier[1] + later[1])


def fold(entries, passed, order):
    decay = jnp.ones((HK,), F32)
    state = jnp.zeros((HK, HV), F32)
    for k in order:
        new = link((decay, state), entries[k])
        decay = jnp.where(passed[k], new[0], decay)
        state = jnp.where(passed[k], new[1], state)
    return decay, state


def along(value, axis, size):
    return [value] + [shift(value, axis, k, size) for k in range(1, size)]


def entering_states(fwd, bwd):
    def pack(f, b):
        return jnp.concatenate([f[1], b[1], f[0][None], b[0][None], jnp.zeros((6, HV), F32)]).astype(BF16)

    def unpack(p):
        p = p.astype(F32)
        return (p[2 * HK], p[:HK]), (p[2 * HK + 1], p[HK : 2 * HK])

    before = after = None
    subtotal = (fwd, bwd)
    for axis, size in (("x", NX), ("z", NZ)):
        place = lax.axis_index(axis)
        entries = [unpack(p) for p in along(pack(*subtotal), axis, size)]
        below = [(k <= place) & (k > 0) for k in range(size)]
        above = [k > place for k in range(size)]
        f_below = fold([e[0] for e in entries], below, range(size - 1, 0, -1))
        b_above = fold([e[1] for e in entries], above, range(1, size))
        if before is None:
            f_above = fold([e[0] for e in entries], above, range(size - 1, 0, -1))
            b_below = fold([e[1] for e in entries], below, range(1, size))
            subtotal = (
                link(link(f_below, entries[0][0]), f_above),
                link(link(b_above, entries[0][1]), b_below),
            )
            before, after = f_below, b_above
        else:
            before = link(f_below, before)
            after = link(b_above, after)
    return before[1], after[1]


def on_device(
    tokens,
    norm_gain,
    rec_query,
    fwd_gate,
    bwd_gate,
    rec_value,
    gate_leak,
    log_decay,
    rec_gain,
    att_query,
    att_key,
    att_value,
    lambdas,
    att_gain,
    out_rec,
    out_att,
):
    normed = rms_scale(tokens.astype(F32), norm_gain).astype(BF16)
    weights_all = (att_key, att_value, att_query, rec_query, fwd_gate, bwd_gate, rec_value)
    joined = jnp.concatenate(weights_all, axis=1)
    projected = jnp.dot(gather_rows(normed), joined, preferred_element_type=F32).astype(BF16)
    length = projected.shape[0]
    att_key_raw, att_value_raw, att_query_raw, query_raw, fwd_raw, bwd_raw, value_raw = jnp.split(
        projected, 7, axis=1
    )
    positions = (lax.axis_index(SP) * length + jnp.arange(length, dtype=jnp.int32)).astype(F32)
    att_keys = rotate(att_key_raw.astype(F32).reshape(length, 2, AK), positions).astype(BF16)
    own_kv = jnp.concatenate([att_keys.reshape(length, 2 * AK), att_value_raw], axis=1)
    att_queries = (
        rotate(att_query_raw.astype(F32).reshape(length, 2, AK), positions) * AK ** (-0.5)
    ).astype(BF16)
    own_q = att_queries.reshape(length, 2 * AK).T

    queries_all = jnp.concatenate(
        [own_q, shift(own_q, "x", 1, NX), shift(own_q, "x", -1, NX), shift(own_q, "x", 2, NX)],
        axis=1,
    )
    ups, downs = [own_kv], [own_kv]
    for step in range(NZ // 2):
        ups.append(shift(ups[-1], "z", 1, NZ))
        if step < NZ // 2 - 1:
            downs.append(shift(downs[-1], "z", -1, NZ))

    def split_heads(table):
        return table.astype(F32)[None]

    queries = jax.nn.silu(split_heads(query_raw))
    values = split_heads(value_raw)
    key_fwd = gate_leak[0] * jax.nn.sigmoid(-split_heads(fwd_raw))
    key_bwd = gate_leak[1] * jax.nn.sigmoid(-split_heads(bwd_raw))
    log_fwd = jnp.log1p(-key_fwd) + log_decay[0].T[:, :, None]
    log_bwd = jnp.log1p(-key_bwd) + log_decay[1].T[:, :, None]
    out_fwd, decay_fwd, ending_fwd, read_fwd = local_direction(queries, key_fwd, values, log_fwd)
    out_back, decay_bwd, ending_bwd, read_bwd = local_direction(
        jnp.flip(queries, 1), jnp.flip(key_bwd, 1), jnp.flip(values, 1), jnp.flip(log_bwd, 1)
    )
    entry_fwd, entry_bwd = entering_states(
        (decay_fwd[0], ending_fwd[0]), (decay_bwd[0], ending_bwd[0])
    )

    state = attend(queries_all, [ups[0], ups[1], downs[1]])
    state = attend(queries_all, [ups[2], downs[2]], state)
    sends = attend(queries_all, [ups[3], downs[3], ups[4]], state, last=True)[0]
    partials = [
        sends[0],
        shift(sends[1], "x", -1, NX),
        shift(sends[2], "x", 1, NX),
        shift(sends[3], "x", -2, NX),
    ]
    att_rows = mix(partials, lambdas, att_gain)

    out_fwd = out_fwd[0] + jnp.dot(read_fwd[0], entry_fwd)
    out_back = out_back[0] + jnp.dot(read_bwd[0], entry_bwd)
    rec_rows = rms_scale(out_fwd + jnp.flip(out_back, 0), rec_gain).astype(BF16)
    rows = jnp.stack([rec_rows, att_rows], axis=1).reshape(8, length // 8, 2, HV)
    swapped = lax.all_to_all(rows, TP, split_axis=0, concat_axis=0, tiled=True)
    rec_all = swapped[:, :, 0].transpose(1, 0, 2).reshape(length // 8, -1)
    att_all = swapped[:, :, 1].transpose(1, 0, 2).reshape(length // 8, -1)
    projected_out = jnp.dot(rec_all, out_rec, preferred_element_type=F32) + jnp.dot(
        att_all, out_att, preferred_element_type=F32
    )
    return projected_out.astype(BF16)


def solution(mesh):
    torus = Mesh(mesh.devices.reshape(NZ, NX, NY, NC), AXES)
    in_specs = (
        P(AXES, None),
        P(),
        P(None, TP),
        P(None, TP),
        P(None, TP),
        P(None, TP),
        P(None, TP),
        P(None, SP, TP),
        P(),
        P(None, TP),
        P(None, TP),
        P(None, TP),
        P(TP),
        P(),
        P(),
        P(),
    )
    out_specs = P(AXES, None)
    return jax.shard_map(
        on_device, mesh=torus, in_specs=in_specs, out_specs=out_specs, check_vma=False
    )
```

time: 372 us -> 180 us (0.48)
  matrix products: 106 us -> 12.3 us
  blocking collectives: 67.4 us -> 14.8 us
  local copies, waits for them, and re-layouts: 70.9 us -> 28.6 us
  other arithmetic: 60.9 us -> 20.2 us
  Pallas kernels: 0 us -> 31.2 us
  starting transfers between devices: 28.3 us -> 47.6 us
  between operations: 14.7 us -> 1.53 us
    dot_general x37 -> x5, matrix products: 105 us -> 9.81 us  [the longest x1 3.03 us: on_device(): jnp.dot(rec_all, out_rec, preferred_element_type=F32)]
    all_gather x4 -> x0, blocking collectives: 67.4 us -> none  [all_in_one(): both, at, found = (lax.all_gather(jnp.concatenate(lines), axis), 0, {})]
    reduce_sum x17 -> x0, other arithmetic: 48 us -> none  [the longest x16 46.8 us: absorb(): totals = totals * shrink + jnp.sum(weights_raw, axis=-1)]
    ppermute x0 -> x28, starting transfers between devices: none -> 47.6 us  [shift(): lax.ppermute(value, axis, [(i, (i + by) % size) for i in range(size)])]
    pallas_call x0 -> x4, Pallas kernels: none -> 31.2 us  [the longest x3 28.9 us: attend(): pl.pallas_call(body, grid=(tiles,), in_specs=in_specs, out_specs=out_spec...]
    all_to_all x3 -> x0, starting transfers between devices: 28.3 us -> none  [the longest x1 16.7 us: on_device(): lax.all_to_all(rec_rows, 'tp', split_axis=0, concat_axis=1, tiled=True)]
    ppermute x0 -> x28, waiting for transfers between devices: none -> 21.5 us  [shift(): lax.ppermute(value, axis, [(i, (i + by) % size) for i in range(size)])]
    unnamed x31 -> x59, local copies, waits for them, and re-layouts: 28.8 us -> 8.61 us
  transfers between devices with their start and end apart: 4 -> 28, of which waited for: 2 -> 10; matrix products, arithmetic and copies ran while one was open for 58% -> 14% of each run, Pallas kernels for 0% -> 10%
where the time goes in v1:
time: 180 us; the launch traced here: 178 us
  starting transfers between devices  47.6 us (26%)
  Pallas kernels  31.2 us (17%)
  local copies, waits for them, and re-layouts  28.6 us (16%)
  waiting for transfers between devices  21.5 us (12%)
  other arithmetic  20.2 us (11%)
  blocking collectives  14.8 us (8%)
  matrix products  12.3 us (7%)
    ppermute x28, starting transfers between devices, shift(): lax.ppermute(value, axis, [(i, (i + by) % size) for i in range(size)])  47.6 us
    pallas_call x3, Pallas kernels, attend(): pl.pallas_call(body, grid=(tiles,), in_specs=in_specs, out_specs=out_spec...  28.9 us
    ppermute x28, waiting for transfers between devices, shift(): lax.ppermute(value, axis, [(i, (i + by) % size) for i in range(size)])  21.5 us
    all_to_all x1, blocking collectives, on_device(): swapped = lax.all_to_all(rows, TP, split_axis=0, concat_axis=0, tiled=True)  14.8 us
    mul x16, local copies, waits for them, and re-layouts, advance(): return (factor[..., None] * running + added_state, running)  10.4 us
    unnamed x59, local copies, waits for them, and re-layouts  8.61 us
    convert_element_type x11, other arithmetic, unpack(): p = p.astype(F32)  3.68 us
  transfers between devices with their start and end apart: 28, of which 10 were waited for; matrix products, arithmetic and copies ran while one was open for 14% of the time, Pallas kernels for 10%

profile of v1, /device:TPU:1, one launch (start us, length us, event | category | flops | bytes accessed | tf_op | source)
XLA Modules:
  0.0 178.2 jit_solution(1282694122288672817)
XLA Ops:
  2.5 2.2 %collective-permute-start = (bf16[64,2048]{1,0:T(8,128)(2,1)S(1)}, bf16[64,2048]{1,0:T(8,128)(2,1)}, u32[]{:S(2)}, u32[]{:S(2)}) collective-permute-start(bf16[64,2048]{1,0:T(8,128)(2,1)S(1)} %get-tuple-element.160), channel_id=1, source_target_pairs={{0,2},{2,4},{4,6},{6,0},{1,3},{3,5},{5,7},{7,1},{8,10},{10,12},{12... | collective-permute-start | bytes 786440 | tf_op jit(solution)/shard_map/ppermute | solution.py:32
  10.0 1.9 %constant_dynamic-update-slice_fusion.6 = bf16[2048,896]{1,0:T(8,128)(2,1)} fusion(bf16[2048,128]{1,0:T(8,128)(2,1)} %param.30), kind=kLoop, calls=%fused_computation.229 | loop fusion | bytes 1048576
  20.2 3.4 %collective-permute-start.4 = (bf16[4,64,2048]{2,1,0:T(8,128)(2,1)S(1)}, bf16[4,64,2048]{2,1,0:T(8,128)(2,1)S(1)}, u32[]{:S(2)}, u32[]{:S(2)}) collective-permute-start(bf16[4,64,2048]{2,1,0:T(8,128)(2,1)S(1)} %fusion.14), channel_id=1, source_target_pairs={{0,1},{1,0},{2,3},{3,2},{4,5},{5,4},{6,7},{7,6},{8,9},{9,8},{10,11... | collective-permute-start | bytes 3145736 | tf_op jit(solution)/shard_map/ppermute | solution.py:32
  27.4 2.3 %convolution_convert_fusion = bf16[512,896]{1,0:T(8,128)(2,1)S(1)} fusion(bf16[512,2048]{1,0:T(8,128)(2,1)S(1)} %bitcast.270, bf16[2048,896]{1,0:T(8,128)(2,1)S(1)} %copy-done.19), kind=kOutput, calls=%fused_computation.10 | convolution fusion | flops 1879506944 | bytes 6684672 | tf_op jit(solution)/shard_map/dot_general | solution.py:326
  34.9 6.2 %while.26 = (s32[]{:T(128)}, f32[1,128,128]{2,1,0:T(8,128)S(1)}, bf16[8,1,128,128]{3,2,1,0:T(8,128)(2,1)S(1)}, f32[8,1,128]{2,1,0:T(1,128)}, f32[8,1,128,128]{3,2,1,0:T(8,128)S(1)}, /*index=5*/s32[]{:T(128)}, s32[]{:T(128)}) while((s32[]{:T(128)}, f32[1,128,128]{2,1,0:T(8,128)S(1)}, bf16[8,1,128,128]{3,2,1,0:T(8,128)(2,1)S(1)}, ...), condition=%wide.region_3.4_spmd.clone, body=%wide.region_2.3_spmd.clone.sunk | while | flops 65539 | bytes 296548 | solution.py:90
  41.1 1.7 reverse.13
  44.4 6.3 %while.27 = (s32[]{:T(128)}, f32[1,128,128]{2,1,0:T(8,128)S(1)}, bf16[8,1,128,128]{3,2,1,0:T(8,128)(2,1)S(1)}, f32[8,1,128]{2,1,0:T(1,128)}, f32[8,1,128,128]{3,2,1,0:T(8,128)S(1)}, /*index=5*/s32[]{:T(128)}, s32[]{:T(128)}) while((s32[]{:T(128)}, f32[1,128,128]{2,1,0:T(8,128)S(1)}, bf16[8,1,128,128]{3,2,1,0:T(8,128)(2,1)S(1)}, ...), condition=%wide.region_7.8_spmd.clone, body=%wide.region_6.7_spmd.clone.sunk | while | flops 65539 | bytes 296548 | solution.py:90
  50.8 1.8 %concatenate.30 = bf16[264,128]{1,0:T(8,128)(2,1)} concatenate(bf16[128,128]{1,0:T(8,128)(2,1)S(1)} %convert_bitcast_fusion.1, bf16[128,128]{1,0:T(8,128)(2,1)S(1)} %convert_bitcast_fusion, bf16[1,128]{1,0:T(2,128)(2,1)S(1)} %convert_bitcast_fusion.3, bf16[1,128]{1,0:T(2,128)(2,1)S(1)} %convert_bitcast_fusion.2, bf16[6,128]{1,0:T(8,128)(2,1)S(1)} %broadcast.262), dimensions={0} | concatenate | bytes 135168 | tf_op jit(solution)/shard_map/concatenate | solution.py:276
  55.8 1.7 subtract_convert_fusion
  57.6 1.9 %collective-permute-start.18 = (bf16[512,256]{1,0:T(8,128)(2,1)S(1)}, bf16[512,256]{1,0:T(8,128)(2,1)S(1)}, u32[]{:S(2)}, u32[]{:S(2)}) collective-permute-start(bf16[512,256]{1,0:T(8,128)(2,1)S(1)} %pad_maximum_fusion.1.refs_1_), channel_id=1, source_target_pairs={{0,32},{32,64},{64,96},{96,128},{128,160},{160,192},{192,224},{224... | collective-permute-start | bytes 786440 | tf_op jit(solution)/shard_map/ppermute | solution.py:32
  59.5 4.0 %collective-permute-start.21 = (bf16[512,256]{1,0:T(8,128)(2,1)S(1)}, bf16[512,256]{1,0:T(8,128)(2,1)S(1)}, u32[]{:S(2)}, u32[]{:S(2)}) collective-permute-start(bf16[512,256]{1,0:T(8,128)(2,1)S(1)} %pad_maximum_fusion.1.refs_1_), channel_id=1, source_target_pairs={{0,224},{32,0},{64,32},{96,64},{128,96},{160,128},{192,160},{224,1... | collective-permute-start | bytes 786440 | tf_op jit(solution)/shard_map/ppermute | solution.py:32
  67.2 1.6 collective-permute-start.15
  74.0 1.8 %collective-permute-start.9 = (bf16[264,128]{1,0:T(8,128)(2,1)S(1)}, bf16[264,128]{1,0:T(8,128)(2,1)S(1)}, u32[]{:S(2)}, u32[]{:S(2)}) collective-permute-start(bf16[264,128]{1,0:T(8,128)(2,1)S(1)} %concatenate.31), channel_id=1, source_target_pairs={{0,64},{32,96},{64,128},{96,160},{128,192},{160,224},{192,0},{224,... | collective-permute-start | bytes 202760 | tf_op jit(solution)/shard_map/ppermute | solution.py:32
  78.8 3.7 %collective-permute-start.11 = (bf16[264,128]{1,0:T(8,128)(2,1)S(1)}, bf16[264,128]{1,0:T(8,128)(2,1)S(1)}, u32[]{:S(2)}, u32[]{:S(2)}) collective-permute-start(bf16[264,128]{1,0:T(8,128)(2,1)S(1)} %concatenate.31), channel_id=1, source_target_pairs={{0,128},{32,160},{64,192},{96,224},{128,0},{160,32},{192,64},{224,... | collective-permute-start | bytes 202760 | tf_op jit(solution)/shard_map/ppermute | solution.py:32
  82.6 3.3 %collective-permute-start.12 = (bf16[264,128]{1,0:T(8,128)(2,1)S(1)}, bf16[264,128]{1,0:T(8,128)(2,1)S(1)}, u32[]{:S(2)}, u32[]{:S(2)}) collective-permute-start(bf16[264,128]{1,0:T(8,128)(2,1)S(1)} %concatenate.31), channel_id=1, source_target_pairs={{0,160},{32,192},{64,224},{96,0},{128,32},{160,64},{192,96},{224,1... | collective-permute-start | bytes 202760 | tf_op jit(solution)/shard_map/ppermute | solution.py:32
  88.2 5.4 %collective-permute-done.13 = bf16[264,128]{1,0:T(8,128)(2,1)S(1)} collective-permute-done((bf16[264,128]{1,0:T(8,128)(2,1)S(1)}, bf16[264,128]{1,0:T(8,128)(2,1)S(1)}, u32[]{:S(2)}, u32[]{:S(2)}) %collective-permute-start.13) | collective-permute-done | bytes 67616 | tf_op jit(solution)/shard_map/ppermute | solution.py:32
  94.1 2.5 %collective-permute-start.19 = (bf16[512,256]{1,0:T(8,128)(2,1)S(1)}, bf16[512,256]{1,0:T(8,128)(2,1)S(1)}, u32[]{:S(2)}, u32[]{:S(2)}) collective-permute-start(bf16[512,256]{1,0:T(8,128)(2,1)S(1)} %collective-permute-done.18.refs_2_), channel_id=1, source_target_pairs={{0,32},{32,64},{64,96},{96,128},{128,160},{160,192},{192,224},{224... | collective-permute-start | bytes 786440 | tf_op jit(solution)/shard_map/ppermute | solution.py:32
  98.2 1.8 collective-permute-start.22
  100.0 1.7 collective-permute-done.19.refs_1_
  103.9 2.5 %collective-permute-start.23 = (bf16[512,256]{1,0:T(8,128)(2,1)S(1)}, bf16[512,256]{1,0:T(8,128)(2,1)S(1)}, u32[]{:S(2)}, u32[]{:S(2)}) collective-permute-start(bf16[512,256]{1,0:T(8,128)(2,1)S(1)} %collective-permute-done.22.refs_2_), channel_id=1, source_target_pairs={{0,224},{32,0},{64,32},{96,64},{128,96},{160,128},{192,160},{224,1... | collective-permute-start | bytes 786440 | tf_op jit(solution)/shard_map/ppermute | solution.py:32
  106.4 1.7 collective-permute-done.20.refs_1_
  108.1 10.4 %attend.3 = (f32[2,8,2048]{2,1,0:T(8,128)S(1)}, f32[2,144,2048]{2,1,0:T(8,128)S(1)}) custom-call(bf16[128,2048]{1,0:T(8,128)(2,1)S(1)} %pad_maximum_fusion.refs_0_, bf16[512,256]{1,0:T(8,128)(2,1)S(1)} %pad_maximum_fusion.1.refs_1_, bf16[512,256]{1,0:T(8,128)(2,1)S(1)} %collective-permute-done.18.refs_2_, bf16[512,256]{1,0:T(8,128)(2,1)S(1)} %collective-permute-done.21.refs_3_), custom_call_target="tpu_custom_call" | custom-call | flops 2415919104 | bytes 4194304 | tf_op jit(solution)/shard_map/attend/pallas_call | solution.py:209
  118.5 7.5 %attend.4 = (f32[2,8,2048]{2,1,0:T(8,128)S(1)}, f32[2,144,2048]{2,1,0:T(8,128)S(1)}) custom-call(bf16[128,2048]{1,0:T(8,128)(2,1)S(1)} %pad_maximum_fusion.refs_0_, bf16[512,256]{1,0:T(8,128)(2,1)S(1)} %collective-permute-done.19.refs_1_, bf16[512,256]{1,0:T(8,128)(2,1)S(1)} %collective-permute-done.22.refs_2_, f32[2,8,2048]{2,1,0:T(8,128)S(1)} %get-tuple-element.69.refs_3_, ...), custom_call_target="tpu_custom_call" | custom-call | flops 1610612736 | bytes 4194304 | tf_op jit(solution)/shard_map/attend/pallas_call | solution.py:209
  126.1 10.9 %attend.5 = bf16[4,272,512]{2,1,0:T(8,128)(2,1)S(1)} custom-call(bf16[128,2048]{1,0:T(8,128)(2,1)S(1)} %pad_maximum_fusion.refs_0_, bf16[512,256]{1,0:T(8,128)(2,1)S(1)} %collective-permute-done.20.refs_1_, bf16[512,256]{1,0:T(8,128)(2,1)S(1)} %collective-permute-done.23.refs_2_, bf16[512,256]{1,0:T(8,128)(2,1)S(1)} %collective-permute-done.24.refs_3_, ...), custom_call_target="tpu_custom_call" | custom-call | flops 2415919104 | bytes 4194304 | tf_op jit(solution)/shard_map/attend/pallas_call | solution.py:209
  137.8 3.8 %collective-permute-start.25 = (bf16[272,512]{1,0:T(8,128)(2,1)S(1)}, bf16[272,512]{1,0:T(8,128)(2,1)S(1)}, u32[]{:S(2)}, u32[]{:S(2)}) collective-permute-start(bf16[272,512]{1,0:T(8,128)(2,1)S(1)} %get-tuple-element.163), channel_id=1, source_target_pairs={{0,24},{8,0},{16,8},{24,16},{1,25},{9,1},{17,9},{25,17},{2,26},{10... | collective-permute-start | bytes 835592 | tf_op jit(solution)/shard_map/ppermute | solution.py:32
  141.6 2.2 %collective-permute-start.26 = (bf16[272,512]{1,0:T(8,128)(2,1)S(1)}, bf16[272,512]{1,0:T(8,128)(2,1)S(1)}, u32[]{:S(2)}, u32[]{:S(2)}) collective-permute-start(bf16[272,512]{1,0:T(8,128)(2,1)S(1)} %get-tuple-element.162), channel_id=1, source_target_pairs={{0,8},{8,16},{16,24},{24,0},{1,9},{9,17},{17,25},{25,1},{2,10},{10... | collective-permute-start | bytes 835592 | tf_op jit(solution)/shard_map/ppermute | solution.py:32
  143.8 1.8 %collective-permute-start.27 = (bf16[272,512]{1,0:T(8,128)(2,1)S(1)}, bf16[272,512]{1,0:T(8,128)(2,1)S(1)}, u32[]{:S(2)}, u32[]{:S(2)}) collective-permute-start(bf16[272,512]{1,0:T(8,128)(2,1)S(1)} %get-tuple-element.161), channel_id=1, source_target_pairs={{0,16},{8,24},{16,0},{24,8},{1,17},{9,25},{17,1},{25,9},{2,18},{10... | collective-permute-start | bytes 835592 | tf_op jit(solution)/shard_map/ppermute | solution.py:32
  145.7 2.8 %collective-permute-done.25.b_ref = bf16[272,512]{1,0:T(8,128)(2,1)S(1)} collective-permute-done((bf16[272,512]{1,0:T(8,128)(2,1)S(1)}, bf16[272,512]{1,0:T(8,128)(2,1)S(1)}, u32[]{:S(2)}, u32[]{:S(2)}) %collective-permute-start.25) | collective-permute-done | bytes 278560 | tf_op jit(solution)/shard_map/ppermute | solution.py:32
  148.6 6.1 %collective-permute-done.27.d_ref = bf16[272,512]{1,0:T(8,128)(2,1)S(1)} collective-permute-done((bf16[272,512]{1,0:T(8,128)(2,1)S(1)}, bf16[272,512]{1,0:T(8,128)(2,1)S(1)}, u32[]{:S(2)}, u32[]{:S(2)}) %collective-permute-start.27) | collective-permute-done | bytes 278560 | tf_op jit(solution)/shard_map/ppermute | solution.py:32
  155.4 2.3 %mix.1 = bf16[512,128]{1,0:T(8,128)(2,1)} custom-call(bf16[272,512]{1,0:T(8,128)(2,1)} %get-tuple-element.164.a_ref, bf16[272,512]{1,0:T(8,128)(2,1)} %copy-done.16, bf16[272,512]{1,0:T(8,128)(2,1)} %copy-done.17, bf16[272,512]{1,0:T(8,128)(2,1)} %copy-done.18, f32[1]{0:T(128)S(6)} %copy.172.weight_ref, f32[1,128]{1,0:T(1,128)} %bitcast.292), custom_call_target="tpu_custom_call" | custom-call | tf_op jit(solution)/shard_map/mix/pallas_call | solution.py:247
  158.8 14.8 %all_to_all.5 = bf16[8,64,2,128]{3,1,2,0:T(8,128)(2,1)S(1)} all-to-all(bf16[8,64,2,128]{3,1,2,0:T(8,128)(2,1)S(1)} %pad_maximum_fusion.2), channel_id=1, replica_groups=mesh['z'=8,'x'=4,'y'=4,'c'=2] {'y','c'}, dimensions={0} | all-to-all | bytes 524288 | tf_op jit(solution)/shard_map/all_to_all | solution.py:381
  173.6 3.0 %fusion.52 = f32[64,2048]{1,0:T(8,128)S(1)} fusion(bf16[1024,2048]{1,0:T(8,128)(2,1)} %param.34, bf16[8,8,8,128]{3,2,1,0:T(8,128)(2,1)S(1)} %get-tuple-element.201), kind=kOutput, calls=%fused_computation.98 | convolution fusion | flops 268435456 | bytes 4849664 | tf_op jit(solution)/shard_map/dot_general | solution.py:384
  (233 shorter events, 63.6 us)
Async XLA Ops:
  2.5 14.6 %collective-permute-start = (bf16[64,2048]{1,0:T(8,128)(2,1)S(1)}, bf16[64,2048]{1,0:T(8,128)(2,1)}, u32[]{:S(2)}, u32[]{:S(2)}) collective-permute-start(bf16[64,2048]{1,0:T(8,128)(2,1)S(1)} %get-tuple-element.160), channel_id=1, source_target_pairs={{0,2},{2,4},{4,6},{6,0},{1,3},{3,5},{5,7},{7,1},{8,10},{10,12},{12... | collective-permute-start | bytes 786440 | tf_op jit(solution)/shard_map/ppermute | solution.py:32
  4.7 13.4 %collective-permute-start.1 = (bf16[64,2048]{1,0:T(8,128)(2,1)S(1)}, bf16[64,2048]{1,0:T(8,128)(2,1)}, u32[]{:S(2)}, u32[]{:S(2)}) collective-permute-start(bf16[64,2048]{1,0:T(8,128)(2,1)S(1)} %get-tuple-element.160), channel_id=1, source_target_pairs={{0,6},{2,0},{4,2},{6,4},{1,7},{3,1},{5,3},{7,5},{8,14},{10,8},{12,... | collective-permute-start | bytes 786440 | tf_op jit(solution)/shard_map/ppermute | solution.py:32
  7.0 12.2 %collective-permute-start.2 = (bf16[32,2048]{1,0:T(8,128)(2,1)}, bf16[32,2048]{1,0:T(8,128)(2,1)}, u32[]{:S(2)}, u32[]{:S(2)}) collective-permute-start(bf16[32,2048]{1,0:T(8,128)(2,1)} %get-tuple-element.212), channel_id=1, source_target_pairs={{0,4},{2,6},{4,0},{6,2},{1,5},{3,7},{5,1},{7,3},{8,12},{10,14},{12... | collective-permute-start | bytes 393224 | tf_op jit(solution)/shard_map/ppermute | solution.py:32
  8.5 10.6 %collective-permute-start.3 = (bf16[32,2048]{1,0:T(8,128)(2,1)}, bf16[32,2048]{1,0:T(8,128)(2,1)}, u32[]{:S(2)}, u32[]{:S(2)}) collective-permute-start(bf16[32,2048]{1,0:T(8,128)(2,1)} %get-tuple-element.213), channel_id=1, source_target_pairs={{0,4},{2,6},{4,0},{6,2},{1,5},{3,7},{5,1},{7,3},{8,12},{10,14},{12... | collective-permute-start | bytes 393224 | tf_op jit(solution)/shard_map/ppermute | solution.py:32
  20.2 5.7 %collective-permute-start.4 = (bf16[4,64,2048]{2,1,0:T(8,128)(2,1)S(1)}, bf16[4,64,2048]{2,1,0:T(8,128)(2,1)S(1)}, u32[]{:S(2)}, u32[]{:S(2)}) collective-permute-start(bf16[4,64,2048]{2,1,0:T(8,128)(2,1)S(1)} %fusion.14), channel_id=1, source_target_pairs={{0,1},{1,0},{2,3},{3,2},{4,5},{5,4},{6,7},{7,6},{8,9},{9,8},{10,11... | collective-permute-start | bytes 3145736 | tf_op jit(solution)/shard_map/ppermute | solution.py:32
  44.1 20.2 %copy-start.13 = (bf16[8,64,128]{2,0,1:T(8,128)(2,1)S(1)}, bf16[8,64,128]{2,0,1:T(8,128)(2,1)}, u32[]{:S(2)}) copy-start(bf16[8,64,128]{2,0,1:T(8,128)(2,1)} %get-tuple-element.182) | copy-start | bytes 393220
  44.1 20.2 %copy-start.14 = (bf16[8,64,128]{2,0,1:T(8,128)(2,1)S(1)}, bf16[8,64,128]{2,0,1:T(8,128)(2,1)}, u32[]{:S(2)}) copy-start(bf16[8,64,128]{2,0,1:T(8,128)(2,1)} %get-tuple-element.198) | copy-start | bytes 393220
  52.6 14.6 %collective-permute-start.5 = (bf16[264,128]{1,0:T(8,128)(2,1)}, bf16[264,128]{1,0:T(8,128)(2,1)}, u32[]{:S(2)}, u32[]{:S(2)}) collective-permute-start(bf16[264,128]{1,0:T(8,128)(2,1)} %concatenate.30), channel_id=1, source_target_pairs={{0,24},{8,0},{16,8},{24,16},{1,25},{9,1},{17,9},{25,17},{2,26},{10... | collective-permute-start | bytes 202760 | tf_op jit(solution)/shard_map/ppermute | solution.py:32
  53.4 16.3 %collective-permute-start.6 = (bf16[264,128]{1,0:T(8,128)(2,1)}, bf16[264,128]{1,0:T(8,128)(2,1)}, u32[]{:S(2)}, u32[]{:S(2)}) collective-permute-start(bf16[264,128]{1,0:T(8,128)(2,1)} %concatenate.30), channel_id=1, source_target_pairs={{0,16},{8,24},{16,0},{24,8},{1,17},{9,25},{17,1},{25,9},{2,18},{10... | collective-permute-start | bytes 202760 | tf_op jit(solution)/shard_map/ppermute | solution.py:32
  53.9 17.9 %collective-permute-start.7 = (bf16[264,128]{1,0:T(8,128)(2,1)}, bf16[264,128]{1,0:T(8,128)(2,1)}, u32[]{:S(2)}, u32[]{:S(2)}) collective-permute-start(bf16[264,128]{1,0:T(8,128)(2,1)} %concatenate.30), channel_id=1, source_target_pairs={{0,8},{8,16},{16,24},{24,0},{1,9},{9,17},{17,25},{25,1},{2,10},{10... | collective-permute-start | bytes 202760 | tf_op jit(solution)/shard_map/ppermute | solution.py:32
  57.6 36.5 %collective-permute-start.18 = (bf16[512,256]{1,0:T(8,128)(2,1)S(1)}, bf16[512,256]{1,0:T(8,128)(2,1)S(1)}, u32[]{:S(2)}, u32[]{:S(2)}) collective-permute-start(bf16[512,256]{1,0:T(8,128)(2,1)S(1)} %pad_maximum_fusion.1.refs_1_), channel_id=1, source_target_pairs={{0,32},{32,64},{64,96},{96,128},{128,160},{160,192},{192,224},{224... | collective-permute-start | bytes 786440 | tf_op jit(solution)/shard_map/ppermute | solution.py:32
  59.5 38.7 %collective-permute-start.21 = (bf16[512,256]{1,0:T(8,128)(2,1)S(1)}, bf16[512,256]{1,0:T(8,128)(2,1)S(1)}, u32[]{:S(2)}, u32[]{:S(2)}) collective-permute-start(bf16[512,256]{1,0:T(8,128)(2,1)S(1)} %pad_maximum_fusion.1.refs_1_), channel_id=1, source_target_pairs={{0,224},{32,0},{64,32},{96,64},{128,96},{160,128},{192,160},{224,1... | collective-permute-start | bytes 786440 | tf_op jit(solution)/shard_map/ppermute | solution.py:32
  66.0 36.4 %copy-start.6 = (bf16[512,128]{1,0:T(8,128)(2,1)S(1)}, bf16[512,128]{1,0:T(8,128)(2,1)}, u32[]{:S(2)}) copy-start(bf16[512,128]{1,0:T(8,128)(2,1)} %get-tuple-element.169) | copy-start | bytes 393220
  67.2 6.7 %collective-permute-start.15 = (bf16[128,512]{1,0:T(8,128)(2,1)S(1)}, bf16[128,512]{1,0:T(8,128)(2,1)S(1)}, u32[]{:S(2)}, u32[]{:S(2)}) collective-permute-start(bf16[128,512]{1,0:T(8,128)(2,1)S(1)} %bitcast.283), channel_id=1, source_target_pairs={{0,8},{8,16},{16,24},{24,0},{1,9},{9,17},{17,25},{25,1},{2,10},{10... | collective-permute-start | bytes 393224 | tf_op jit(solution)/shard_map/ppermute | solution.py:32
  69.7 4.3 %collective-permute-start.16 = (bf16[128,512]{1,0:T(8,128)(2,1)S(1)}, bf16[128,512]{1,0:T(8,128)(2,1)S(1)}, u32[]{:S(2)}, u32[]{:S(2)}) collective-permute-start(bf16[128,512]{1,0:T(8,128)(2,1)S(1)} %bitcast.284), channel_id=1, source_target_pairs={{0,24},{8,0},{16,8},{24,16},{1,25},{9,1},{17,9},{25,17},{2,26},{10... | collective-permute-start | bytes 393224 | tf_op jit(solution)/shard_map/ppermute | solution.py:32
  71.8 5.4 %collective-permute-start.17 = (bf16[128,512]{1,0:T(8,128)(2,1)S(1)}, bf16[128,512]{1,0:T(8,128)(2,1)S(1)}, u32[]{:S(2)}, u32[]{:S(2)}) collective-permute-start(bf16[128,512]{1,0:T(8,128)(2,1)S(1)} %bitcast.285), channel_id=1, source_target_pairs={{0,16},{8,24},{16,0},{24,8},{1,17},{9,25},{17,1},{25,9},{2,18},{10... | collective-permute-start | bytes 393224 | tf_op jit(solution)/shard_map/ppermute | solution.py:32
  73.9 4.9 %collective-permute-start.8 = (bf16[264,128]{1,0:T(8,128)(2,1)S(1)}, bf16[264,128]{1,0:T(8,128)(2,1)S(1)}, u32[]{:S(2)}, u32[]{:S(2)}) collective-permute-start(bf16[264,128]{1,0:T(8,128)(2,1)S(1)} %concatenate.31), channel_id=1, source_target_pairs={{0,32},{32,64},{64,96},{96,128},{128,160},{160,192},{192,224},{224... | collective-permute-start | bytes 202760 | tf_op jit(solution)/shard_map/ppermute | solution.py:32
  74.0 8.6 %collective-permute-start.9 = (bf16[264,128]{1,0:T(8,128)(2,1)S(1)}, bf16[264,128]{1,0:T(8,128)(2,1)S(1)}, u32[]{:S(2)}, u32[]{:S(2)}) collective-permute-start(bf16[264,128]{1,0:T(8,128)(2,1)S(1)} %concatenate.31), channel_id=1, source_target_pairs={{0,64},{32,96},{64,128},{96,160},{128,192},{160,224},{192,0},{224,... | collective-permute-start | bytes 202760 | tf_op jit(solution)/shard_map/ppermute | solution.py:32
  77.2 9.0 %collective-permute-start.10 = (bf16[264,128]{1,0:T(8,128)(2,1)S(1)}, bf16[264,128]{1,0:T(8,128)(2,1)S(1)}, u32[]{:S(2)}, u32[]{:S(2)}) collective-permute-start(bf16[264,128]{1,0:T(8,128)(2,1)S(1)} %concatenate.31), channel_id=1, source_target_pairs={{0,96},{32,128},{64,160},{96,192},{128,224},{160,0},{192,32},{224,... | collective-permute-start | bytes 202760 | tf_op jit(solution)/shard_map/ppermute | solution.py:32
  78.8 9.3 %collective-permute-start.11 = (bf16[264,128]{1,0:T(8,128)(2,1)S(1)}, bf16[264,128]{1,0:T(8,128)(2,1)S(1)}, u32[]{:S(2)}, u32[]{:S(2)}) collective-permute-start(bf16[264,128]{1,0:T(8,128)(2,1)S(1)} %concatenate.31), channel_id=1, source_target_pairs={{0,128},{32,160},{64,192},{96,224},{128,0},{160,32},{192,64},{224,... | collective-permute-start | bytes 202760 | tf_op jit(solution)/shard_map/ppermute | solution.py:32
  82.6 5.6 %collective-permute-start.12 = (bf16[264,128]{1,0:T(8,128)(2,1)S(1)}, bf16[264,128]{1,0:T(8,128)(2,1)S(1)}, u32[]{:S(2)}, u32[]{:S(2)}) collective-permute-start(bf16[264,128]{1,0:T(8,128)(2,1)S(1)} %concatenate.31), channel_id=1, source_target_pairs={{0,160},{32,192},{64,224},{96,0},{128,32},{160,64},{192,96},{224,1... | collective-permute-start | bytes 202760 | tf_op jit(solution)/shard_map/ppermute | solution.py:32
  86.2 7.3 %collective-permute-start.13 = (bf16[264,128]{1,0:T(8,128)(2,1)S(1)}, bf16[264,128]{1,0:T(8,128)(2,1)S(1)}, u32[]{:S(2)}, u32[]{:S(2)}) collective-permute-start(bf16[264,128]{1,0:T(8,128)(2,1)S(1)} %concatenate.31), channel_id=1, source_target_pairs={{0,192},{32,224},{64,0},{96,32},{128,64},{160,96},{192,128},{224,1... | collective-permute-start | bytes 202760 | tf_op jit(solution)/shard_map/ppermute | solution.py:32
  88.1 6.0 %collective-permute-start.14 = (bf16[264,128]{1,0:T(8,128)(2,1)S(1)}, bf16[264,128]{1,0:T(8,128)(2,1)S(1)}, u32[]{:S(2)}, u32[]{:S(2)}) collective-permute-start(bf16[264,128]{1,0:T(8,128)(2,1)S(1)} %concatenate.31), channel_id=1, source_target_pairs={{0,224},{32,0},{64,32},{96,64},{128,96},{160,128},{192,160},{224,1... | collective-permute-start | bytes 202760 | tf_op jit(solution)/shard_map/ppermute | solution.py:32
  94.1 7.5 %collective-permute-start.19 = (bf16[512,256]{1,0:T(8,128)(2,1)S(1)}, bf16[512,256]{1,0:T(8,128)(2,1)S(1)}, u32[]{:S(2)}, u32[]{:S(2)}) collective-permute-start(bf16[512,256]{1,0:T(8,128)(2,1)S(1)} %collective-permute-done.18.refs_2_), channel_id=1, source_target_pairs={{0,32},{32,64},{64,96},{96,128},{128,160},{160,192},{192,224},{224... | collective-permute-start | bytes 786440 | tf_op jit(solution)/shard_map/ppermute | solution.py:32
  98.2 5.7 %collective-permute-start.22 = (bf16[512,256]{1,0:T(8,128)(2,1)S(1)}, bf16[512,256]{1,0:T(8,128)(2,1)S(1)}, u32[]{:S(2)}, u32[]{:S(2)}) collective-permute-start(bf16[512,256]{1,0:T(8,128)(2,1)S(1)} %collective-permute-done.21.refs_3_), channel_id=1, source_target_pairs={{0,224},{32,0},{64,32},{96,64},{128,96},{160,128},{192,160},{224,1... | collective-permute-start | bytes 786440 | tf_op jit(solution)/shard_map/ppermute | solution.py:32
  101.7 6.4 %collective-permute-start.20 = (bf16[512,256]{1,0:T(8,128)(2,1)S(1)}, bf16[512,256]{1,0:T(8,128)(2,1)S(1)}, u32[]{:S(2)}, u32[]{:S(2)}) collective-permute-start(bf16[512,256]{1,0:T(8,128)(2,1)S(1)} %collective-permute-done.19.refs_1_), channel_id=1, source_target_pairs={{0,32},{32,64},{64,96},{96,128},{128,160},{160,192},{192,224},{224... | collective-permute-start | bytes 786440 | tf_op jit(solution)/shard_map/ppermute | solution.py:32
  103.9 22.2 %collective-permute-start.23 = (bf16[512,256]{1,0:T(8,128)(2,1)S(1)}, bf16[512,256]{1,0:T(8,128)(2,1)S(1)}, u32[]{:S(2)}, u32[]{:S(2)}) collective-permute-start(bf16[512,256]{1,0:T(8,128)(2,1)S(1)} %collective-permute-done.22.refs_2_), channel_id=1, source_target_pairs={{0,224},{32,0},{64,32},{96,64},{128,96},{160,128},{192,160},{224,1... | collective-permute-start | bytes 786440 | tf_op jit(solution)/shard_map/ppermute | solution.py:32
  108.1 18.0 %collective-permute-start.24 = (bf16[512,256]{1,0:T(8,128)(2,1)S(1)}, bf16[512,256]{1,0:T(8,128)(2,1)S(1)}, u32[]{:S(2)}, u32[]{:S(2)}) collective-permute-start(bf16[512,256]{1,0:T(8,128)(2,1)S(1)} %collective-permute-done.20.refs_1_), channel_id=1, source_target_pairs={{0,32},{32,64},{64,96},{96,128},{128,160},{160,192},{192,224},{224... | collective-permute-start | bytes 786440 | tf_op jit(solution)/shard_map/ppermute | solution.py:32
  126.1 19.5 %copy-start.23 = (f32[128]{0:T(128)S(1)}, f32[128]{0:T(128)}, u32[]{:S(2)}) copy-start(f32[128]{0:T(128)} %param.28) | copy-start | bytes 1540
  137.8 10.7 %collective-permute-start.25 = (bf16[272,512]{1,0:T(8,128)(2,1)S(1)}, bf16[272,512]{1,0:T(8,128)(2,1)S(1)}, u32[]{:S(2)}, u32[]{:S(2)}) collective-permute-start(bf16[272,512]{1,0:T(8,128)(2,1)S(1)} %get-tuple-element.163), channel_id=1, source_target_pairs={{0,24},{8,0},{16,8},{24,16},{1,25},{9,1},{17,9},{25,17},{2,26},{10... | collective-permute-start | bytes 835592 | tf_op jit(solution)/shard_map/ppermute | solution.py:32
  141.6 6.9 %collective-permute-start.26 = (bf16[272,512]{1,0:T(8,128)(2,1)S(1)}, bf16[272,512]{1,0:T(8,128)(2,1)S(1)}, u32[]{:S(2)}, u32[]{:S(2)}) collective-permute-start(bf16[272,512]{1,0:T(8,128)(2,1)S(1)} %get-tuple-element.162), channel_id=1, source_target_pairs={{0,8},{8,16},{16,24},{24,0},{1,9},{9,17},{17,25},{25,1},{2,10},{10... | collective-permute-start | bytes 835592 | tf_op jit(solution)/shard_map/ppermute | solution.py:32
  143.8 10.9 %collective-permute-start.27 = (bf16[272,512]{1,0:T(8,128)(2,1)S(1)}, bf16[272,512]{1,0:T(8,128)(2,1)S(1)}, u32[]{:S(2)}, u32[]{:S(2)}) collective-permute-start(bf16[272,512]{1,0:T(8,128)(2,1)S(1)} %get-tuple-element.161), channel_id=1, source_target_pairs={{0,16},{8,24},{16,0},{24,8},{1,17},{9,25},{17,1},{25,9},{2,18},{10... | collective-permute-start | bytes 835592 | tf_op jit(solution)/shard_map/ppermute | solution.py:32
  (22 other events, 218.9 us)

commit v2 on v1

v2 whole, which is shorter than its diff:
```python
import functools

import jax
import jax.numpy as jnp
from jax import lax
from jax.experimental import pallas as pl
from jax.experimental.pallas import tpu as pltpu
from jax.sharding import Mesh
from jax.sharding import PartitionSpec as P


HK = 128
HV = 128
AK = 64
AV = 128
BLOCK = 64
NZ, NX, NY, NC = 8, 4, 4, 2
AXES = ("z", "x", "y", "c")
SP = ("z", "x")
TP = ("y", "c")
TOK = 512
ACC_ROWS = 144
SEND_ROWS = 2 * AV + 16
PACK = 784
BF16 = jnp.bfloat16
F32 = jnp.float32

EPS = 1e-06
THETA = 500000.0
LOW = -1e30


def shift(value, axis, by, size):
    return lax.ppermute(value, axis, [(i, (i + by) % size) for i in range(size)])


def gather_rows(rows):
    y, c = lax.axis_index("y"), lax.axis_index("c")
    half = rows.shape[0] // 2
    up = shift(rows, "y", 1, NY)
    down = shift(rows, "y", -1, NY)
    far_low = shift(rows[:half], "y", 2, NY)
    far_high = shift(rows[half:], "y", -2, NY)
    mine = jnp.zeros((NY, *rows.shape), rows.dtype)
    for piece, source in (
        (rows, y),
        (up, (y + 3) % 4),
        (down, (y + 1) % 4),
        (jnp.concatenate([far_low, far_high]), (y + 2) % 4),
    ):
        mine = lax.dynamic_update_slice(mine, piece[None], (source, 0, 0))
    other = shift(mine, "c", 1, NC)
    both = jnp.zeros((NY, NC, *rows.shape), rows.dtype)
    both = lax.dynamic_update_slice(both, mine[:, None], (0, c, 0, 0))
    both = lax.dynamic_update_slice(both, other[:, None], (0, 1 - c, 0, 0))
    return both.reshape(-1, rows.shape[1])


def rms_scale(values, gain):
    return values * lax.rsqrt(jnp.mean(values * values, axis=-1, keepdims=True) + EPS) * gain


VMEM = pl.BlockSpec(memory_space=pltpu.VMEM)
SMEM = pl.BlockSpec(memory_space=pltpu.SMEM)


def columns(n):
    return pl.BlockSpec((TOK, 128), lambda *_: (0, n))


def cost(flops, transcendentals=0):
    return pl.CostEstimate(flops=flops, transcendentals=transcendentals, bytes_accessed=1 << 20)


def rotation_tables(length):
    positions = (lax.axis_index(SP) * length + jnp.arange(length, dtype=jnp.int32)).astype(F32)
    frequency = THETA ** (-(jnp.arange(AK // 2, dtype=F32) * 2.0 / AK))
    angles = positions[:, None] * frequency[None, :]
    cosine, sine = jnp.cos(angles), jnp.sin(angles)
    return (
        jnp.concatenate([cosine] * 4, axis=1),
        jnp.concatenate([-sine, sine, -sine, sine], axis=1),
    )


def rotated(vectors, cosine, sine):
    lane = lax.broadcasted_iota(jnp.int32, vectors.shape, 1)
    half = AK // 2
    partner = jnp.where(
        (lane & half) == 0, pltpu.roll(vectors, 128 - half, 1), pltpu.roll(vectors, half, 1)
    )
    return vectors * cosine + partner * sine


def keys_body(key_ref, value_ref, cos_ref, sin_ref, out_ref):
    out_ref[:, :128] = rotated(key_ref[...].astype(F32), cos_ref[...], sin_ref[...]).astype(BF16)
    out_ref[:, 128:] = value_ref[...]


def make_keys(projected, cosine, sine):
    table = pl.BlockSpec((TOK, 128), lambda i: (0, 0))
    return pl.pallas_call(
        keys_body,
        grid=(1,),
        in_specs=[columns(0), columns(1), table, table],
        out_specs=pl.BlockSpec((TOK, 256), lambda i: (0, 0)),
        out_shape=jax.ShapeDtypeStruct((TOK, 256), BF16),
        cost_estimate=cost(1 << 22),
        name="make_keys",
    )(projected, projected, cosine, sine)


def local_body(
    aq_ref, q_ref, f_ref, b_ref, v_ref, leak_ref, decay_ref, cos_ref, sin_ref,
    pack_ref, out_ref, read_f_ref, read_b_ref,
):
    pack_ref[:TOK, :] = (
        rotated(aq_ref[...].astype(F32), cos_ref[...], sin_ref[...]) * AK ** (-0.5)
    ).astype(BF16)
    raw = q_ref[...].astype(F32)
    queries = raw / (1.0 + jnp.exp(-raw))
    row = lax.broadcasted_iota(jnp.int32, (BLOCK, BLOCK), 0)
    col = lax.broadcasted_iota(jnp.int32, (BLOCK, BLOCK), 1)
    totals = []
    for way, (gate_ref, read_ref) in enumerate(((f_ref, read_f_ref), (b_ref, read_b_ref))):
        keys = leak_ref[way : way + 1, :] / (1.0 + jnp.exp(gate_ref[...].astype(F32)))
        logs = jnp.log1p(-keys) + decay_ref[way]
        reach = (row >= col) if way == 0 else (row <= col)
        sums = jnp.where(reach, 1.0, 0.0)
        middle_row, last_row = (BLOCK // 2 - 1, BLOCK - 1) if way == 0 else (BLOCK // 2, 0)
        state = jnp.zeros((HV, HK), F32)
        before = jnp.zeros((1, HK), F32)
        blocks = range(TOK // BLOCK)
        for n in blocks if way == 0 else reversed(blocks):
            at = slice(n * BLOCK, (n + 1) * BLOCK)
            cumulative = jnp.dot(
                sums, logs[at], precision=lax.Precision.HIGHEST, preferred_element_type=F32
            )
            middle = cumulative[middle_row : middle_row + 1]
            last = cumulative[last_row : last_row + 1]
            scores = lax.dot_general(
                (queries[at] * jnp.exp(cumulative - middle)).astype(BF16),
                (keys[at] * jnp.exp(middle - cumulative)).astype(BF16),
                (((1,), (1,)), ((), ())),
                preferred_element_type=F32,
            )
            scores = jnp.where(reach, scores, 0.0).astype(BF16)
            values = v_ref[at, :]
            out = jnp.dot(scores, values, preferred_element_type=F32)
            read = queries[at] * jnp.exp(cumulative)
            out = out + lax.dot_general(
                read.astype(BF16),
                state.astype(BF16),
                (((1,), (1,)), ((), ())),
                preferred_element_type=F32,
            )
            out_ref[at, :] = out if way == 0 else out_ref[at, :] + out
            read_ref[at, :] = (read * jnp.exp(before)).astype(BF16)
            added = lax.dot_general(
                values,
                (keys[at] * jnp.exp(last - cumulative)).astype(BF16),
                (((0,), (0,)), ((), ())),
                preferred_element_type=F32,
            )
            state = state * jnp.exp(last) + added
            before = before + last
        pack_ref[TOK + way * HV : TOK + (way + 1) * HV, :] = state.astype(BF16)
        totals.append(jnp.exp(before))
    pack_ref[TOK + 2 * HV :, :] = jnp.concatenate(
        [*totals, jnp.zeros((PACK - TOK - 2 * HV - 2, HK), F32)]
    ).astype(BF16)


def make_local(projected, leak, decays, cosine, sine):
    whole = pl.BlockSpec((TOK, 128), lambda i: (0, 0))
    return pl.pallas_call(
        local_body,
        grid=(1,),
        in_specs=[columns(n) for n in range(2, 7)]
        + [pl.BlockSpec((2, 128), lambda i: (0, 0)), pl.BlockSpec((2, TOK, 128), lambda i: (0, 0, 0)), whole, whole],
        out_specs=[pl.BlockSpec((PACK, 128), lambda i: (0, 0)), whole, whole, whole],
        out_shape=[
            jax.ShapeDtypeStruct((PACK, 128), BF16),
            jax.ShapeDtypeStruct((TOK, 128), F32),
            jax.ShapeDtypeStruct((TOK, 128), BF16),
            jax.ShapeDtypeStruct((TOK, 128), BF16),
        ],
        cost_estimate=cost(1 << 28),
        compiler_params=pltpu.CompilerParams(vmem_limit_bytes=32 * 1024 * 1024),
        name="local",
    )(projected, projected, projected, projected, projected, leak, decays, cosine, sine)


def link(earlier, later):
    return (earlier[0] * later[0], later[0] * earlier[1] + later[1])


def pick(condition, new, old):
    return tuple(jnp.where(condition, a, b) for a, b in zip(new, old))


def read_sent(ref, at):
    decays = ref[at + 2 * HV : at + 2 * HV + 16, :].astype(F32)
    return (
        (decays[0:1], ref[at : at + HV, :].astype(F32)),
        (decays[1:2], ref[at + HV : at + 2 * HV, :].astype(F32)),
    )


def write_sent(ref, fwd, bwd):
    ref[:HV, :] = fwd[1].astype(BF16)
    ref[HV : 2 * HV, :] = bwd[1].astype(BF16)
    ref[2 * HV :, :] = jnp.concatenate([fwd[0], bwd[0], jnp.zeros((14, HK), F32)]).astype(BF16)


def write_kept(ref, n, pair):
    ref[n, :HV, :] = pair[1]
    ref[n, HV:, :] = jnp.broadcast_to(pair[0], (8, HK))


def read_kept(ref, n):
    return ref[n, HV : HV + 1, :], ref[n, :HV, :]


def fold_body(place_ref, own_ref, below1_ref, below2_ref, below3_ref, kept_ref, sent_ref):
    place = place_ref[0]
    entries = [read_sent(ref, TOK) for ref in (own_ref, below1_ref, below2_ref, below3_ref)]
    none = (jnp.ones((1, HK), F32), jnp.zeros((HV, HK), F32))

    def fold(way, below, order):
        found = none
        for k in order:
            passed = (place >= k) if below else (place < k)
            found = pick(passed, link(found, entries[k][way]), found)
        return found

    f_below, f_above = fold(0, True, (3, 2, 1)), fold(0, False, (3, 2, 1))
    b_above, b_below = fold(1, False, (1, 2, 3)), fold(1, True, (1, 2, 3))
    fwd = link(link(f_below, entries[0][0]), f_above)
    bwd = link(link(b_above, entries[0][1]), b_below)
    for n, pair in enumerate((fwd, bwd, f_below, b_above)):
        write_kept(kept_ref, n, pair)
    write_sent(sent_ref, fwd, bwd)


KEPT = jax.ShapeDtypeStruct((4, HV + 8, HK), F32)
SENT = jax.ShapeDtypeStruct((2 * HV + 16, HK), BF16)


def fold_x(place, packs):
    return pl.pallas_call(
        fold_body,
        in_specs=[SMEM] + [VMEM] * 4,
        out_specs=[VMEM, VMEM],
        out_shape=[KEPT, SENT],
        cost_estimate=cost(1 << 22),
        name="fold_x",
    )(place, *packs)


def met(lower, kept_ref, received_ref):
    fwd, bwd, before, after = (read_kept(kept_ref, n) for n in range(4))
    peer_f, peer_b = read_sent(received_ref, 0)
    return (
        pick(lower, link(peer_f, fwd), link(fwd, peer_f)),
        pick(lower, link(bwd, peer_b), link(peer_b, bwd)),
        pick(lower, link(peer_f, before), before),
        pick(lower, after, link(peer_b, after)),
    )


def merge_body(lower_ref, kept_ref, received_ref, out_ref, sent_ref):
    pairs = met(lower_ref[0] == 1, kept_ref, received_ref)
    for n, pair in enumerate(pairs):
        write_kept(out_ref, n, pair)
    write_sent(sent_ref, pairs[0], pairs[1])


def merge(lower, kept, received):
    return pl.pallas_call(
        merge_body,
        in_specs=[SMEM, VMEM, VMEM],
        out_specs=[VMEM, VMEM],
        out_shape=[KEPT, SENT],
        cost_estimate=cost(1 << 22),
        name="merge",
    )(lower, kept, received)


def finish_body(lower_ref, kept_ref, received_ref, out_ref, read_f_ref, read_b_ref, gain_ref, rows_ref):
    _, _, before, after = met(lower_ref[0] == 1, kept_ref, received_ref)
    total = out_ref[...]
    for read_ref, (_, state) in ((read_f_ref, before), (read_b_ref, after)):
        total = total + lax.dot_general(
            read_ref[...], state.astype(BF16), (((1,), (1,)), ((), ())), preferred_element_type=F32
        )
    rows_ref[...] = rms_scale(total, gain_ref[...]).astype(BF16)


def finish(lower, kept, received, out, read_f, read_b, gain):
    return pl.pallas_call(
        finish_body,
        in_specs=[SMEM] + [VMEM] * 6,
        out_specs=VMEM,
        out_shape=jax.ShapeDtypeStruct((TOK, HV), BF16),
        cost_estimate=cost(1 << 25),
        name="finish",
    )(lower, kept, received, out, read_f, read_b, gain.reshape(1, HV))


def attend_body(*refs, first, last, chunks, key_block):
    counts = (4 if first else 1, chunks, 0 if first else 2)
    q_refs, kv_refs, state_in = (
        refs[sum(counts[:n]) : sum(counts[: n + 1])] for n in range(3)
    )
    rest = refs[sum(counts) :]
    if last:
        send_ref, k_all, v_all, peaks, accs = rest
    elif first:
        turned_ref, peaks, accs, k_all, v_all = rest
    else:
        peaks, accs, k_all, v_all = rest
    rows = kv_refs[0].shape[0]
    tile = pl.program_id(0)

    @pl.when(tile == 0)
    def _():
        for n, kv in enumerate(kv_refs):
            k_all[n * rows : (n + 1) * rows, :] = kv[:, :128]
            v_all[:AV, n * rows : (n + 1) * rows] = kv[:, 128:].T
        v_all[AV:, :] = jnp.ones((ACC_ROWS - AV, chunks * rows), BF16)

    if first:
        peaks[...] = jnp.full(peaks.shape, LOW, F32)
        accs[...] = jnp.zeros(accs.shape, F32)
        for n, ref in enumerate(q_refs):

            @pl.when(tile == n)
            def _():
                turned_ref[0] = ref[...].T

        both = turned_ref[0]
    else:
        peaks[...] = state_in[0][...]
        accs[...] = state_in[1][...]
        both = q_refs[0][0]
    width = both.shape[-1]
    upper = lax.broadcasted_iota(jnp.int32, (2 * AK, width), 0) < AK
    zero = jnp.zeros_like(both)
    maps = (jnp.where(upper, both, zero), jnp.where(upper, zero, both))

    def absorb(i, unused):
        at = pl.multiple_of(i * key_block, key_block)
        keys = k_all[pl.ds(at, key_block), :]
        values = v_all[:, pl.ds(at, key_block)]
        scores = [jnp.dot(keys, q, preferred_element_type=F32) for q in maps]
        for m in range(2):
            old = peaks[m, 0:1, :]
            new = jnp.maximum(old, jnp.max(scores[m], axis=0, keepdims=True))
            weights = jnp.exp(scores[m] - new).astype(BF16)
            accs[m] = accs[m] * jnp.exp(old - new) + jnp.dot(
                values, weights, preferred_element_type=F32
            )
            peaks[m, 0:1, :] = new
        return 0

    lax.fori_loop(0, chunks * rows // key_block, absorb, 0)
    if last:
        for m in range(2):
            acc = accs[m]
            total = acc[AV : AV + 1, :]
            send_ref[0, m * AV : (m + 1) * AV, :] = (acc[:AV] / total).astype(BF16)
            level = peaks[m, 0:1, :] + jnp.log(total)
            high = level.astype(BF16)
            left = level - high.astype(F32)
            middle = left.astype(BF16)
            low = (left - middle.astype(F32)).astype(BF16)
            at = 2 * AV + 8 * m
            send_ref[0, at : at + 8, :] = jnp.concatenate(
                [high.astype(F32), middle.astype(F32), low.astype(F32), jnp.zeros((5, width), F32)]
            ).astype(BF16)


def attend(queries, pieces, state=None, last=False):
    chunks, rows = len(pieces), pieces[0].shape[0]
    tiles = NX
    count = tiles * TOK
    first = state is None
    kv_spec = pl.BlockSpec((rows, 256), lambda i: (0, 0))
    q_spec = pl.BlockSpec((1, 2 * AK, TOK), lambda i: (i, 0, 0))
    peak_spec = pl.BlockSpec((2, 8, TOK), lambda i: (0, 0, i))
    acc_spec = pl.BlockSpec((2, ACC_ROWS, TOK), lambda i: (0, 0, i))
    state_specs = [peak_spec, acc_spec]
    state_shapes = [
        jax.ShapeDtypeStruct((2, 8, count), F32),
        jax.ShapeDtypeStruct((2, ACC_ROWS, count), F32),
    ]
    scratch = [pltpu.VMEM((chunks * rows, 128), BF16), pltpu.VMEM((ACC_ROWS, chunks * rows), BF16)]
    if first:
        in_specs = [pl.BlockSpec((TOK, 128), lambda i: (0, 0))] * NX + [kv_spec] * chunks
        operands = [*queries, *pieces]
    else:
        in_specs = [q_spec] + [kv_spec] * chunks + state_specs
        operands = [queries, *pieces, *state]
    if last:
        out_specs = [pl.BlockSpec((1, SEND_ROWS, TOK), lambda i: (i, 0, 0))]
        out_shape = [jax.ShapeDtypeStruct((tiles, SEND_ROWS, TOK), BF16)]
        scratch += [pltpu.VMEM((2, 8, TOK), F32), pltpu.VMEM((2, ACC_ROWS, TOK), F32)]
    else:
        out_specs, out_shape = state_specs, state_shapes
        if first:
            out_specs = [q_spec] + out_specs
            out_shape = [jax.ShapeDtypeStruct((tiles, 2 * AK, TOK), BF16)] + out_shape
    key_block = 1024 if chunks == 2 else TOK
    body = functools.partial(
        attend_body, first=first, last=last, chunks=chunks, key_block=key_block
    )
    work = 2 * count * chunks * rows
    return pl.pallas_call(
        body,
        grid=(tiles,),
        in_specs=in_specs,
        out_specs=out_specs,
        out_shape=out_shape,
        scratch_shapes=scratch,
        cost_estimate=cost(work * 2 * (AK + AV), work),
        compiler_params=pltpu.CompilerParams(vmem_limit_bytes=48 * 1024 * 1024),
        name="attend",
    )(*operands)


def mix_body(a_ref, b_ref, c_ref, d_ref, weight_ref, gain_ref, out_ref):
    refs = (a_ref, b_ref, c_ref, d_ref)
    mixed = None
    for m in range(2):
        at = 2 * AV + 8 * m
        levels = []
        for ref in refs:
            parts = ref[at : at + 8, :].astype(F32)
            levels.append(parts[0:1] + parts[1:2] + parts[2:3])
        peak = functools.reduce(jnp.maximum, levels)
        shares = [jnp.exp(level - peak) for level in levels]
        total = functools.reduce(jnp.add, shares)
        summed = None
        for ref, share in zip(refs, shares):
            term = ref[m * AV : (m + 1) * AV, :].astype(F32) * (share / total)
            summed = term if summed is None else summed + term
        mixed = summed if m == 0 else mixed - weight_ref[0] * summed
    scale = lax.rsqrt(jnp.mean(mixed * mixed, axis=0, keepdims=True) + EPS)
    out_ref[...] = ((mixed * scale).T * gain_ref[...]).astype(BF16)


def mix(partials, weight, gain):
    vmem = pl.BlockSpec(memory_space=pltpu.VMEM)
    return pl.pallas_call(
        mix_body,
        in_specs=[vmem] * 4 + [pl.BlockSpec(memory_space=pltpu.SMEM), vmem],
        out_specs=vmem,
        out_shape=jax.ShapeDtypeStruct((TOK, AV), BF16),
        name="mix",
    )(*partials, weight, gain.reshape(1, AV))


def on_device(
    tokens,
    norm_gain,
    rec_query,
    fwd_gate,
    bwd_gate,
    rec_value,
    gate_leak,
    log_decay,
    rec_gain,
    att_query,
    att_key,
    att_value,
    lambdas,
    att_gain,
    out_rec,
    out_att,
):
    z, x = lax.axis_index("z"), lax.axis_index("x")
    decays = jnp.broadcast_to(log_decay, (2, TOK, 128))
    cosine, sine = rotation_tables(TOK)
    weights_all = (att_key, att_value, att_query, rec_query, fwd_gate, bwd_gate, rec_value)
    joined = jnp.concatenate(weights_all, axis=1)
    normed = rms_scale(tokens.astype(F32), norm_gain).astype(BF16)
    projected = jnp.dot(gather_rows(normed), joined, preferred_element_type=F32).astype(BF16)
    own_kv = make_keys(projected, cosine, sine)
    ups, downs = [own_kv], [own_kv]
    for step in range(1, NZ // 2 + 1):
        ups.append(shift(ups[-1], "z", 1, NZ))
        if step < NZ // 2:
            downs.append(shift(downs[-1], "z", -1, NZ))
    pack, out_local, read_f, read_b = make_local(projected, gate_leak, decays, cosine, sine)
    packs = [pack]
    for by in (1, 2, -1):
        packs.append(shift(pack, "x", by, NX))
    kept, sent = fold_x(x.reshape(1), packs)
    turned, *state = attend([packs[0], packs[1], packs[3], packs[2]], [own_kv])
    for bit in (1, 2, 4):
        received = lax.ppermute(sent, "z", [(i, i ^ bit) for i in range(NZ)])
        lower = ((z // bit) % 2).astype(jnp.int32).reshape(1)
        if bit < 4:
            kept, sent = merge(lower, kept, received)
    state = attend(turned, [ups[1], downs[1]], state)
    state = attend(turned, [ups[2], downs[2]], state)
    sends = attend(turned, [ups[3], downs[3], ups[4]], state, last=True)[0]
    half = SEND_ROWS // 2
    far_low = shift(sends[3, :half], "x", 2, NX)
    far_high = shift(sends[3, half:], "x", -2, NX)
    from_above = shift(sends[1], "x", -1, NX)
    from_below = shift(sends[2], "x", 1, NX)
    rec_rows = finish(lower, kept, received, out_local, read_f, read_b, rec_gain)
    rec_all = lax.all_to_all(rec_rows, TP, split_axis=0, concat_axis=1, tiled=True)
    rec_part = jnp.dot(rec_all, out_rec, preferred_element_type=F32)
    far = jnp.concatenate([far_low, far_high])
    att_rows = mix([sends[0], from_above, from_below, far], lambdas, att_gain)
    att_all = lax.all_to_all(att_rows, TP, split_axis=0, concat_axis=1, tiled=True)
    return (rec_part + jnp.dot(att_all, out_att, preferred_element_type=F32)).astype(BF16)


def solution(mesh):
    torus = Mesh(mesh.devices.reshape(NZ, NX, NY, NC), AXES)
    in_specs = (
        P(AXES, None),
        P(),
        P(None, TP),
        P(None, TP),
        P(None, TP),
        P(None, TP),
        P(None, TP),
        P(None, SP, TP),
        P(),
        P(None, TP),
        P(None, TP),
        P(None, TP),
        P(TP),
        P(),
        P(),
        P(),
    )
    out_specs = P(AXES, None)
    return jax.shard_map(
        on_device, mesh=torus, in_specs=in_specs, out_specs=out_specs, check_vma=False
    )
```

time: 180 us -> 157 us (0.87)
  Pallas kernels: 31.2 us -> 48 us
  blocking collectives: 14.8 us -> 0 us
  other arithmetic: 20.2 us -> 6.28 us
  local copies, waits for them, and re-layouts: 28.6 us -> 22.3 us
  matrix products: 12.3 us -> 10.1 us
    ppermute x28 -> x19, starting transfers between devices: 47.6 us -> 29.6 us  [shift(): lax.ppermute(value, axis, [(i, (i + by) % size) for i in range(size)])]
    all_to_all x1 -> x0, blocking collectives: 14.8 us -> none  [on_device(): swapped = lax.all_to_all(rows, TP, split_axis=0, concat_axis=0, tiled=True)]
    pallas_call x0 -> x6, Pallas kernels: none -> 14.3 us  [the longest x1 4.51 us: make_local(): pl.pallas_call(local_body, grid=(1,), in_specs=[columns(n) for n in range...]
    all_to_all x0 -> x2, starting transfers between devices: none -> 13.7 us  [the longest x1 9.54 us: on_device(): lax.all_to_all(rec_rows, TP, split_axis=0, concat_axis=1, tiled=True)]
    mul x23 -> x0, local copies, waits for them, and re-layouts: 10.4 us -> none  [the longest x16 10.4 us: advance(): return (factor[..., None] * running + added_state, running)]
    ppermute x28 -> x19, waiting for transfers between devices: 21.5 us -> 11.8 us  [shift(): lax.ppermute(value, axis, [(i, (i + by) % size) for i in range(size)])]
    unnamed x59 -> x69, local copies, waits for them, and re-layouts: 8.61 us -> 17.9 us
    dot_general x9 -> x1, matrix products: 8.4 us -> 3.02 us  [on_device(): rec_part = jnp.dot(rec_all, out_rec, preferred_element_type=F32)]
  transfers between devices with their start and end apart: 28 -> 24, of which waited for: 10 -> 7; matrix products, arithmetic and copies ran while one was open for 14% -> 10% of each run, Pallas kernels for 10% -> 29%
where the time goes in v2:
time: 157 us; the launch traced here: 156 us
  starting transfers between devices  48 us (31%)
  Pallas kernels  48 us (31%)
  local copies, waits for them, and re-layouts  22.3 us (14%)
  waiting for transfers between devices  20.1 us (13%)
  matrix products  10.1 us (6%)
  other arithmetic  6.28 us (4%)
    pallas_call x4, Pallas kernels, attend(): pl.pallas_call(body, grid=(tiles,), in_specs=in_specs, out_specs=out_spec...  31.3 us
    ppermute x19, starting transfers between devices, shift(): lax.ppermute(value, axis, [(i, (i + by) % size) for i in range(size)])  29.6 us
    unnamed x69, local copies, waits for them, and re-layouts  17.9 us
    ppermute x19, waiting for transfers between devices, shift(): lax.ppermute(value, axis, [(i, (i + by) % size) for i in range(size)])  11.8 us
    all_to_all x1, starting transfers between devices, on_device(): lax.all_to_all(rec_rows, TP, split_axis=0, concat_axis=1, tiled=True)  9.54 us
    ppermute x3, starting transfers between devices, on_device(): received = lax.ppermute(sent, 'z', [(i, i ^ bit) for i in range(NZ)])  4.71 us
    ppermute x3, waiting for transfers between devices, on_device(): received = lax.ppermute(sent, 'z', [(i, i ^ bit) for i in range(NZ)])  4.66 us
    pallas_call x1, Pallas kernels, make_local(): pl.pallas_call(local_body, grid=(1,), in_specs=[columns(n) for n in range...  4.51 us
  transfers between devices with their start and end apart: 24, of which 7 were waited for; matrix products, arithmetic and copies ran while one was open for 10% of the time, Pallas kernels for 29%

profile of v2, /device:TPU:1, one launch (start us, length us, event | category | flops | bytes accessed | tf_op | source)
XLA Modules:
  0.0 155.8 jit_solution(1473581895050104637)
XLA Ops:
  2.5 2.2 %collective-permute-start = (bf16[64,2048]{1,0:T(8,128)(2,1)S(1)}, bf16[64,2048]{1,0:T(8,128)(2,1)}, u32[]{:S(2)}, u32[]{:S(2)}) collective-permute-start(bf16[64,2048]{1,0:T(8,128)(2,1)S(1)} %get-tuple-element.40), channel_id=1, source_target_pairs={{0,2},{2,4},{4,6},{6,0},{1,3},{3,5},{5,7},{7,1},{8,10},{10,12},{12... | collective-permute-start | bytes 786440 | tf_op jit(solution)/shard_map/ppermute | solution.py:34
  9.9 1.9 %constant_dynamic-update-slice_fusion.6 = bf16[2048,896]{1,0:T(8,128)(2,1)} fusion(bf16[2048,128]{1,0:T(8,128)(2,1)} %param.26), kind=kLoop, calls=%fused_computation.37 | loop fusion | bytes 1048576
  19.7 3.2 %collective-permute-start.4 = (bf16[4,64,2048]{2,1,0:T(8,128)(2,1)S(1)}, bf16[4,64,2048]{2,1,0:T(8,128)(2,1)S(1)}, u32[]{:S(2)}, u32[]{:S(2)}) collective-permute-start(bf16[4,64,2048]{2,1,0:T(8,128)(2,1)S(1)} %fusion.4), channel_id=1, source_target_pairs={{0,1},{1,0},{2,3},{3,2},{4,5},{5,4},{6,7},{7,6},{8,9},{9,8},{10,11... | collective-permute-start | bytes 3145736 | tf_op jit(solution)/shard_map/ppermute | solution.py:34
  25.3 3.3 %convolution_convert_fusion.aq_ref.q_ref.f_ref.b_ref.v_ref.key_ref.value_ref = bf16[512,896]{1,0:T(8,128)(2,1)} fusion(bf16[512,2048]{1,0:T(8,128)(2,1)S(1)} %bitcast.58, bf16[2048,896]{1,0:T(8,128)(2,1)S(1)} %constant_dynamic-update-slice_fusion), kind=kOutput, calls=%fused_computation.2 | convolution fusion | flops 1879506944 | bytes 6684672 | tf_op jit(solution)/shard_map/dot_general | solution.py:488
  28.7 2.1 %make_keys.1.refs_4_ = bf16[512,256]{1,0:T(8,128)(2,1)} custom-call(bf16[512,896]{1,0:T(8,128)(2,1)} %convolution_convert_fusion.aq_ref.q_ref.f_ref.b_ref.v_ref.key_ref.value_ref, bf16[512,896]{1,0:T(8,128)(2,1)} %convolution_convert_fusion.aq_ref.q_ref.f_ref.b_ref.v_ref.key_ref.value_ref, f32[512,128]{1,0:T(8,128)} %get-tuple-element.51.cos_ref, ...), custom_call_target="tpu_custom_call" | custom-call | flops 4194304 | bytes 1048576 | tf_op jit(solution)/shard_map/make_keys/pallas_call | solution.py:102
  30.9 3.9 %collective-permute-start.14 = (bf16[512,256]{1,0:T(8,128)(2,1)}, bf16[512,256]{1,0:T(8,128)(2,1)S(1)}, u32[]{:S(2)}, u32[]{:S(2)}) collective-permute-start(bf16[512,256]{1,0:T(8,128)(2,1)} %make_keys.1.refs_4_), channel_id=1, source_target_pairs={{0,224},{32,0},{64,32},{96,64},{128,96},{160,128},{192,160},{224,1... | collective-permute-start | bytes 786440 | tf_op jit(solution)/shard_map/ppermute | solution.py:34
  34.8 6.6 %collective-permute-done.11.refs_1_ = bf16[512,256]{1,0:T(8,128)(2,1)S(1)} collective-permute-done((bf16[512,256]{1,0:T(8,128)(2,1)}, bf16[512,256]{1,0:T(8,128)(2,1)S(1)}, u32[]{:S(2)}, u32[]{:S(2)}) %collective-permute-start.11) | collective-permute-done | bytes 262176 | tf_op jit(solution)/shard_map/ppermute | solution.py:34
  41.6 4.5 %local.1 = (bf16[784,128]{1,0:T(8,128)(2,1)S(1)}, f32[512,128]{1,0:T(8,128)S(1)}, bf16[512,128]{1,0:T(8,128)(2,1)S(1)}, bf16[512,128]{1,0:T(8,128)(2,1)S(1)}) custom-call(bf16[512,896]{1,0:T(8,128)(2,1)S(1)} %copy-done, bf16[512,896]{1,0:T(8,128)(2,1)S(1)} %copy-done, bf16[512,896]{1,0:T(8,128)(2,1)S(1)} %copy-done, bf16[512,896]{1,0:T(8,128)(2,1)S(1)} %copy-done, ...), custom_call_target="tpu_custom_call" | custom-call | flops 268435456 | bytes 1048576 | tf_op jit(solution)/shard_map/local/pallas_call | solution.py:176
  49.4 2.5 %collective-permute-start.6 = (bf16[784,128]{1,0:T(8,128)(2,1)S(1)}, bf16[784,128]{1,0:T(8,128)(2,1)S(1)}, u32[]{:S(2)}, u32[]{:S(2)}) collective-permute-start(bf16[784,128]{1,0:T(8,128)(2,1)S(1)} %get-tuple-element.22.own_ref.refs_0_), channel_id=1, source_target_pairs={{0,16},{8,24},{16,0},{24,8},{1,17},{9,25},{17,1},{25,9},{2,18},{10... | collective-permute-start | bytes 602120 | tf_op jit(solution)/shard_map/ppermute | solution.py:34
  53.0 2.7 %collective-permute-start.15 = (bf16[512,256]{1,0:T(8,128)(2,1)S(1)}, bf16[512,256]{1,0:T(8,128)(2,1)S(1)}, u32[]{:S(2)}, u32[]{:S(2)}) collective-permute-start(bf16[512,256]{1,0:T(8,128)(2,1)S(1)} %collective-permute-done.14.refs_2_), channel_id=1, source_target_pairs={{0,224},{32,0},{64,32},{96,64},{128,96},{160,128},{192,160},{224,1... | collective-permute-start | bytes 786440 | tf_op jit(solution)/shard_map/ppermute | solution.py:34
  55.7 4.6 %collective-permute-done.6.below2_ref.refs_3_ = bf16[784,128]{1,0:T(8,128)(2,1)S(1)} collective-permute-done((bf16[784,128]{1,0:T(8,128)(2,1)S(1)}, bf16[784,128]{1,0:T(8,128)(2,1)S(1)}, u32[]{:S(2)}, u32[]{:S(2)}) %collective-permute-start.6) | collective-permute-done | bytes 200736 | tf_op jit(solution)/shard_map/ppermute | solution.py:34
  61.0 2.1 %fold_x.1 = (f32[4,136,128]{2,1,0:T(8,128)}, bf16[272,128]{1,0:T(8,128)(2,1)}) custom-call(s32[1]{0:T(128)} %bitcast.3.place_ref, bf16[784,128]{1,0:T(8,128)(2,1)} %copy-done.5, bf16[784,128]{1,0:T(8,128)(2,1)} %copy-done.7, bf16[784,128]{1,0:T(8,128)(2,1)} %copy-done.9, bf16[784,128]{1,0:T(8,128)(2,1)} %copy-done.11), custom_call_target="tpu_custom_call" | custom-call | flops 4194304 | bytes 1048576 | tf_op jit(solution)/shard_map/fold_x/pallas_call | solution.py:251
  66.8 4.5 %attend.4 = (bf16[4,128,512]{2,1,0:T(8,128)(2,1)S(1)}, f32[2,8,2048]{2,1,0:T(8,128)S(1)}, f32[2,144,2048]{2,1,0:T(8,128)S(1)}) custom-call(bf16[784,128]{1,0:T(8,128)(2,1)S(1)} %copy-done.6, bf16[784,128]{1,0:T(8,128)(2,1)S(1)} %copy-done.8, bf16[784,128]{1,0:T(8,128)(2,1)S(1)} %copy-done.12, bf16[784,128]{1,0:T(8,128)(2,1)S(1)} %copy-done.10, ...), custom_call_target="tpu_custom_call" | custom-call | flops 805306368 | bytes 1048576 | tf_op jit(solution)/shard_map/attend/pallas_call | solution.py:419
  71.4 2.5 %collective-permute-start.16 = (bf16[512,256]{1,0:T(8,128)(2,1)S(1)}, bf16[512,256]{1,0:T(8,128)(2,1)S(1)}, u32[]{:S(2)}, u32[]{:S(2)}) collective-permute-start(bf16[512,256]{1,0:T(8,128)(2,1)S(1)} %collective-permute-done.15.refs_2_), channel_id=1, source_target_pairs={{0,224},{32,0},{64,32},{96,64},{128,96},{160,128},{192,160},{224,1... | collective-permute-start | bytes 786440 | tf_op jit(solution)/shard_map/ppermute | solution.py:34
  73.8 7.3 %attend.5 = (f32[2,8,2048]{2,1,0:T(8,128)S(1)}, f32[2,144,2048]{2,1,0:T(8,128)S(1)}) custom-call(bf16[4,128,512]{2,1,0:T(8,128)(2,1)S(1)} %get-tuple-element.32.refs_0_, bf16[512,256]{1,0:T(8,128)(2,1)S(1)} %collective-permute-done.11.refs_1_, bf16[512,256]{1,0:T(8,128)(2,1)S(1)} %collective-permute-done.14.refs_2_, ...), custom_call_target="tpu_custom_call" | custom-call | flops 1610612736 | bytes 1048576 | tf_op jit(solution)/shard_map/attend/pallas_call | solution.py:419
  83.2 1.7 %merge.2 = (f32[4,136,128]{2,1,0:T(8,128)}, bf16[272,128]{1,0:T(8,128)(2,1)}) custom-call(s32[1]{0:T(128)} %bitcast.2.lower_ref, f32[4,136,128]{2,1,0:T(8,128)} %get-tuple-element.23.kept_ref, bf16[272,128]{1,0:T(8,128)(2,1)} %copy-done.29), custom_call_target="tpu_custom_call" | custom-call | flops 4194304 | bytes 1048576 | tf_op jit(solution)/shard_map/merge/pallas_call | solution.py:280
  84.9 2.7 %collective-permute-start.9 = (bf16[272,128]{1,0:T(8,128)(2,1)}, bf16[272,128]{1,0:T(8,128)(2,1)S(1)}, u32[]{:S(2)}, u32[]{:S(2)}) collective-permute-start(bf16[272,128]{1,0:T(8,128)(2,1)} %get-tuple-element.26), channel_id=1, source_target_pairs={{0,64},{32,96},{64,0},{96,32},{128,192},{160,224},{192,128},{224,1... | collective-permute-start | bytes 208904 | tf_op jit(solution)/shard_map/ppermute | solution.py:502
  87.6 1.7 %copy-done.17 = f32[2,144,2048]{2,1,0:T(8,128)S(1)} copy-done((f32[2,144,2048]{2,1,0:T(8,128)S(1)}, f32[2,144,2048]{2,1,0:T(8,128)}, u32[]{:S(2)}) %copy-start.17) | copy-done | bytes 2359320
  89.3 7.3 %attend.6 = (f32[2,8,2048]{2,1,0:T(8,128)S(1)}, f32[2,144,2048]{2,1,0:T(8,128)S(1)}) custom-call(bf16[4,128,512]{2,1,0:T(8,128)(2,1)S(1)} %get-tuple-element.32.refs_0_, bf16[512,256]{1,0:T(8,128)(2,1)S(1)} %collective-permute-done.12.refs_1_, bf16[512,256]{1,0:T(8,128)(2,1)S(1)} %collective-permute-done.15.refs_2_, ...), custom_call_target="tpu_custom_call" | custom-call | flops 1610612736 | bytes 1048576 | tf_op jit(solution)/shard_map/attend/pallas_call | solution.py:419
  96.6 12.3 %attend.7 = bf16[4,272,512]{2,1,0:T(8,128)(2,1)S(1)} custom-call(bf16[4,128,512]{2,1,0:T(8,128)(2,1)S(1)} %get-tuple-element.32.refs_0_, bf16[512,256]{1,0:T(8,128)(2,1)S(1)} %collective-permute-done.13.refs_1_, bf16[512,256]{1,0:T(8,128)(2,1)S(1)} %collective-permute-done.16.refs_2_, bf16[512,256]{1,0:T(8,128)(2,1)S(1)} %collective-permute-done.17.refs_3_, ...), custom_call_target="tpu_custom_call" | custom-call | flops 2415919104 | bytes 1048576 | tf_op jit(solution)/shard_map/attend/pallas_call | solution.py:419
  109.6 2.7 %collective-permute-start.18 = (bf16[272,512]{1,0:T(8,128)(2,1)S(1)}, bf16[272,512]{1,0:T(8,128)(2,1)S(1)}, u32[]{:S(2)}, u32[]{:S(2)}) collective-permute-start(bf16[272,512]{1,0:T(8,128)(2,1)S(1)} %get-tuple-element.44), channel_id=1, source_target_pairs={{0,24},{8,0},{16,8},{24,16},{1,25},{9,1},{17,9},{25,17},{2,26},{10... | collective-permute-start | bytes 835592 | tf_op jit(solution)/shard_map/ppermute | solution.py:34
  113.7 1.7 %collective-permute-start.21 = (bf16[136,512]{1,0:T(8,128)(2,1)S(1)}, bf16[136,512]{1,0:T(8,128)(2,1)S(1)}, u32[]{:S(2)}, u32[]{:S(2)}) collective-permute-start(bf16[136,512]{1,0:T(8,128)(2,1)S(1)} %get-tuple-element.42), channel_id=1, source_target_pairs={{0,16},{8,24},{16,0},{24,8},{1,17},{9,25},{17,1},{25,9},{2,18},{10... | collective-permute-start | bytes 417800 | tf_op jit(solution)/shard_map/ppermute | solution.py:34
  116.1 1.8 %merge.3 = (f32[4,136,128]{2,1,0:T(8,128)}, bf16[272,128]{1,0:T(8,128)(2,1)}) custom-call(s32[1]{0:T(128)} %bitcast.1.lower_ref, f32[4,136,128]{2,1,0:T(8,128)} %get-tuple-element.25.kept_ref, bf16[272,128]{1,0:T(8,128)(2,1)} %copy-done.28), custom_call_target="tpu_custom_call" | custom-call | flops 4194304 | bytes 1048576 | tf_op jit(solution)/shard_map/merge/pallas_call | solution.py:280
  117.8 2.0 %collective-permute-start.10 = (bf16[272,128]{1,0:T(8,128)(2,1)}, bf16[272,128]{1,0:T(8,128)(2,1)S(1)}, u32[]{:S(2)}, u32[]{:S(2)}) collective-permute-start(bf16[272,128]{1,0:T(8,128)(2,1)} %get-tuple-element.28), channel_id=1, source_target_pairs={{0,128},{32,160},{64,192},{96,224},{128,0},{160,32},{192,64},{224,... | collective-permute-start | bytes 208904 | tf_op jit(solution)/shard_map/ppermute | solution.py:502
  120.4 4.7 %collective-permute-done.10.received_ref = bf16[272,128]{1,0:T(8,128)(2,1)S(1)} collective-permute-done((bf16[272,128]{1,0:T(8,128)(2,1)}, bf16[272,128]{1,0:T(8,128)(2,1)S(1)}, u32[]{:S(2)}, u32[]{:S(2)}) %collective-permute-start.10) | collective-permute-done | bytes 69664 | tf_op jit(solution)/shard_map/ppermute | solution.py:502
  125.7 2.1 %finish.1 = bf16[512,128]{1,0:T(8,128)(2,1)} custom-call(s32[1]{0:T(128)} %bitcast.lower_ref, f32[4,136,128]{2,1,0:T(8,128)} %get-tuple-element.27.kept_ref, bf16[272,128]{1,0:T(8,128)(2,1)} %copy-done.27, f32[512,128]{1,0:T(8,128)} %copy-done.3, bf16[512,128]{1,0:T(8,128)(2,1)} %copy-done.13, bf16[512,128]{1,0:T(8,128)(2,1)} %copy-done.14, f32[1,128]{1,0:T(1,128)} %bitcast.62), custom_call_target="tpu_custom_call" | custom-call | flops 33554432 | bytes 1048576 | tf_op jit(solution)/shard_map/finish/pallas_call | solution.py:301
  127.9 9.5 %all-to-all-start = ((bf16[8,64,128]{2,1,0:T(8,128)(2,1)}), bf16[8,64,128]{2,1,0:T(8,128)(2,1)S(1)}, u32[]{:S(2)}, u32[]{:S(2)}) async-start(bf16[8,64,128]{2,1,0:T(8,128)(2,1)} %bitcast.59), calls=%async_computation | async-start | bytes 262144 | tf_op jit(solution)/shard_map/all_to_all | solution.py:515
  139.0 2.3 %mix.1 = bf16[512,128]{1,0:T(8,128)(2,1)} custom-call(bf16[272,512]{1,0:T(8,128)(2,1)} %get-tuple-element.45.a_ref, bf16[272,512]{1,0:T(8,128)(2,1)} %copy-done.24, bf16[272,512]{1,0:T(8,128)(2,1)} %copy-done.25, bf16[272,512]{1,0:T(8,128)(2,1)} %pad_maximum_fusion.d_ref, f32[1]{0:T(128)S(6)} %copy.52.weight_ref, f32[1,128]{1,0:T(1,128)} %bitcast.63), custom_call_target="tpu_custom_call" | custom-call | tf_op jit(solution)/shard_map/mix/pallas_call | solution.py:455
  142.6 4.1 %all-to-all-start.1 = ((bf16[8,64,128]{2,1,0:T(8,128)(2,1)}), bf16[8,64,128]{2,1,0:T(8,128)(2,1)S(1)}, u32[]{:S(2)}, u32[]{:S(2)}) async-start(bf16[8,64,128]{2,1,0:T(8,128)(2,1)} %bitcast.60), calls=%async_computation.1 | async-start | bytes 262144 | tf_op jit(solution)/shard_map/all_to_all | solution.py:519
  146.8 3.0 %fusion.7 = f32[64,2048]{1,0:T(8,128)S(1)} fusion(bf16[1024,2048]{1,0:T(8,128)(2,1)} %param.30, bf16[8,64,128]{2,1,0:T(8,128)(2,1)S(1)} %all-to-all-done), kind=kOutput, calls=%fused_computation.27 | convolution fusion | flops 268435456 | bytes 4849664 | tf_op jit(solution)/shard_map/dot_general | solution.py:516
  149.8 2.2 %all-to-all-done.1 = bf16[8,64,128]{2,1,0:T(8,128)(2,1)S(1)} async-done(((bf16[8,64,128]{2,1,0:T(8,128)(2,1)}), bf16[8,64,128]{2,1,0:T(8,128)(2,1)S(1)}, u32[]{:S(2)}, u32[]{:S(2)}) %all-to-all-start.1) | async-done | bytes 131104 | tf_op jit(solution)/shard_map/all_to_all | solution.py:519
  152.0 3.7 %fusion = bf16[64,2048]{1,0:T(8,128)(2,1)} fusion(f32[64,2048]{1,0:T(8,128)S(1)} %fusion.7, bf16[1024,2048]{1,0:T(8,128)(2,1)} %param.31, bf16[8,64,128]{2,1,0:T(8,128)(2,1)S(1)} %all-to-all-done.1), kind=kOutput, calls=%fused_computation.1 | convolution fusion | flops 268697600 | bytes 5111808 | tf_op jit(solution)/shard_map/dot_general | solution.py:520
  (119 shorter events, 35.3 us)
Async XLA Ops:
  0.0 13.7 %copy-start.20 = (bf16[2048,128]{1,0:T(8,128)(2,1)S(1)}, bf16[2048,128]{1,0:T(8,128)(2,1)}, u32[]{:S(2)}) copy-start(bf16[2048,128]{1,0:T(8,128)(2,1)} %param.18) | copy-start | bytes 1572868
  0.0 14.6 %copy-start.21 = (bf16[2048,128]{1,0:T(8,128)(2,1)S(1)}, bf16[2048,128]{1,0:T(8,128)(2,1)}, u32[]{:S(2)}) copy-start(bf16[2048,128]{1,0:T(8,128)(2,1)} %param.19) | copy-start | bytes 1572868
  2.5 13.9 %collective-permute-start = (bf16[64,2048]{1,0:T(8,128)(2,1)S(1)}, bf16[64,2048]{1,0:T(8,128)(2,1)}, u32[]{:S(2)}, u32[]{:S(2)}) collective-permute-start(bf16[64,2048]{1,0:T(8,128)(2,1)S(1)} %get-tuple-element.40), channel_id=1, source_target_pairs={{0,2},{2,4},{4,6},{6,0},{1,3},{3,5},{5,7},{7,1},{8,10},{10,12},{12... | collective-permute-start | bytes 786440 | tf_op jit(solution)/shard_map/ppermute | solution.py:34
  4.7 12.8 %collective-permute-start.1 = (bf16[64,2048]{1,0:T(8,128)(2,1)S(1)}, bf16[64,2048]{1,0:T(8,128)(2,1)}, u32[]{:S(2)}, u32[]{:S(2)}) collective-permute-start(bf16[64,2048]{1,0:T(8,128)(2,1)S(1)} %get-tuple-element.40), channel_id=1, source_target_pairs={{0,6},{2,0},{4,2},{6,4},{1,7},{3,1},{5,3},{7,5},{8,14},{10,8},{12,... | collective-permute-start | bytes 786440 | tf_op jit(solution)/shard_map/ppermute | solution.py:34
  6.9 11.6 %collective-permute-start.2 = (bf16[32,2048]{1,0:T(8,128)(2,1)}, bf16[32,2048]{1,0:T(8,128)(2,1)S(1)}, u32[]{:S(2)}, u32[]{:S(2)}) collective-permute-start(bf16[32,2048]{1,0:T(8,128)(2,1)} %get-tuple-element.46), channel_id=1, source_target_pairs={{0,4},{2,6},{4,0},{6,2},{1,5},{3,7},{5,1},{7,3},{8,12},{10,14},{12... | collective-permute-start | bytes 393224 | tf_op jit(solution)/shard_map/ppermute | solution.py:34
  8.5 10.3 %collective-permute-start.3 = (bf16[32,2048]{1,0:T(8,128)(2,1)}, bf16[32,2048]{1,0:T(8,128)(2,1)}, u32[]{:S(2)}, u32[]{:S(2)}) collective-permute-start(bf16[32,2048]{1,0:T(8,128)(2,1)} %get-tuple-element.47), channel_id=1, source_target_pairs={{0,4},{2,6},{4,0},{6,2},{1,5},{3,7},{5,1},{7,3},{8,12},{10,14},{12... | collective-permute-start | bytes 393224 | tf_op jit(solution)/shard_map/ppermute | solution.py:34
  19.7 5.5 %collective-permute-start.4 = (bf16[4,64,2048]{2,1,0:T(8,128)(2,1)S(1)}, bf16[4,64,2048]{2,1,0:T(8,128)(2,1)S(1)}, u32[]{:S(2)}, u32[]{:S(2)}) collective-permute-start(bf16[4,64,2048]{2,1,0:T(8,128)(2,1)S(1)} %fusion.4), channel_id=1, source_target_pairs={{0,1},{1,0},{2,3},{3,2},{4,5},{5,4},{6,7},{7,6},{8,9},{9,8},{10,11... | collective-permute-start | bytes 3145736 | tf_op jit(solution)/shard_map/ppermute | solution.py:34
  25.3 16.1 %copy-start.30 = (f32[2,512,1]{1,2,0:T(1,128)S(1)}, f32[2,512,1]{1,2,0:T(1,128)}, u32[]{:S(2)}) copy-start(f32[2,512,1]{1,2,0:T(1,128)} %param.23) | copy-start | bytes 12292
  25.3 16.3 %copy-start.1 = (f32[512,128]{1,0:T(8,128)S(1)}, f32[512,128]{1,0:T(8,128)}, u32[]{:S(2)}) copy-start(f32[512,128]{1,0:T(8,128)} %get-tuple-element.51.cos_ref) | copy-start | bytes 786436
  25.3 16.3 %copy-start.2 = (f32[512,128]{1,0:T(8,128)S(1)}, f32[512,128]{1,0:T(8,128)}, u32[]{:S(2)}) copy-start(f32[512,128]{1,0:T(8,128)} %get-tuple-element.52.sin_ref) | copy-start | bytes 786436
  25.3 16.3 %copy-start.15 = (f32[2,128]{1,0:T(2,128)S(1)}, f32[2,128]{1,0:T(2,128)}, u32[]{:S(2)}) copy-start(f32[2,128]{1,0:T(2,128)} %leak_ref.1) | copy-start | bytes 3076
  28.7 13.0 %copy-start = (bf16[512,896]{1,0:T(8,128)(2,1)S(1)}, bf16[512,896]{1,0:T(8,128)(2,1)}, u32[]{:S(2)}) copy-start(bf16[512,896]{1,0:T(8,128)(2,1)} %convolution_convert_fusion.aq_ref.q_ref.f_ref.b_ref.v_ref.key_ref.value_ref) | copy-start | bytes 2752516
  30.8 32.3 %copy-start.4 = (bf16[512,256]{1,0:T(8,128)(2,1)S(1)}, bf16[512,256]{1,0:T(8,128)(2,1)}, u32[]{:S(2)}) copy-start(bf16[512,256]{1,0:T(8,128)(2,1)} %make_keys.1.refs_4_) | copy-start | bytes 786436
  30.8 10.6 %collective-permute-start.11 = (bf16[512,256]{1,0:T(8,128)(2,1)}, bf16[512,256]{1,0:T(8,128)(2,1)S(1)}, u32[]{:S(2)}, u32[]{:S(2)}) collective-permute-start(bf16[512,256]{1,0:T(8,128)(2,1)} %make_keys.1.refs_4_), channel_id=1, source_target_pairs={{0,32},{32,64},{64,96},{96,128},{128,160},{160,192},{192,224},{224... | collective-permute-start | bytes 786440 | tf_op jit(solution)/shard_map/ppermute | solution.py:34
  30.9 22.1 %collective-permute-start.14 = (bf16[512,256]{1,0:T(8,128)(2,1)}, bf16[512,256]{1,0:T(8,128)(2,1)S(1)}, u32[]{:S(2)}, u32[]{:S(2)}) collective-permute-start(bf16[512,256]{1,0:T(8,128)(2,1)} %make_keys.1.refs_4_), channel_id=1, source_target_pairs={{0,224},{32,0},{64,32},{96,64},{128,96},{160,128},{192,160},{224,1... | collective-permute-start | bytes 786440 | tf_op jit(solution)/shard_map/ppermute | solution.py:34
  41.4 14.3 %collective-permute-start.12 = (bf16[512,256]{1,0:T(8,128)(2,1)S(1)}, bf16[512,256]{1,0:T(8,128)(2,1)S(1)}, u32[]{:S(2)}, u32[]{:S(2)}) collective-permute-start(bf16[512,256]{1,0:T(8,128)(2,1)S(1)} %collective-permute-done.11.refs_1_), channel_id=1, source_target_pairs={{0,32},{32,64},{64,96},{96,128},{128,160},{160,192},{192,224},{224... | collective-permute-start | bytes 786440 | tf_op jit(solution)/shard_map/ppermute | solution.py:34
  48.2 7.5 %collective-permute-start.5 = (bf16[784,128]{1,0:T(8,128)(2,1)S(1)}, bf16[784,128]{1,0:T(8,128)(2,1)S(1)}, u32[]{:S(2)}, u32[]{:S(2)}) collective-permute-start(bf16[784,128]{1,0:T(8,128)(2,1)S(1)} %get-tuple-element.22.own_ref.refs_0_), channel_id=1, source_target_pairs={{0,8},{8,16},{16,24},{24,0},{1,9},{9,17},{17,25},{25,1},{2,10},{10... | collective-permute-start | bytes 602120 | tf_op jit(solution)/shard_map/ppermute | solution.py:34
  49.4 10.9 %collective-permute-start.6 = (bf16[784,128]{1,0:T(8,128)(2,1)S(1)}, bf16[784,128]{1,0:T(8,128)(2,1)S(1)}, u32[]{:S(2)}, u32[]{:S(2)}) collective-permute-start(bf16[784,128]{1,0:T(8,128)(2,1)S(1)} %get-tuple-element.22.own_ref.refs_0_), channel_id=1, source_target_pairs={{0,16},{8,24},{16,0},{24,8},{1,17},{9,25},{17,1},{25,9},{2,18},{10... | collective-permute-start | bytes 602120 | tf_op jit(solution)/shard_map/ppermute | solution.py:34
  51.8 8.4 %collective-permute-start.7 = (bf16[784,128]{1,0:T(8,128)(2,1)S(1)}, bf16[784,128]{1,0:T(8,128)(2,1)S(1)}, u32[]{:S(2)}, u32[]{:S(2)}) collective-permute-start(bf16[784,128]{1,0:T(8,128)(2,1)S(1)} %get-tuple-element.22.own_ref.refs_0_), channel_id=1, source_target_pairs={{0,24},{8,0},{16,8},{24,16},{1,25},{9,1},{17,9},{25,17},{2,26},{10... | collective-permute-start | bytes 602120 | tf_op jit(solution)/shard_map/ppermute | solution.py:34
  53.0 18.4 %collective-permute-start.15 = (bf16[512,256]{1,0:T(8,128)(2,1)S(1)}, bf16[512,256]{1,0:T(8,128)(2,1)S(1)}, u32[]{:S(2)}, u32[]{:S(2)}) collective-permute-start(bf16[512,256]{1,0:T(8,128)(2,1)S(1)} %collective-permute-done.14.refs_2_), channel_id=1, source_target_pairs={{0,224},{32,0},{64,32},{96,64},{128,96},{160,128},{192,160},{224,1... | collective-permute-start | bytes 786440 | tf_op jit(solution)/shard_map/ppermute | solution.py:34
  55.7 18.2 %collective-permute-start.13 = (bf16[512,256]{1,0:T(8,128)(2,1)S(1)}, bf16[512,256]{1,0:T(8,128)(2,1)S(1)}, u32[]{:S(2)}, u32[]{:S(2)}) collective-permute-start(bf16[512,256]{1,0:T(8,128)(2,1)S(1)} %collective-permute-done.12.refs_1_), channel_id=1, source_target_pairs={{0,32},{32,64},{64,96},{96,128},{128,160},{160,192},{192,224},{224... | collective-permute-start | bytes 786440 | tf_op jit(solution)/shard_map/ppermute | solution.py:34
  63.1 19.4 %collective-permute-start.8 = (bf16[272,128]{1,0:T(8,128)(2,1)}, bf16[272,128]{1,0:T(8,128)(2,1)S(1)}, u32[]{:S(2)}, u32[]{:S(2)}) collective-permute-start(bf16[272,128]{1,0:T(8,128)(2,1)} %get-tuple-element.24), channel_id=1, source_target_pairs={{0,32},{32,0},{64,96},{96,64},{128,160},{160,128},{192,224},{224,1... | collective-permute-start | bytes 208904 | tf_op jit(solution)/shard_map/ppermute | solution.py:502
  71.4 25.2 %collective-permute-start.16 = (bf16[512,256]{1,0:T(8,128)(2,1)S(1)}, bf16[512,256]{1,0:T(8,128)(2,1)S(1)}, u32[]{:S(2)}, u32[]{:S(2)}) collective-permute-start(bf16[512,256]{1,0:T(8,128)(2,1)S(1)} %collective-permute-done.15.refs_2_), channel_id=1, source_target_pairs={{0,224},{32,0},{64,32},{96,64},{128,96},{160,128},{192,160},{224,1... | collective-permute-start | bytes 786440 | tf_op jit(solution)/shard_map/ppermute | solution.py:34
  73.8 22.7 %collective-permute-start.17 = (bf16[512,256]{1,0:T(8,128)(2,1)S(1)}, bf16[512,256]{1,0:T(8,128)(2,1)S(1)}, u32[]{:S(2)}, u32[]{:S(2)}) collective-permute-start(bf16[512,256]{1,0:T(8,128)(2,1)S(1)} %collective-permute-done.13.refs_1_), channel_id=1, source_target_pairs={{0,32},{32,64},{64,96},{96,128},{128,160},{160,192},{192,224},{224... | collective-permute-start | bytes 786440 | tf_op jit(solution)/shard_map/ppermute | solution.py:34
  84.9 30.5 %collective-permute-start.9 = (bf16[272,128]{1,0:T(8,128)(2,1)}, bf16[272,128]{1,0:T(8,128)(2,1)S(1)}, u32[]{:S(2)}, u32[]{:S(2)}) collective-permute-start(bf16[272,128]{1,0:T(8,128)(2,1)} %get-tuple-element.26), channel_id=1, source_target_pairs={{0,64},{32,96},{64,0},{96,32},{128,192},{160,224},{192,128},{224,1... | collective-permute-start | bytes 208904 | tf_op jit(solution)/shard_map/ppermute | solution.py:502
  109.6 28.5 %collective-permute-start.18 = (bf16[272,512]{1,0:T(8,128)(2,1)S(1)}, bf16[272,512]{1,0:T(8,128)(2,1)S(1)}, u32[]{:S(2)}, u32[]{:S(2)}) collective-permute-start(bf16[272,512]{1,0:T(8,128)(2,1)S(1)} %get-tuple-element.44), channel_id=1, source_target_pairs={{0,24},{8,0},{16,8},{24,16},{1,25},{9,1},{17,9},{25,17},{2,26},{10... | collective-permute-start | bytes 835592 | tf_op jit(solution)/shard_map/ppermute | solution.py:34
  112.3 25.8 %collective-permute-start.19 = (bf16[272,512]{1,0:T(8,128)(2,1)S(1)}, bf16[272,512]{1,0:T(8,128)(2,1)S(1)}, u32[]{:S(2)}, u32[]{:S(2)}) collective-permute-start(bf16[272,512]{1,0:T(8,128)(2,1)S(1)} %get-tuple-element.43), channel_id=1, source_target_pairs={{0,8},{8,16},{16,24},{24,0},{1,9},{9,17},{17,25},{25,1},{2,10},{10... | collective-permute-start | bytes 835592 | tf_op jit(solution)/shard_map/ppermute | solution.py:34
  112.4 25.0 %collective-permute-start.20 = (bf16[136,512]{1,0:T(8,128)(2,1)S(1)}, bf16[136,512]{1,0:T(8,128)(2,1)S(1)}, u32[]{:S(2)}, u32[]{:S(2)}) collective-permute-start(bf16[136,512]{1,0:T(8,128)(2,1)S(1)} %get-tuple-element.41), channel_id=1, source_target_pairs={{0,16},{8,24},{16,0},{24,8},{1,17},{9,25},{17,1},{25,9},{2,18},{10... | collective-permute-start | bytes 417800 | tf_op jit(solution)/shard_map/ppermute | solution.py:34
  113.7 23.7 %collective-permute-start.21 = (bf16[136,512]{1,0:T(8,128)(2,1)S(1)}, bf16[136,512]{1,0:T(8,128)(2,1)S(1)}, u32[]{:S(2)}, u32[]{:S(2)}) collective-permute-start(bf16[136,512]{1,0:T(8,128)(2,1)S(1)} %get-tuple-element.42), channel_id=1, source_target_pairs={{0,16},{8,24},{16,0},{24,8},{1,17},{9,25},{17,1},{25,9},{2,18},{10... | collective-permute-start | bytes 417800 | tf_op jit(solution)/shard_map/ppermute | solution.py:34
  117.8 7.3 %collective-permute-start.10 = (bf16[272,128]{1,0:T(8,128)(2,1)}, bf16[272,128]{1,0:T(8,128)(2,1)S(1)}, u32[]{:S(2)}, u32[]{:S(2)}) collective-permute-start(bf16[272,128]{1,0:T(8,128)(2,1)} %get-tuple-element.28), channel_id=1, source_target_pairs={{0,128},{32,160},{64,192},{96,224},{128,0},{160,32},{192,64},{224,... | collective-permute-start | bytes 208904 | tf_op jit(solution)/shard_map/ppermute | solution.py:502
  127.9 14.8 %all-to-all-start = ((bf16[8,64,128]{2,1,0:T(8,128)(2,1)}), bf16[8,64,128]{2,1,0:T(8,128)(2,1)S(1)}, u32[]{:S(2)}, u32[]{:S(2)}) async-start(bf16[8,64,128]{2,1,0:T(8,128)(2,1)} %bitcast.59), calls=%async_computation | async-start | bytes 262144 | tf_op jit(solution)/shard_map/all_to_all | solution.py:515
  142.6 9.4 %all-to-all-start.1 = ((bf16[8,64,128]{2,1,0:T(8,128)(2,1)}), bf16[8,64,128]{2,1,0:T(8,128)(2,1)S(1)}, u32[]{:S(2)}, u32[]{:S(2)}) async-start(bf16[8,64,128]{2,1,0:T(8,128)(2,1)} %bitcast.60), calls=%async_computation.1 | async-start | bytes 262144 | tf_op jit(solution)/shard_map/all_to_all | solution.py:519
  (23 other events, 85.7 us)

commit v3 on v2

v3 whole, which is shorter than its diff:
```python
import functools

import jax
import jax.numpy as jnp
from jax import lax
from jax.experimental import pallas as pl
from jax.experimental.pallas import tpu as pltpu
from jax.sharding import Mesh
from jax.sharding import PartitionSpec as P


HK = 128
HV = 128
AK = 64
AV = 128
BLOCK = 64
NZ, NX, NY, NC = 8, 4, 4, 2
AXES = ("z", "x", "y", "c")
SP = ("z", "x")
TP = ("y", "c")
TOK = 512
ACC_ROWS = 144
MAP_ROWS = AV + 16
SEND_ROWS = 2 * MAP_ROWS
PACK = 784
BF16 = jnp.bfloat16
F32 = jnp.float32

EPS = 1e-06
THETA = 500000.0
RISE = 40.0


def shift(value, axis, by, size):
    return lax.ppermute(value, axis, [(i, (i + by) % size) for i in range(size)])


def gather_rows(rows):
    half = rows.shape[0] // 2
    far_low = shift(rows[:half], "y", 2, NY)
    far_high = shift(rows[half:], "y", -2, NY)
    up = shift(rows, "y", 1, NY)
    down = shift(rows, "y", -1, NY)
    mine = jnp.concatenate([rows, up, down, far_low, far_high])
    return mine, shift(mine, "c", 1, NC)


def rms_scale(values, gain):
    return values * lax.rsqrt(jnp.mean(values * values, axis=-1, keepdims=True) + EPS) * gain


VMEM = pl.BlockSpec(memory_space=pltpu.VMEM)
SMEM = pl.BlockSpec(memory_space=pltpu.SMEM)


def limit(mib):
    return pltpu.CompilerParams(vmem_limit_bytes=mib << 20)


def cost(flops, transcendentals=0):
    return pl.CostEstimate(flops=flops, transcendentals=transcendentals, bytes_accessed=1 << 20)


def rotation_tables(length):
    positions = (lax.axis_index(SP) * length + jnp.arange(length, dtype=jnp.int32)).astype(F32)
    frequency = THETA ** (-(jnp.arange(AK // 2, dtype=F32) * 2.0 / AK))
    angles = positions[:, None] * frequency[None, :]
    cosine, sine = jnp.cos(angles), jnp.sin(angles)
    return (
        jnp.concatenate([cosine] * 4, axis=1),
        jnp.concatenate([-sine, sine, -sine, sine], axis=1),
    )


def rotated(vectors, cosine, sine):
    lane = lax.broadcasted_iota(jnp.int32, vectors.shape, 1)
    half = AK // 2
    partner = jnp.where(
        (lane & half) == 0, pltpu.roll(vectors, 128 - half, 1), pltpu.roll(vectors, half, 1)
    )
    return vectors * cosine + partner * sine


def keys_body(
    place_ref, mine_ref, other_ref, key_ref, value_ref, cos_ref, sin_ref, rows_ref, out_ref
):
    y, c = place_ref[2], place_ref[3]
    size = mine_ref.shape[0] // NY
    for core, ref in ((c, mine_ref), (1 - c, other_ref)):
        for n, distance in enumerate((0, 3, 1, 2)):
            at = pl.multiple_of((((y + distance) % NY) * NC + core) * size, size)
            rows_ref[pl.ds(at, size), :] = ref[n * size : (n + 1) * size, :]
    weights = jnp.concatenate([key_ref[...], value_ref[...]], axis=1)
    raw = jnp.dot(rows_ref[...], weights, preferred_element_type=F32).astype(BF16)
    out_ref[:TOK, :] = rotated(raw[:, :128].astype(F32), cos_ref[...], sin_ref[...]).astype(BF16)
    for n in range(TOK // 128):
        out_ref[TOK + n * 128 : TOK + (n + 1) * 128, :] = raw[n * 128 : (n + 1) * 128, 128:].T


def make_keys(place, mine, other, key, value, cosine, sine):
    return pl.pallas_call(
        keys_body,
        in_specs=[SMEM] + [VMEM] * 6,
        out_specs=[VMEM, VMEM],
        out_shape=[
            jax.ShapeDtypeStruct((TOK, mine.shape[1]), BF16),
            jax.ShapeDtypeStruct((2 * TOK, 128), BF16),
        ],
        cost_estimate=cost(1 << 29),
        compiler_params=limit(6),
        name="make_keys",
    )(place, mine, other, key, value, cosine, sine)


def local_body(
    rows_ref, aq_ref, q_ref, f_ref, b_ref, v_ref, leak_ref, decay_ref, cos_ref, sin_ref,
    pack_ref, out_ref, read_f_ref, read_b_ref,
):
    def project(*weights):
        joined = jnp.concatenate([w[...] for w in weights], axis=1)
        return jnp.dot(rows_ref[...], joined, preferred_element_type=F32).astype(BF16)

    raw_f_b = project(f_ref, b_ref)
    raw_q_v = project(q_ref, v_ref)
    raw_aq = project(aq_ref)
    pack_ref[:TOK, :] = (
        rotated(raw_aq.astype(F32), cos_ref[...], sin_ref[...]) * AK ** (-0.5)
    ).astype(BF16)
    raw = raw_q_v[:, :128].astype(F32)
    queries = raw / (1.0 + jnp.exp(-raw))
    row = lax.broadcasted_iota(jnp.int32, (BLOCK, BLOCK), 0)
    col = lax.broadcasted_iota(jnp.int32, (BLOCK, BLOCK), 1)
    totals = []
    for way, read_ref in enumerate((read_f_ref, read_b_ref)):
        gates = raw_f_b[:, way * HK : (way + 1) * HK].astype(F32)
        keys = leak_ref[way : way + 1, :] / (1.0 + jnp.exp(gates))
        logs = jnp.log1p(-keys) + decay_ref[way]
        reach = (row >= col) if way == 0 else (row <= col)
        sums = jnp.where(reach, 1.0, 0.0)
        middle_row, last_row = (BLOCK // 2 - 1, BLOCK - 1) if way == 0 else (BLOCK // 2, 0)
        state = jnp.zeros((HV, HK), F32)
        before = jnp.zeros((1, HK), F32)
        blocks = range(TOK // BLOCK)
        for n in blocks if way == 0 else reversed(blocks):
            at = slice(n * BLOCK, (n + 1) * BLOCK)
            cumulative = jnp.dot(
                sums, logs[at], precision=lax.Precision.HIGHEST, preferred_element_type=F32
            )
            middle = cumulative[middle_row : middle_row + 1]
            last = cumulative[last_row : last_row + 1]
            scores = lax.dot_general(
                (queries[at] * jnp.exp(cumulative - middle)).astype(BF16),
                (keys[at] * jnp.exp(middle - cumulative)).astype(BF16),
                (((1,), (1,)), ((), ())),
                preferred_element_type=F32,
            )
            scores = jnp.where(reach, scores, 0.0).astype(BF16)
            values = raw_q_v[at, 128:]
            out = jnp.dot(scores, values, preferred_element_type=F32)
            read = queries[at] * jnp.exp(cumulative)
            out = out + lax.dot_general(
                read.astype(BF16),
                state.astype(BF16),
                (((1,), (1,)), ((), ())),
                preferred_element_type=F32,
            )
            out_ref[at, :] = out if way == 0 else out_ref[at, :] + out
            read_ref[at, :] = (read * jnp.exp(before)).astype(BF16)
            added = lax.dot_general(
                values,
                (keys[at] * jnp.exp(last - cumulative)).astype(BF16),
                (((0,), (0,)), ((), ())),
                preferred_element_type=F32,
            )
            state = state * jnp.exp(last) + added
            before = before + last
        pack_ref[TOK + way * HV : TOK + (way + 1) * HV, :] = state.astype(BF16)
        totals.append(jnp.exp(before))
    pack_ref[TOK + 2 * HV :, :] = jnp.concatenate(
        [*totals, jnp.zeros((PACK - TOK - 2 * HV - 2, HK), F32)]
    ).astype(BF16)


def make_local(rows, weights, leak, decays, cosine, sine):
    return pl.pallas_call(
        local_body,
        in_specs=[VMEM] * 10,
        out_specs=[VMEM] * 4,
        out_shape=[
            jax.ShapeDtypeStruct((PACK, 128), BF16),
            jax.ShapeDtypeStruct((TOK, 128), F32),
            jax.ShapeDtypeStruct((TOK, 128), BF16),
            jax.ShapeDtypeStruct((TOK, 128), BF16),
        ],
        cost_estimate=cost(1 << 31),
        compiler_params=limit(12),
        name="local",
    )(rows, *weights, leak, decays, cosine, sine)


def link(earlier, later):
    return (earlier[0] * later[0], later[0] * earlier[1] + later[1])


def pick(condition, new, old):
    return tuple(jnp.where(condition, a, b) for a, b in zip(new, old))


def read_sent(ref, at):
    decays = ref[at + 2 * HV : at + 2 * HV + 16, :].astype(F32)
    return (
        (decays[0:1], ref[at : at + HV, :].astype(F32)),
        (decays[1:2], ref[at + HV : at + 2 * HV, :].astype(F32)),
    )


def write_sent(ref, fwd, bwd):
    ref[:HV, :] = fwd[1].astype(BF16)
    ref[HV : 2 * HV, :] = bwd[1].astype(BF16)
    ref[2 * HV :, :] = jnp.concatenate([fwd[0], bwd[0], jnp.zeros((14, HK), F32)]).astype(BF16)


def write_kept(ref, n, pair):
    ref[n, :HV, :] = pair[1]
    ref[n, HV:, :] = jnp.broadcast_to(pair[0], (8, HK))


def read_kept(ref, n):
    return ref[n, HV : HV + 1, :], ref[n, :HV, :]


def fold_body(place_ref, own_ref, below1_ref, below2_ref, below3_ref, kept_ref, sent_ref):
    place = place_ref[1]
    entries = [read_sent(ref, TOK) for ref in (own_ref, below1_ref, below2_ref, below3_ref)]
    none = (jnp.ones((1, HK), F32), jnp.zeros((HV, HK), F32))

    def fold(way, below, order):
        found = none
        for k in order:
            passed = (place >= k) if below else (place < k)
            found = pick(passed, link(found, entries[k][way]), found)
        return found

    f_below, f_above = fold(0, True, (3, 2, 1)), fold(0, False, (3, 2, 1))
    b_above, b_below = fold(1, False, (1, 2, 3)), fold(1, True, (1, 2, 3))
    fwd = link(link(f_below, entries[0][0]), f_above)
    bwd = link(link(b_above, entries[0][1]), b_below)
    for n, pair in enumerate((fwd, bwd, f_below, b_above)):
        write_kept(kept_ref, n, pair)
    write_sent(sent_ref, fwd, bwd)


KEPT = jax.ShapeDtypeStruct((4, HV + 8, HK), F32)
SENT = jax.ShapeDtypeStruct((2 * HV + 16, HK), BF16)


def fold_x(place, packs):
    return pl.pallas_call(
        fold_body,
        in_specs=[SMEM] + [VMEM] * 4,
        out_specs=[VMEM, VMEM],
        out_shape=[KEPT, SENT],
        cost_estimate=cost(1 << 22),
        compiler_params=limit(4),
        name="fold_x",
    )(place, *packs)


def is_lower(place_ref, bit):
    return (place_ref[0] & bit) != 0


def met(lower, kept_ref, received_ref):
    fwd, bwd, before, after = (read_kept(kept_ref, n) for n in range(4))
    peer_f, peer_b = read_sent(received_ref, 0)
    return (
        pick(lower, link(peer_f, fwd), link(fwd, peer_f)),
        pick(lower, link(bwd, peer_b), link(peer_b, bwd)),
        pick(lower, link(peer_f, before), before),
        pick(lower, after, link(peer_b, after)),
    )


def merge_body(place_ref, kept_ref, received_ref, out_ref, sent_ref, *, bit):
    pairs = met(is_lower(place_ref, bit), kept_ref, received_ref)
    for n, pair in enumerate(pairs):
        write_kept(out_ref, n, pair)
    write_sent(sent_ref, pairs[0], pairs[1])


def merge(place, bit, kept, received):
    return pl.pallas_call(
        functools.partial(merge_body, bit=bit),
        in_specs=[SMEM, VMEM, VMEM],
        out_specs=[VMEM, VMEM],
        out_shape=[KEPT, SENT],
        cost_estimate=cost(1 << 22),
        compiler_params=limit(4),
        name="merge",
    )(place, kept, received)


def finish_body(
    place_ref, kept_ref, received_ref, out_ref, read_f_ref, read_b_ref, gain_ref, rows_ref, *, bit
):
    _, _, before, after = met(is_lower(place_ref, bit), kept_ref, received_ref)
    total = out_ref[...]
    for read_ref, (_, state) in ((read_f_ref, before), (read_b_ref, after)):
        total = total + lax.dot_general(
            read_ref[...], state.astype(BF16), (((1,), (1,)), ((), ())), preferred_element_type=F32
        )
    rows_ref[...] = rms_scale(total, gain_ref[...]).astype(BF16)


def finish(place, bit, kept, received, out, read_f, read_b, gain):
    return pl.pallas_call(
        functools.partial(finish_body, bit=bit),
        in_specs=[SMEM] + [VMEM] * 6,
        out_specs=VMEM,
        out_shape=jax.ShapeDtypeStruct((TOK, HV), BF16),
        cost_estimate=cost(1 << 25),
        compiler_params=limit(4),
        name="finish",
    )(place, kept, received, out, read_f, read_b, gain.reshape(1, HV))


def attend_tile(maps, kv_refs, peaks, accs, first):
    ones = jnp.ones((ACC_ROWS - AV, TOK), BF16)
    values = [
        jnp.concatenate(
            [
                jnp.concatenate(
                    [kv[TOK + n * 128 : TOK + (n + 1) * 128, :] for n in range(TOK // 128)], axis=1
                ),
                ones,
            ]
        )
        for kv in kv_refs
    ]
    accs, peaks, rises = list(accs), list(peaks), []
    units = [(m, n) for m in range(len(maps)) for n in range(len(kv_refs))]

    def scores_of(unit):
        return jnp.dot(kv_refs[unit[1]][:TOK, :], maps[unit[0]], preferred_element_type=F32)

    scores = scores_of(units[0])
    for at, (m, n) in enumerate(units):
        upcoming = scores_of(units[at + 1]) if at + 1 < len(units) else None
        if first:
            peaks[m] = jnp.max(scores, axis=0, keepdims=True)
        above = scores - peaks[m]
        if not first:
            rises.append(jnp.max(above.reshape(-1, 8, above.shape[1]), axis=0))
        added = jnp.dot(values[n], jnp.exp(above).astype(BF16), preferred_element_type=F32)
        accs[m] = added if first else accs[m] + added
        scores = upcoming
    return accs, peaks, None if first else jnp.max(functools.reduce(jnp.maximum, rises))


def attend_again(maps_ref, kv_refs, peaks_ref, accs_ref):
    ones = jnp.ones((ACC_ROWS - AV, 128), BF16)
    for kv in kv_refs:

        def absorb(i, unused):
            m, n = i // (TOK // 128), i % (TOK // 128)
            keys = kv[pl.ds(pl.multiple_of(n * 128, 128), 128), :]
            values = kv[pl.ds(pl.multiple_of(TOK + n * 128, 128), 128), :]
            scores = jnp.dot(keys, maps_ref[m], preferred_element_type=F32)
            old = peaks_ref[m, 0:1, :]
            new = jnp.maximum(old, jnp.max(scores, axis=0, keepdims=True))
            accs_ref[m] = accs_ref[m] * jnp.exp(old - new) + jnp.dot(
                jnp.concatenate([values, ones]),
                jnp.exp(scores - new).astype(BF16),
                preferred_element_type=F32,
            )
            peaks_ref[m, 0:1, :] = new
            return 0

        lax.fori_loop(0, 2 * TOK // 128, absorb, 0)


def both_maps(turned):
    upper = lax.broadcasted_iota(jnp.int32, turned.shape, 0) < AK
    zero = jnp.zeros_like(turned)
    return jnp.where(upper, turned, zero), jnp.where(upper, zero, turned)


def attend_first_body(*refs):
    q_refs, (kv_ref, turned_ref, peaks_ref, accs_ref) = refs[:NX], refs[NX:]
    for n, ref in enumerate(q_refs):
        turned_ref[n] = ref[:TOK, :].T

    def tile(t, unused):
        accs, peaks, _ = attend_tile(
            both_maps(turned_ref[t]), [kv_ref], [None] * 2, [None] * 2, True
        )
        for m in range(2):
            accs_ref[t, m] = accs[m]
            peaks_ref[t, m] = jnp.broadcast_to(peaks[m], (8, TOK))
        return 0

    lax.fori_loop(0, NX, tile, 0)


def attend_more_body(turned_ref, *refs, chunks):
    kv_refs, (peaks_in, accs_in, peaks_ref, accs_ref, maps_ref) = refs[:chunks], refs[chunks:]
    peaks_ref[...] = peaks_in[...]

    def tile(t, unused):
        maps = both_maps(turned_ref[t])
        peaks = [peaks_in[t, m, 0:1, :] for m in range(2)]
        accs, _, rise = attend_tile(maps, kv_refs, peaks, [accs_in[t, m] for m in range(2)], False)
        for m in range(2):
            accs_ref[t, m] = accs[m]

        @pl.when(rise > RISE)
        def _():
            maps_ref[0], maps_ref[1] = maps
            accs_ref[t] = accs_in[t]
            attend_again(maps_ref, kv_refs, peaks_ref.at[t], accs_ref.at[t])

        return 0

    lax.fori_loop(0, NX, tile, 0)


def attend_last_body(turned_ref, *refs, chunks, tile):
    kv_refs, rest = refs[:chunks], refs[chunks:]
    peaks_in, accs_in, *send_refs, peaks_ref, accs_ref, maps_ref, rise_ref = rest
    maps_ref[0], maps_ref[1] = both_maps(turned_ref[tile])
    peaks_ref[...] = peaks_in[tile]
    rise_ref[0] = 0.0

    def one_map(m, unused):
        accs, _, rise = attend_tile(
            [maps_ref[m]], kv_refs, [peaks_in[tile, m, 0:1, :]], [accs_in[tile, m]], False
        )
        accs_ref[m] = accs[0]
        rise_ref[0] = jnp.maximum(rise_ref[0], rise)
        return 0

    lax.fori_loop(0, 2, one_map, 0)

    @pl.when(rise_ref[0] > RISE)
    def _():
        accs_ref[...] = accs_in[tile]
        attend_again(maps_ref, kv_refs, peaks_ref, accs_ref)

    for m in range(2):
        acc = accs_ref[m]
        total = acc[AV : AV + 1, :]
        level = peaks_ref[m, 0:1, :] + jnp.log(total)
        high = level.astype(BF16)
        left = level - high.astype(F32)
        middle = left.astype(BF16)
        low = (left - middle.astype(F32)).astype(BF16)
        mean = (acc[:AV] * (1.0 / total)).astype(BF16)
        levels = jnp.concatenate(
            [high.astype(F32), middle.astype(F32), low.astype(F32), jnp.zeros((13, TOK), F32)]
        ).astype(BF16)
        ref = send_refs[m] if len(send_refs) > 1 else send_refs[0]
        at = 0 if len(send_refs) > 1 else m * MAP_ROWS
        ref[at : at + AV, :] = mean
        ref[at + AV : at + MAP_ROWS, :] = levels


STATE = [
    jax.ShapeDtypeStruct((NX, 2, 8, TOK), F32),
    jax.ShapeDtypeStruct((NX, 2, ACC_ROWS, TOK), F32),
]


def attend_cost(tiles, chunks):
    work = 2 * tiles * TOK * chunks * TOK
    return cost(work * 2 * (AK + AV), work)


def attend_first(packs, kv):
    return pl.pallas_call(
        attend_first_body,
        in_specs=[VMEM] * (NX + 1),
        out_specs=[VMEM] * 3,
        out_shape=[jax.ShapeDtypeStruct((NX, 2 * AK, TOK), BF16), *STATE],
        cost_estimate=attend_cost(NX, 1),
        compiler_params=limit(14),
        name="attend_first",
    )(*packs, kv)


def attend_more(turned, pieces, state):
    return pl.pallas_call(
        functools.partial(attend_more_body, chunks=len(pieces)),
        in_specs=[VMEM] * (len(pieces) + 3),
        out_specs=[VMEM] * 2,
        out_shape=STATE,
        scratch_shapes=[pltpu.VMEM((2, 2 * AK, TOK), BF16)],
        cost_estimate=attend_cost(NX, len(pieces)),
        compiler_params=limit(14),
        name="attend_more",
    )(turned, *pieces, *state)


def attend_last(turned, pieces, state, tile, parts):
    return pl.pallas_call(
        functools.partial(attend_last_body, chunks=len(pieces), tile=tile),
        in_specs=[VMEM] * (len(pieces) + 3),
        out_specs=[VMEM] * parts,
        out_shape=[jax.ShapeDtypeStruct((SEND_ROWS // parts, TOK), BF16)] * parts,
        scratch_shapes=[
            pltpu.VMEM((2, 8, TOK), F32),
            pltpu.VMEM((2, ACC_ROWS, TOK), F32),
            pltpu.VMEM((2, 2 * AK, TOK), BF16),
            pltpu.SMEM((1,), F32),
        ],
        cost_estimate=attend_cost(1, len(pieces)),
        compiler_params=limit(14),
        name="attend_last",
    )(turned, *pieces, *state)


def mix_body(a_ref, b_ref, c_ref, low_ref, high_ref, weight_ref, gain_ref, out_ref):
    mixed = None
    for m in range(2):
        places = [(ref, m * MAP_ROWS) for ref in (a_ref, b_ref, c_ref)]
        places.append(((low_ref, high_ref)[m], 0))
        levels = []
        for ref, at in places:
            parts = ref[at + AV : at + MAP_ROWS, :].astype(F32)
            levels.append(parts[0:1] + parts[1:2] + parts[2:3])
        peak = functools.reduce(jnp.maximum, levels)
        shares = [jnp.exp(level - peak) for level in levels]
        scale = 1.0 / functools.reduce(jnp.add, shares)
        if m == 1:
            scale = scale * -weight_ref[0]
        for (ref, at), share in zip(places, shares):
            term = ref[at : at + AV, :].astype(F32) * (share * scale)
            mixed = term if mixed is None else mixed + term
    scale = lax.rsqrt(jnp.mean(mixed * mixed, axis=0, keepdims=True) + EPS)
    out_ref[...] = ((mixed * scale).T * gain_ref[...]).astype(BF16)


def mix(partials, weight, gain):
    return pl.pallas_call(
        mix_body,
        in_specs=[VMEM] * 5 + [SMEM, VMEM],
        out_specs=VMEM,
        out_shape=jax.ShapeDtypeStruct((TOK, AV), BF16),
        cost_estimate=cost(1 << 22),
        compiler_params=limit(6),
        name="mix",
    )(*partials, weight, gain.reshape(1, AV))


def on_device(
    tokens,
    norm_gain,
    rec_query,
    fwd_gate,
    bwd_gate,
    rec_value,
    gate_leak,
    log_decay,
    rec_gain,
    att_query,
    att_key,
    att_value,
    lambdas,
    att_gain,
    out_rec,
    out_att,
):
    place = jnp.stack([lax.axis_index(axis) for axis in AXES]).astype(jnp.int32)
    decays = jnp.broadcast_to(log_decay, (2, TOK, 128))
    cosine, sine = rotation_tables(TOK)
    normed = rms_scale(tokens.astype(F32), norm_gain).astype(BF16)
    mine, other = gather_rows(normed)
    rows, own_kv = make_keys(place, mine, other, att_key, att_value, cosine, sine)
    ups, downs = [own_kv], [own_kv]
    for step in range(1, NZ // 2 + 1):
        ups.append(shift(ups[-1], "z", 1, NZ))
        if step < NZ // 2:
            downs.append(shift(downs[-1], "z", -1, NZ))
    pack, out_local, read_f, read_b = make_local(
        rows,
        (att_query, rec_query, fwd_gate, bwd_gate, rec_value),
        gate_leak,
        decays,
        cosine,
        sine,
    )
    packs = [pack]
    for by in (1, 2, -1):
        packs.append(shift(pack, "x", by, NX))
    kept, sent = fold_x(place, packs)
    turned, *state = attend_first([packs[0], packs[1], packs[3], packs[2]], own_kv)
    for bit in (1, 2, 4):
        received = lax.ppermute(sent, "z", [(i, i ^ bit) for i in range(NZ)])
        if bit < 4:
            kept, sent = merge(place, bit, kept, received)
    state = attend_more(turned, [ups[1], downs[1]], state)
    state = attend_more(turned, [ups[2], downs[2]], state)
    ends = [ups[3], downs[3], ups[4]]
    low, high = attend_last(turned, ends, state, 3, 2)
    far_low = shift(low, "x", 2, NX)
    far_high = shift(high, "x", -2, NX)
    (send,) = attend_last(turned, ends, state, 1, 1)
    from_above = shift(send, "x", -1, NX)
    (send,) = attend_last(turned, ends, state, 2, 1)
    from_below = shift(send, "x", 1, NX)
    (own,) = attend_last(turned, ends, state, 0, 1)
    rec_rows = finish(place, bit, kept, received, out_local, read_f, read_b, rec_gain)
    rec_all = lax.all_to_all(rec_rows, TP, split_axis=0, concat_axis=1, tiled=True)
    rec_part = jnp.dot(rec_all, out_rec, preferred_element_type=F32)
    att_rows = mix([own, from_above, from_below, far_low, far_high], lambdas, att_gain)
    att_all = lax.all_to_all(att_rows, TP, split_axis=0, concat_axis=1, tiled=True)
    return (rec_part + jnp.dot(att_all, out_att, preferred_element_type=F32)).astype(BF16)


def solution(mesh):
    torus = Mesh(mesh.devices.reshape(NZ, NX, NY, NC), AXES)
    in_specs = (
        P(AXES, None),
        P(),
        P(None, TP),
        P(None, TP),
        P(None, TP),
        P(None, TP),
        P(None, TP),
        P(None, SP, TP),
        P(),
        P(None, TP),
        P(None, TP),
        P(None, TP),
        P(TP),
        P(),
        P(),
        P(),
    )
    out_specs = P(AXES, None)
    return jax.shard_map(
        on_device, mesh=torus, in_specs=in_specs, out_specs=out_specs, check_vma=False
    )
```

time: 157 us -> 196 us (1.25)
  starting transfers between devices: 48 us -> 116 us
  local copies, waits for them, and re-layouts: 22.3 us -> 1.92 us
  Pallas kernels: 48 us -> 41 us
  waiting for transfers between devices: 20.1 us -> 24.6 us
  matrix products: 10.1 us -> 6.84 us
  other arithmetic: 6.28 us -> 3.87 us
    all_to_all x1, starting transfers between devices: 9.54 us -> 74.2 us  [on_device(): lax.all_to_all(rec_rows, TP, split_axis=0, concat_axis=1, tiled=True)]
    unnamed x69 -> x32, local copies, waits for them, and re-layouts: 17.9 us -> 1.71 us
    ppermute x19, waiting for transfers between devices: 11.8 us -> 20.8 us  [shift(): lax.ppermute(value, axis, [(i, (i + by) % size) for i in range(size)])]
    pallas_call x10 -> x13, Pallas kernels: 45.9 us -> 40.4 us  [the longest x4 12.3 us: attend_last(): pl.pallas_call(functools.partial(attend_last_body, chunks=len(pieces), ti...]
    dot_general x1 -> x0, matrix products: 3.32 us -> none  [on_device(): jnp.dot(gather_rows(normed), joined, preferred_element_type=F32)]
    ppermute x3, waiting for transfers between devices: 4.66 us -> 1.7 us  [on_device(): received = lax.ppermute(sent, 'z', [(i, i ^ bit) for i in range(NZ)])]
    dynamic_update_slice x4 -> x0, local copies, waits for them, and re-layouts: 2.28 us -> none  [the longest x2 2.04 us: gather_rows(): mine = lax.dynamic_update_slice(mine, piece[None], (source, 0, 0))]
    ppermute x3, starting transfers between devices: 4.71 us -> 6.87 us  [on_device(): received = lax.ppermute(sent, 'z', [(i, i ^ bit) for i in range(NZ)])]
  transfers between devices with their start and end apart: 24 -> 24, of which waited for: 7 -> 9; matrix products, arithmetic and copies ran while one was open for 10% -> 3% of each run, Pallas kernels for 29% -> 20%
where the time goes in v3:
time: 196 us; the launch traced here: 195 us
  starting transfers between devices  116 us (59%)
  Pallas kernels  41 us (21%)
  waiting for transfers between devices  24.6 us (13%)
  matrix products  6.84 us (3%)
  other arithmetic  3.87 us (2%)
    all_to_all x1, starting transfers between devices, on_device(): lax.all_to_all(rec_rows, TP, split_axis=0, concat_axis=1, tiled=True)  74.2 us
    ppermute x19, starting transfers between devices, shift(): lax.ppermute(value, axis, [(i, (i + by) % size) for i in range(size)])  30 us
    ppermute x19, waiting for transfers between devices, shift(): lax.ppermute(value, axis, [(i, (i + by) % size) for i in range(size)])  20.8 us
    pallas_call x4, Pallas kernels, attend_last(): pl.pallas_call(functools.partial(attend_last_body, chunks=len(pieces), ti...  12.3 us
    pallas_call x2, Pallas kernels, attend_more(): pl.pallas_call(functools.partial(attend_more_body, chunks=len(pieces)), i...  12.3 us
    ppermute x3, starting transfers between devices, on_device(): received = lax.ppermute(sent, 'z', [(i, i ^ bit) for i in range(NZ)])  6.87 us
    pallas_call x1, Pallas kernels, make_local(): pl.pallas_call(local_body, in_specs=[VMEM] * 10, out_specs=[VMEM] * 4, ou...  5.91 us
    all_to_all x1, starting transfers between devices, on_device(): lax.all_to_all(att_rows, TP, split_axis=0, concat_axis=1, tiled=True)  4.82 us
  transfers between devices with their start and end apart: 24, of which 9 were waited for; matrix products, arithmetic and copies ran while one was open for 3% of the time, Pallas kernels for 20%

profile of v3, /device:TPU:1, one launch (start us, length us, event | category | flops | bytes accessed | tf_op | source)
XLA Modules:
  0.0 195.2 jit_solution(12594408158159193212)
XLA Ops:
  2.3 2.2 %collective-permute-start = (bf16[64,2048]{1,0:T(8,128)(2,1)S(1)}, bf16[64,2048]{1,0:T(8,128)(2,1)S(1)}, u32[]{:S(2)}, u32[]{:S(2)}) collective-permute-start(bf16[64,2048]{1,0:T(8,128)(2,1)S(1)} %get-tuple-element.48), channel_id=1, source_target_pairs={{0,2},{2,4},{4,6},{6,0},{1,3},{3,5},{5,7},{7,1},{8,10},{10,12},{12... | collective-permute-start | bytes 786440 | tf_op jit(solution)/shard_map/ppermute | solution.py:35
  4.5 1.5 collective-permute-start.1
  6.1 1.6 collective-permute-start.2
  11.2 4.4 %collective-permute-done.2 = bf16[32,2048]{1,0:T(8,128)(2,1)S(1)} collective-permute-done((bf16[32,2048]{1,0:T(8,128)(2,1)S(1)}, bf16[32,2048]{1,0:T(8,128)(2,1)S(1)}, u32[]{:S(2)}, u32[]{:S(2)}) %collective-permute-start.2) | collective-permute-done | bytes 131104 | tf_op jit(solution)/shard_map/ppermute | solution.py:35
  15.7 2.8 %collective-permute-done.3 = bf16[32,2048]{1,0:T(8,128)(2,1)S(1)} collective-permute-done((bf16[32,2048]{1,0:T(8,128)(2,1)S(1)}, bf16[32,2048]{1,0:T(8,128)(2,1)S(1)}, u32[]{:S(2)}, u32[]{:S(2)}) %collective-permute-start.3) | collective-permute-done | bytes 131104 | tf_op jit(solution)/shard_map/ppermute | solution.py:35
  18.5 1.6 collective-permute-start.4
  23.9 1.7 collective-permute-start.11
  25.6 4.0 %collective-permute-start.14 = (bf16[1024,128]{1,0:T(8,128)(2,1)S(1)}, bf16[1024,128]{1,0:T(8,128)(2,1)S(1)}, u32[]{:S(2)}, u32[]{:S(2)}) collective-permute-start(bf16[1024,128]{1,0:T(8,128)(2,1)S(1)} %get-tuple-element.37.refs_4_), channel_id=1, source_target_pairs={{0,224},{32,0},{64,32},{96,64},{128,96},{160,128},{192,160},{224,1... | collective-permute-start | bytes 786440 | tf_op jit(solution)/shard_map/ppermute | solution.py:35
  29.6 6.2 %collective-permute-done.11.refs_0_ = bf16[1024,128]{1,0:T(8,128)(2,1)S(1)} collective-permute-done((bf16[1024,128]{1,0:T(8,128)(2,1)S(1)}, bf16[1024,128]{1,0:T(8,128)(2,1)S(1)}, u32[]{:S(2)}, u32[]{:S(2)}) %collective-permute-start.11) | collective-permute-done | bytes 262176 | tf_op jit(solution)/shard_map/ppermute | solution.py:35
  36.1 5.9 %local.1 = (bf16[784,128]{1,0:T(8,128)(2,1)S(1)}, f32[512,128]{1,0:T(8,128)S(1)}, bf16[512,128]{1,0:T(8,128)(2,1)S(1)}, bf16[512,128]{1,0:T(8,128)(2,1)S(1)}) custom-call(bf16[512,2048]{1,0:T(8,128)(2,1)S(1)} %get-tuple-element.26.rows_ref, bf16[2048,128]{1,0:T(8,128)(2,1)S(1)} %copy-done.7, bf16[2048,128]{1,0:T(8,128)(2,1)S(1)} %copy-done.8, ...), custom_call_target="tpu_custom_call" | custom-call | flops 2147483648 | bytes 1048576 | tf_op jit(solution)/shard_map/local/pallas_call | solution.py:185
  43.4 2.4 %collective-permute-start.6 = (bf16[784,128]{1,0:T(8,128)(2,1)S(1)}, bf16[784,128]{1,0:T(8,128)(2,1)S(1)}, u32[]{:S(2)}, u32[]{:S(2)}) collective-permute-start(bf16[784,128]{1,0:T(8,128)(2,1)S(1)} %get-tuple-element.27.own_ref.refs_0_), channel_id=1, source_target_pairs={{0,16},{8,24},{16,0},{24,8},{1,17},{9,25},{17,1},{25,9},{2,18},{10... | collective-permute-start | bytes 602120 | tf_op jit(solution)/shard_map/ppermute | solution.py:35
  47.0 2.7 %collective-permute-start.15 = (bf16[1024,128]{1,0:T(8,128)(2,1)S(1)}, bf16[1024,128]{1,0:T(8,128)(2,1)S(1)}, u32[]{:S(2)}, u32[]{:S(2)}) collective-permute-start(bf16[1024,128]{1,0:T(8,128)(2,1)S(1)} %collective-permute-done.14.refs_1_), channel_id=1, source_target_pairs={{0,224},{32,0},{64,32},{96,64},{128,96},{160,128},{192,160},{224,1... | collective-permute-start | bytes 786440 | tf_op jit(solution)/shard_map/ppermute | solution.py:35
  49.7 4.6 %collective-permute-done.6.below2_ref.refs_3_ = bf16[784,128]{1,0:T(8,128)(2,1)S(1)} collective-permute-done((bf16[784,128]{1,0:T(8,128)(2,1)S(1)}, bf16[784,128]{1,0:T(8,128)(2,1)S(1)}, u32[]{:S(2)}, u32[]{:S(2)}) %collective-permute-start.6) | collective-permute-done | bytes 200736 | tf_op jit(solution)/shard_map/ppermute | solution.py:35
  55.1 4.1 %attend_first.1 = (bf16[4,128,512]{2,1,0:T(8,128)(2,1)S(1)}, f32[4,2,8,512]{3,2,1,0:T(8,128)S(1)}, f32[4,2,144,512]{3,2,1,0:T(8,128)S(1)}) custom-call(bf16[784,128]{1,0:T(8,128)(2,1)S(1)} %get-tuple-element.27.own_ref.refs_0_, bf16[784,128]{1,0:T(8,128)(2,1)S(1)} %collective-permute-done.5.below1_ref.refs_1_, ...), custom_call_target="tpu_custom_call" | custom-call | flops 805306368 | bytes 1048576 | tf_op jit(solution)/shard_map/attend_first/pallas_call | solution.py:479
  59.2 2.5 %collective-permute-start.16 = (bf16[1024,128]{1,0:T(8,128)(2,1)S(1)}, bf16[1024,128]{1,0:T(8,128)(2,1)S(1)}, u32[]{:S(2)}, u32[]{:S(2)}) collective-permute-start(bf16[1024,128]{1,0:T(8,128)(2,1)S(1)} %collective-permute-done.15.refs_1_), channel_id=1, source_target_pairs={{0,224},{32,0},{64,32},{96,64},{128,96},{160,128},{192,160},{224,1... | collective-permute-start | bytes 786440 | tf_op jit(solution)/shard_map/ppermute | solution.py:35
  61.6 6.1 %attend_more.2 = (f32[4,2,8,512]{3,2,1,0:T(8,128)S(1)}, f32[4,2,144,512]{3,2,1,0:T(8,128)S(1)}) custom-call(bf16[4,128,512]{2,1,0:T(8,128)(2,1)S(1)} %get-tuple-element.38.turned_ref, bf16[1024,128]{1,0:T(8,128)(2,1)S(1)} %collective-permute-done.11.refs_0_, bf16[1024,128]{1,0:T(8,128)(2,1)S(1)} %collective-permute-done.14.refs_1_, ...), custom_call_target="tpu_custom_call" | custom-call | flops 1610612736 | bytes 1048576 | tf_op jit(solution)/shard_map/attend_more/pallas_call | solution.py:491
  67.8 6.1 %attend_more.3 = (f32[4,2,8,512]{3,2,1,0:T(8,128)S(1)}, f32[4,2,144,512]{3,2,1,0:T(8,128)S(1)}) custom-call(bf16[4,128,512]{2,1,0:T(8,128)(2,1)S(1)} %get-tuple-element.38.turned_ref, bf16[1024,128]{1,0:T(8,128)(2,1)S(1)} %collective-permute-done.12.refs_0_, bf16[1024,128]{1,0:T(8,128)(2,1)S(1)} %collective-permute-done.15.refs_1_, ...), custom_call_target="tpu_custom_call" | custom-call | flops 1610612736 | bytes 1048576 | tf_op jit(solution)/shard_map/attend_more/pallas_call | solution.py:491
  74.0 3.3 %attend_last.6 = bf16[288,512]{1,0:T(8,128)(2,1)} custom-call(bf16[4,128,512]{2,1,0:T(8,128)(2,1)S(1)} %get-tuple-element.38.turned_ref, bf16[1024,128]{1,0:T(8,128)(2,1)S(1)} %collective-permute-done.13.refs_0_, bf16[1024,128]{1,0:T(8,128)(2,1)S(1)} %collective-permute-done.16.refs_1_, bf16[1024,128]{1,0:T(8,128)(2,1)S(1)} %collective-permute-done.17.refs_2_, ...), custom_call_target="tpu_custom_call" | custom-call | flops 603979776 | bytes 1048576 | tf_op jit(solution)/shard_map/attend_last/pallas_call | solution.py:504
  77.3 2.0 collective-permute-start.19
  79.2 3.3 %attend_last.5 = bf16[288,512]{1,0:T(8,128)(2,1)} custom-call(bf16[4,128,512]{2,1,0:T(8,128)(2,1)S(1)} %get-tuple-element.38.turned_ref, bf16[1024,128]{1,0:T(8,128)(2,1)S(1)} %collective-permute-done.13.refs_0_, bf16[1024,128]{1,0:T(8,128)(2,1)S(1)} %collective-permute-done.16.refs_1_, bf16[1024,128]{1,0:T(8,128)(2,1)S(1)} %collective-permute-done.17.refs_2_, ...), custom_call_target="tpu_custom_call" | custom-call | flops 603979776 | bytes 1048576 | tf_op jit(solution)/shard_map/attend_last/pallas_call | solution.py:504
  83.9 2.9 %collective-permute-start.9 = (bf16[272,128]{1,0:T(8,128)(2,1)S(1)}, bf16[272,128]{1,0:T(8,128)(2,1)S(1)}, u32[]{:S(2)}, u32[]{:S(2)}) collective-permute-start(bf16[272,128]{1,0:T(8,128)(2,1)S(1)} %get-tuple-element.31), channel_id=1, source_target_pairs={{0,64},{32,96},{64,0},{96,32},{128,192},{160,224},{192,128},{224,1... | collective-permute-start | bytes 208904 | tf_op jit(solution)/shard_map/ppermute | solution.py:597
  86.8 1.7 collective-permute-done.9.received_ref
  89.1 3.9 %collective-permute-start.10 = (bf16[272,128]{1,0:T(8,128)(2,1)S(1)}, bf16[272,128]{1,0:T(8,128)(2,1)S(1)}, u32[]{:S(2)}, u32[]{:S(2)}) collective-permute-start(bf16[272,128]{1,0:T(8,128)(2,1)S(1)} %get-tuple-element.33), channel_id=1, source_target_pairs={{0,128},{32,160},{64,192},{96,224},{128,0},{160,32},{192,64},{224,... | collective-permute-start | bytes 208904 | tf_op jit(solution)/shard_map/ppermute | solution.py:597
  93.0 3.2 %attend_last.7 = (bf16[144,512]{1,0:T(8,128)(2,1)}, bf16[144,512]{1,0:T(8,128)(2,1)}) custom-call(bf16[4,128,512]{2,1,0:T(8,128)(2,1)S(1)} %get-tuple-element.38.turned_ref, bf16[1024,128]{1,0:T(8,128)(2,1)S(1)} %collective-permute-done.13.refs_0_, bf16[1024,128]{1,0:T(8,128)(2,1)S(1)} %collective-permute-done.16.refs_1_, ...), custom_call_target="tpu_custom_call" | custom-call | flops 603979776 | bytes 1048576 | tf_op jit(solution)/shard_map/attend_last/pallas_call | solution.py:504
  97.5 1.7 collective-permute-start.21
  100.8 74.2 %all-to-all-start = ((bf16[8,64,128]{2,1,0:T(8,128)(2,1)}), bf16[8,64,128]{2,1,0:T(8,128)(2,1)}, u32[]{:S(2)}, u32[]{:S(2)}) async-start(bf16[8,64,128]{2,1,0:T(8,128)(2,1)} %bitcast.29), calls=%async_computation | async-start | bytes 262144 | tf_op jit(solution)/shard_map/all_to_all | solution.py:612
  176.6 2.5 %attend_last.4.a_ref = bf16[288,512]{1,0:T(8,128)(2,1)S(1)} custom-call(bf16[4,128,512]{2,1,0:T(8,128)(2,1)S(1)} %get-tuple-element.38.turned_ref, bf16[1024,128]{1,0:T(8,128)(2,1)S(1)} %collective-permute-done.13.refs_0_, bf16[1024,128]{1,0:T(8,128)(2,1)S(1)} %collective-permute-done.16.refs_1_, bf16[1024,128]{1,0:T(8,128)(2,1)S(1)} %copy-done.1, ...), custom_call_target="tpu_custom_call" | custom-call | flops 603979776 | bytes 1048576 | tf_op jit(solution)/shard_map/attend_last/pallas_call | solution.py:504
  179.2 2.2 %mix.1 = bf16[512,128]{1,0:T(8,128)(2,1)} custom-call(bf16[288,512]{1,0:T(8,128)(2,1)S(1)} %attend_last.4.a_ref, bf16[288,512]{1,0:T(8,128)(2,1)} %collective-permute-done.18.b_ref, bf16[288,512]{1,0:T(8,128)(2,1)} %collective-permute-done.19.c_ref, bf16[144,512]{1,0:T(8,128)(2,1)} %collective-permute-done.20.low_ref, ...), custom_call_target="tpu_custom_call" | custom-call | flops 4194304 | bytes 1048576 | tf_op jit(solution)/shard_map/mix/pallas_call | solution.py:543
  181.4 4.8 %all-to-all-start.1 = ((bf16[8,64,128]{2,1,0:T(8,128)(2,1)}), bf16[8,64,128]{2,1,0:T(8,128)(2,1)S(1)}, u32[]{:S(2)}, u32[]{:S(2)}) async-start(bf16[8,64,128]{2,1,0:T(8,128)(2,1)} %bitcast.8), calls=%async_computation.1 | async-start | bytes 262144 | tf_op jit(solution)/shard_map/all_to_all | solution.py:615
  186.2 3.1 %fusion.6 = f32[64,2048]{1,0:T(8,128)S(1)} fusion(bf16[1024,2048]{1,0:T(8,128)(2,1)} %param.30, bf16[8,64,128]{2,1,0:T(8,128)(2,1)} %all-to-all-done), kind=kOutput, calls=%fused_computation.13 | convolution fusion | flops 268435456 | bytes 4849664 | tf_op jit(solution)/shard_map/dot_general | solution.py:613
  189.4 2.1 %all-to-all-done.1 = bf16[8,64,128]{2,1,0:T(8,128)(2,1)S(1)} async-done(((bf16[8,64,128]{2,1,0:T(8,128)(2,1)}), bf16[8,64,128]{2,1,0:T(8,128)(2,1)S(1)}, u32[]{:S(2)}, u32[]{:S(2)}) %all-to-all-start.1) | async-done | bytes 131104 | tf_op jit(solution)/shard_map/all_to_all | solution.py:615
  191.5 3.7 %fusion = bf16[64,2048]{1,0:T(8,128)(2,1)} fusion(f32[64,2048]{1,0:T(8,128)S(1)} %fusion.6, bf16[1024,2048]{1,0:T(8,128)(2,1)} %param.31, bf16[8,64,128]{2,1,0:T(8,128)(2,1)S(1)} %all-to-all-done.1), kind=kOutput, calls=%fused_computation.1 | convolution fusion | flops 268697600 | bytes 5111808 | tf_op jit(solution)/shard_map/dot_general | solution.py:616
  (75 shorter events, 18.9 us)
Async XLA Ops:
  0.0 22.4 %copy-start.3 = (bf16[2048,128]{1,0:T(8,128)(2,1)S(1)}, bf16[2048,128]{1,0:T(8,128)(2,1)}, u32[]{:S(2)}) copy-start(bf16[2048,128]{1,0:T(8,128)(2,1)} %key_ref.1) | copy-start | bytes 1572868
  0.0 22.4 %copy-start.4 = (bf16[2048,128]{1,0:T(8,128)(2,1)S(1)}, bf16[2048,128]{1,0:T(8,128)(2,1)}, u32[]{:S(2)}) copy-start(bf16[2048,128]{1,0:T(8,128)(2,1)} %value_ref.1) | copy-start | bytes 1572868
  1.2 34.6 %copy-start.13 = (f32[2,512,1]{1,2,0:T(1,128)S(1)}, f32[2,512,1]{1,2,0:T(1,128)}, u32[]{:S(2)}) copy-start(f32[2,512,1]{1,2,0:T(1,128)} %param.23) | copy-start | bytes 12292
  2.3 33.7 %copy-start.12 = (f32[2,128]{1,0:T(2,128)S(1)}, f32[2,128]{1,0:T(2,128)}, u32[]{:S(2)}) copy-start(f32[2,128]{1,0:T(2,128)} %leak_ref.1) | copy-start | bytes 3076
  2.3 7.7 %collective-permute-start = (bf16[64,2048]{1,0:T(8,128)(2,1)S(1)}, bf16[64,2048]{1,0:T(8,128)(2,1)S(1)}, u32[]{:S(2)}, u32[]{:S(2)}) collective-permute-start(bf16[64,2048]{1,0:T(8,128)(2,1)S(1)} %get-tuple-element.48), channel_id=1, source_target_pairs={{0,2},{2,4},{4,6},{6,0},{1,3},{3,5},{5,7},{7,1},{8,10},{10,12},{12... | collective-permute-start | bytes 786440 | tf_op jit(solution)/shard_map/ppermute | solution.py:35
  4.5 6.7 %collective-permute-start.1 = (bf16[64,2048]{1,0:T(8,128)(2,1)S(1)}, bf16[64,2048]{1,0:T(8,128)(2,1)S(1)}, u32[]{:S(2)}, u32[]{:S(2)}) collective-permute-start(bf16[64,2048]{1,0:T(8,128)(2,1)S(1)} %get-tuple-element.48), channel_id=1, source_target_pairs={{0,6},{2,0},{4,2},{6,4},{1,7},{3,1},{5,3},{7,5},{8,14},{10,8},{12,... | collective-permute-start | bytes 786440 | tf_op jit(solution)/shard_map/ppermute | solution.py:35
  6.1 9.6 %collective-permute-start.2 = (bf16[32,2048]{1,0:T(8,128)(2,1)S(1)}, bf16[32,2048]{1,0:T(8,128)(2,1)S(1)}, u32[]{:S(2)}, u32[]{:S(2)}) collective-permute-start(bf16[32,2048]{1,0:T(8,128)(2,1)S(1)} %get-tuple-element.50), channel_id=1, source_target_pairs={{0,4},{2,6},{4,0},{6,2},{1,5},{3,7},{5,1},{7,3},{8,12},{10,14},{12... | collective-permute-start | bytes 393224 | tf_op jit(solution)/shard_map/ppermute | solution.py:35
  7.7 10.8 %collective-permute-start.3 = (bf16[32,2048]{1,0:T(8,128)(2,1)S(1)}, bf16[32,2048]{1,0:T(8,128)(2,1)S(1)}, u32[]{:S(2)}, u32[]{:S(2)}) collective-permute-start(bf16[32,2048]{1,0:T(8,128)(2,1)S(1)} %get-tuple-element.49), channel_id=1, source_target_pairs={{0,4},{2,6},{4,0},{6,2},{1,5},{3,7},{5,1},{7,3},{8,12},{10,14},{12... | collective-permute-start | bytes 393224 | tf_op jit(solution)/shard_map/ppermute | solution.py:35
  18.5 3.9 %collective-permute-start.4 = (bf16[256,2048]{1,0:T(8,128)(2,1)S(1)}, bf16[256,2048]{1,0:T(8,128)(2,1)S(1)}, u32[]{:S(2)}, u32[]{:S(2)}) collective-permute-start(bf16[256,2048]{1,0:T(8,128)(2,1)S(1)} %constant_dynamic-update-slice_fusion.mine_ref), channel_id=1, source_target_pairs={{0,1},{1,0},{2,3},{3,2},{4,5},{5,4},{6,7},{7,6},{8,9},{9,8},{10,11... | collective-permute-start | bytes 3145736 | tf_op jit(solution)/shard_map/ppermute | solution.py:35
  20.1 16.0 %copy-start.11 = (bf16[2048,128]{1,0:T(8,128)(2,1)S(1)}, bf16[2048,128]{1,0:T(8,128)(2,1)}, u32[]{:S(2)}) copy-start(bf16[2048,128]{1,0:T(8,128)(2,1)} %v_ref.1) | copy-start | bytes 1572868
  23.9 12.0 %collective-permute-start.11 = (bf16[1024,128]{1,0:T(8,128)(2,1)S(1)}, bf16[1024,128]{1,0:T(8,128)(2,1)S(1)}, u32[]{:S(2)}, u32[]{:S(2)}) collective-permute-start(bf16[1024,128]{1,0:T(8,128)(2,1)S(1)} %get-tuple-element.37.refs_4_), channel_id=1, source_target_pairs={{0,32},{32,64},{64,96},{96,128},{128,160},{160,192},{192,224},{224... | collective-permute-start | bytes 786440 | tf_op jit(solution)/shard_map/ppermute | solution.py:35
  25.6 21.4 %collective-permute-start.14 = (bf16[1024,128]{1,0:T(8,128)(2,1)S(1)}, bf16[1024,128]{1,0:T(8,128)(2,1)S(1)}, u32[]{:S(2)}, u32[]{:S(2)}) collective-permute-start(bf16[1024,128]{1,0:T(8,128)(2,1)S(1)} %get-tuple-element.37.refs_4_), channel_id=1, source_target_pairs={{0,224},{32,0},{64,32},{96,64},{128,96},{160,128},{192,160},{224,1... | collective-permute-start | bytes 786440 | tf_op jit(solution)/shard_map/ppermute | solution.py:35
  35.8 13.9 %collective-permute-start.12 = (bf16[1024,128]{1,0:T(8,128)(2,1)S(1)}, bf16[1024,128]{1,0:T(8,128)(2,1)S(1)}, u32[]{:S(2)}, u32[]{:S(2)}) collective-permute-start(bf16[1024,128]{1,0:T(8,128)(2,1)S(1)} %collective-permute-done.11.refs_0_), channel_id=1, source_target_pairs={{0,32},{32,64},{64,96},{96,128},{128,160},{160,192},{192,224},{224... | collective-permute-start | bytes 786440 | tf_op jit(solution)/shard_map/ppermute | solution.py:35
  42.0 7.7 %collective-permute-start.5 = (bf16[784,128]{1,0:T(8,128)(2,1)S(1)}, bf16[784,128]{1,0:T(8,128)(2,1)S(1)}, u32[]{:S(2)}, u32[]{:S(2)}) collective-permute-start(bf16[784,128]{1,0:T(8,128)(2,1)S(1)} %get-tuple-element.27.own_ref.refs_0_), channel_id=1, source_target_pairs={{0,8},{8,16},{16,24},{24,0},{1,9},{9,17},{17,25},{25,1},{2,10},{10... | collective-permute-start | bytes 602120 | tf_op jit(solution)/shard_map/ppermute | solution.py:35
  43.4 10.9 %collective-permute-start.6 = (bf16[784,128]{1,0:T(8,128)(2,1)S(1)}, bf16[784,128]{1,0:T(8,128)(2,1)S(1)}, u32[]{:S(2)}, u32[]{:S(2)}) collective-permute-start(bf16[784,128]{1,0:T(8,128)(2,1)S(1)} %get-tuple-element.27.own_ref.refs_0_), channel_id=1, source_target_pairs={{0,16},{8,24},{16,0},{24,8},{1,17},{9,25},{17,1},{25,9},{2,18},{10... | collective-permute-start | bytes 602120 | tf_op jit(solution)/shard_map/ppermute | solution.py:35
  45.9 8.4 %collective-permute-start.7 = (bf16[784,128]{1,0:T(8,128)(2,1)S(1)}, bf16[784,128]{1,0:T(8,128)(2,1)S(1)}, u32[]{:S(2)}, u32[]{:S(2)}) collective-permute-start(bf16[784,128]{1,0:T(8,128)(2,1)S(1)} %get-tuple-element.27.own_ref.refs_0_), channel_id=1, source_target_pairs={{0,24},{8,0},{16,8},{24,16},{1,25},{9,1},{17,9},{25,17},{2,26},{10... | collective-permute-start | bytes 602120 | tf_op jit(solution)/shard_map/ppermute | solution.py:35
  47.0 12.1 %collective-permute-start.15 = (bf16[1024,128]{1,0:T(8,128)(2,1)S(1)}, bf16[1024,128]{1,0:T(8,128)(2,1)S(1)}, u32[]{:S(2)}, u32[]{:S(2)}) collective-permute-start(bf16[1024,128]{1,0:T(8,128)(2,1)S(1)} %collective-permute-done.14.refs_1_), channel_id=1, source_target_pairs={{0,224},{32,0},{64,32},{96,64},{128,96},{160,128},{192,160},{224,1... | collective-permute-start | bytes 786440 | tf_op jit(solution)/shard_map/ppermute | solution.py:35
  49.7 11.9 %collective-permute-start.13 = (bf16[1024,128]{1,0:T(8,128)(2,1)S(1)}, bf16[1024,128]{1,0:T(8,128)(2,1)S(1)}, u32[]{:S(2)}, u32[]{:S(2)}) collective-permute-start(bf16[1024,128]{1,0:T(8,128)(2,1)S(1)} %collective-permute-done.12.refs_0_), channel_id=1, source_target_pairs={{0,32},{32,64},{64,96},{96,128},{128,160},{160,192},{192,224},{224... | collective-permute-start | bytes 786440 | tf_op jit(solution)/shard_map/ppermute | solution.py:35
  55.0 28.3 %collective-permute-start.8 = (bf16[272,128]{1,0:T(8,128)(2,1)S(1)}, bf16[272,128]{1,0:T(8,128)(2,1)S(1)}, u32[]{:S(2)}, u32[]{:S(2)}) collective-permute-start(bf16[272,128]{1,0:T(8,128)(2,1)S(1)} %get-tuple-element.29), channel_id=1, source_target_pairs={{0,32},{32,0},{64,96},{96,64},{128,160},{160,128},{192,224},{224,1... | collective-permute-start | bytes 208904 | tf_op jit(solution)/shard_map/ppermute | solution.py:597
  59.2 14.8 %collective-permute-start.16 = (bf16[1024,128]{1,0:T(8,128)(2,1)S(1)}, bf16[1024,128]{1,0:T(8,128)(2,1)S(1)}, u32[]{:S(2)}, u32[]{:S(2)}) collective-permute-start(bf16[1024,128]{1,0:T(8,128)(2,1)S(1)} %collective-permute-done.15.refs_1_), channel_id=1, source_target_pairs={{0,224},{32,0},{64,32},{96,64},{128,96},{160,128},{192,160},{224,1... | collective-permute-start | bytes 786440 | tf_op jit(solution)/shard_map/ppermute | solution.py:35
  61.6 12.3 %collective-permute-start.17 = (bf16[1024,128]{1,0:T(8,128)(2,1)S(1)}, bf16[1024,128]{1,0:T(8,128)(2,1)S(1)}, u32[]{:S(2)}, u32[]{:S(2)}) collective-permute-start(bf16[1024,128]{1,0:T(8,128)(2,1)S(1)} %collective-permute-done.13.refs_0_), channel_id=1, source_target_pairs={{0,32},{32,64},{64,96},{96,128},{128,160},{160,192},{192,224},{224... | collective-permute-start | bytes 786440 | tf_op jit(solution)/shard_map/ppermute | solution.py:35
  74.0 19.0 %copy-start = (bf16[1024,128]{1,0:T(8,128)(2,1)}, bf16[1024,128]{1,0:T(8,128)(2,1)S(1)}, u32[]{:S(2)}) copy-start(bf16[1024,128]{1,0:T(8,128)(2,1)S(1)} %collective-permute-done.17.refs_2_) | copy-start | bytes 786436
  77.3 22.0 %copy-start.5 = (f32[128]{0:T(128)S(1)}, f32[128]{0:T(128)}, u32[]{:S(2)}) copy-start(f32[128]{0:T(128)} %param.24) | copy-start | bytes 1540
  77.3 101.9 %collective-permute-start.19 = (bf16[288,512]{1,0:T(8,128)(2,1)}, bf16[288,512]{1,0:T(8,128)(2,1)}, u32[]{:S(2)}, u32[]{:S(2)}) collective-permute-start(bf16[288,512]{1,0:T(8,128)(2,1)} %attend_last.6), channel_id=1, source_target_pairs={{0,8},{8,16},{16,24},{24,0},{1,9},{9,17},{17,25},{25,1},{2,10},{10... | collective-permute-start | bytes 884744 | tf_op jit(solution)/shard_map/ppermute | solution.py:35
  82.5 96.7 %collective-permute-start.18 = (bf16[288,512]{1,0:T(8,128)(2,1)}, bf16[288,512]{1,0:T(8,128)(2,1)}, u32[]{:S(2)}, u32[]{:S(2)}) collective-permute-start(bf16[288,512]{1,0:T(8,128)(2,1)} %attend_last.5), channel_id=1, source_target_pairs={{0,24},{8,0},{16,8},{24,16},{1,25},{9,1},{17,9},{25,17},{2,26},{10... | collective-permute-start | bytes 884744 | tf_op jit(solution)/shard_map/ppermute | solution.py:35
  83.9 4.6 %collective-permute-start.9 = (bf16[272,128]{1,0:T(8,128)(2,1)S(1)}, bf16[272,128]{1,0:T(8,128)(2,1)S(1)}, u32[]{:S(2)}, u32[]{:S(2)}) collective-permute-start(bf16[272,128]{1,0:T(8,128)(2,1)S(1)} %get-tuple-element.31), channel_id=1, source_target_pairs={{0,64},{32,96},{64,0},{96,32},{128,192},{160,224},{192,128},{224,1... | collective-permute-start | bytes 208904 | tf_op jit(solution)/shard_map/ppermute | solution.py:597
  89.1 90.0 %copy-start.6 = (f32[128]{0:T(128)S(1)}, f32[128]{0:T(128)}, u32[]{:S(2)}) copy-start(f32[128]{0:T(128)} %param.29) | copy-start | bytes 1540
  89.1 10.1 %collective-permute-start.10 = (bf16[272,128]{1,0:T(8,128)(2,1)S(1)}, bf16[272,128]{1,0:T(8,128)(2,1)S(1)}, u32[]{:S(2)}, u32[]{:S(2)}) collective-permute-start(bf16[272,128]{1,0:T(8,128)(2,1)S(1)} %get-tuple-element.33), channel_id=1, source_target_pairs={{0,128},{32,160},{64,192},{96,224},{128,0},{160,32},{192,64},{224,... | collective-permute-start | bytes 208904 | tf_op jit(solution)/shard_map/ppermute | solution.py:597
  96.2 82.9 %collective-permute-start.20 = (bf16[144,512]{1,0:T(8,128)(2,1)}, bf16[144,512]{1,0:T(8,128)(2,1)}, u32[]{:S(2)}, u32[]{:S(2)}) collective-permute-start(bf16[144,512]{1,0:T(8,128)(2,1)} %get-tuple-element.45), channel_id=1, source_target_pairs={{0,16},{8,24},{16,0},{24,8},{1,17},{9,25},{17,1},{25,9},{2,18},{10... | collective-permute-start | bytes 442376 | tf_op jit(solution)/shard_map/ppermute | solution.py:35
  97.5 81.6 %collective-permute-start.21 = (bf16[144,512]{1,0:T(8,128)(2,1)}, bf16[144,512]{1,0:T(8,128)(2,1)}, u32[]{:S(2)}, u32[]{:S(2)}) collective-permute-start(bf16[144,512]{1,0:T(8,128)(2,1)} %get-tuple-element.46), channel_id=1, source_target_pairs={{0,16},{8,24},{16,0},{24,8},{1,17},{9,25},{17,1},{25,9},{2,18},{10... | collective-permute-start | bytes 442376 | tf_op jit(solution)/shard_map/ppermute | solution.py:35
  100.8 80.7 %all-to-all-start = ((bf16[8,64,128]{2,1,0:T(8,128)(2,1)}), bf16[8,64,128]{2,1,0:T(8,128)(2,1)}, u32[]{:S(2)}, u32[]{:S(2)}) async-start(bf16[8,64,128]{2,1,0:T(8,128)(2,1)} %bitcast.29), calls=%async_computation | async-start | bytes 262144 | tf_op jit(solution)/shard_map/all_to_all | solution.py:612
  181.4 10.1 %all-to-all-start.1 = ((bf16[8,64,128]{2,1,0:T(8,128)(2,1)}), bf16[8,64,128]{2,1,0:T(8,128)(2,1)S(1)}, u32[]{:S(2)}, u32[]{:S(2)}) async-start(bf16[8,64,128]{2,1,0:T(8,128)(2,1)} %bitcast.8), calls=%async_computation.1 | async-start | bytes 262144 | tf_op jit(solution)/shard_map/all_to_all | solution.py:615
  (6 other events, 65.4 us)

commit v4 on v3

--- a/solution.py
+++ b/solution.py
@@ -518,7 +518,13 @@
     )(turned, *pieces, *state)
 
 
-def mix_body(a_ref, b_ref, c_ref, low_ref, high_ref, weight_ref, gain_ref, out_ref):
+SWAP = TOK // (NY * NC)
+
+
+def mix_body(
+    place_ref, rec_ref, a_ref, b_ref, c_ref, low_ref, high_ref, weight_ref, gain_ref,
+    keep_ref, give_ref, att_ref,
+):
     mixed = None
     for m in range(2):
         places = [(ref, m * MAP_ROWS) for ref in (a_ref, b_ref, c_ref)]
@@ -536,19 +542,75 @@
             term = ref[at : at + AV, :].astype(F32) * (share * scale)
             mixed = term if mixed is None else mixed + term
     scale = lax.rsqrt(jnp.mean(mixed * mixed, axis=0, keepdims=True) + EPS)
-    out_ref[...] = ((mixed * scale).T * gain_ref[...]).astype(BF16)
-
-
-def mix(partials, weight, gain):
+    att_ref[...] = ((mixed * scale).T * gain_ref[...]).astype(BF16)
+    y, c = place_ref[2], place_ref[3]
+    for ref, core in ((keep_ref, c), (give_ref, 1 - c)):
+        for k in range(NY):
+            at = pl.multiple_of((((y + k) % NY) * NC + core) * SWAP, SWAP)
+            ref[k, :, :HV] = rec_ref[pl.ds(at, SWAP), :]
+            ref[k, :, HV:] = att_ref[pl.ds(at, SWAP), :]
+
+
+def mix(place, rec_rows, partials, weight, gain):
+    half = jax.ShapeDtypeStruct((NY, SWAP, HV + AV), BF16)
     return pl.pallas_call(
         mix_body,
-        in_specs=[VMEM] * 5 + [SMEM, VMEM],
-        out_specs=VMEM,
-        out_shape=jax.ShapeDtypeStruct((TOK, AV), BF16),
+        in_specs=[SMEM] + [VMEM] * 6 + [SMEM, VMEM],
+        out_specs=[VMEM] * 2,
+        out_shape=[half, half],
+        scratch_shapes=[pltpu.VMEM((TOK, AV), BF16)],
         cost_estimate=cost(1 << 22),
         compiler_params=limit(6),
         name="mix",
-    )(*partials, weight, gain.reshape(1, AV))
+    )(place, rec_rows, *partials, weight, gain.reshape(1, AV))
+
+
+def join_body(place_ref, keep_ref, got_ref, *out_refs):
+    first = place_ref[3] == 0
+    for k, ref in enumerate(out_refs):
+        keep, got = keep_ref[k], got_ref[k]
+        low, high = jnp.where(first, keep, got), jnp.where(first, got, keep)
+        ref[:, :HV], ref[:, HV : 2 * HV] = low[:, :HV], high[:, :HV]
+        ref[:, 2 * HV : 2 * HV + AV], ref[:, 2 * HV + AV :] = low[:, HV:], high[:, HV:]
+
+
+def join(place, keep, got):
+    return pl.pallas_call(
+        join_body,
+        in_specs=[SMEM, VMEM, VMEM],
+        out_specs=[VMEM] * NY,
+        out_shape=[jax.ShapeDtypeStruct((SWAP, 2 * (HV + AV)), BF16)] * NY,
+        cost_estimate=cost(1 << 20),
+        compiler_params=limit(2),
+        name="join",
+    )(place, keep, got)
+
+
+def project_body(place_ref, *refs):
+    sources, (rec_ref, att_ref, out_ref) = refs[:NY], refs[NY:]
+    total = None
+    for weights_ref, width, start in ((rec_ref, 2 * HV, 0), (att_ref, 2 * AV, 2 * HV)):
+        for k, ref in enumerate(sources):
+            at = pl.multiple_of(((place_ref[2] + NY - k) % NY) * width, width)
+            term = jnp.dot(
+                ref[:, start : start + width],
+                weights_ref[pl.ds(at, width), :],
+                preferred_element_type=F32,
+            )
+            total = term if total is None else total + term
+    out_ref[...] = total.astype(BF16)
+
+
+def project(place, sources, out_rec, out_att):
+    return pl.pallas_call(
+        project_body,
+        in_specs=[SMEM] + [VMEM] * (NY + 2),
+        out_specs=VMEM,
+        out_shape=jax.ShapeDtypeStruct((SWAP, out_rec.shape[1]), BF16),
+        cost_estimate=cost(1 << 29),
+        compiler_params=limit(6),
+        name="project",
+    )(place, *sources, out_rec, out_att)
 
 
 def on_device(
@@ -609,11 +671,14 @@
     from_below = shift(send, "x", 1, NX)
     (own,) = attend_last(turned, ends, state, 0, 1)
     rec_rows = finish(place, bit, kept, received, out_local, read_f, read_b, rec_gain)
-    rec_all = lax.all_to_all(rec_rows, TP, split_axis=0, concat_axis=1, tiled=True)
-    rec_part = jnp.dot(rec_all, out_rec, preferred_element_type=F32)
-    att_rows = mix([own, from_above, from_below, far_low, far_high], lambdas, att_gain)
-    att_all = lax.all_to_all(att_rows, TP, split_axis=0, concat_axis=1, tiled=True)
-    return (rec_part + jnp.dot(att_all, out_att, preferred_element_type=F32)).astype(BF16)
+    partials = [own, from_above, from_below, far_low, far_high]
+    keep, give = mix(place, rec_rows, partials, lambdas, att_gain)
+    got = shift(give, "c", 1, NC)
+    joined = join(place, keep, got)
+    sources = [joined[0]]
+    for k in range(1, NY):
+        sources.append(shift(joined[k], "y", k, NY))
+    return project(place, sources, out_rec, out_att)
 
 
 def solution(mesh):

time: 196 us -> 190 us (0.969)
  waiting for transfers between devices: 24.6 us -> 33 us
  starting transfers between devices: 116 us -> 109 us
  matrix products: 6.84 us -> 0 us
    all_to_all x2 -> x0, starting transfers between devices: 79 us -> none  [the longest x1 74.2 us: on_device(): lax.all_to_all(rec_rows, TP, split_axis=0, concat_axis=1, tiled=True)]
    ppermute x19 -> x23, starting transfers between devices: 30 us -> 104 us  [shift(): lax.ppermute(value, axis, [(i, (i + by) % size) for i in range(size)])]
    dot_general x2 -> x0, matrix products: 6.84 us -> none  [the longest x1 3.74 us: on_device(): jnp.dot(att_all, out_att, preferred_element_type=F32)]
    ppermute x3, waiting for transfers between devices: 1.7 us -> 7.66 us  [on_device(): received = lax.ppermute(sent, 'z', [(i, i ^ bit) for i in range(NZ)])]
    ppermute x19 -> x23, waiting for transfers between devices: 20.8 us -> 25.3 us  [shift(): lax.ppermute(value, axis, [(i, (i + by) % size) for i in range(size)])]
    pallas_call x1 -> x3, Pallas kernels: 2.25 us -> 4.44 us  [the longest x1 2.83 us: project(): pl.pallas_call(project_body, in_specs=[SMEM] + [VMEM] * (NY + 2), out_spe...]
    pallas_call x4, Pallas kernels: 12.3 us -> 10.2 us  [attend_last(): pl.pallas_call(functools.partial(attend_last_body, chunks=len(pieces), ti...]
    all_to_all x2 -> x0, waiting for transfers between devices: 2.13 us -> none  [the longest x1 2.13 us: on_device(): lax.all_to_all(att_rows, TP, split_axis=0, concat_axis=1, tiled=True)]
  transfers between devices with their start and end apart: 24 -> 26, of which waited for: 9 -> 11; matrix products, arithmetic and copies ran while one was open for 3% -> 1% of each run, Pallas kernels for 20% -> 17%
where the time goes in v4:
time: 190 us; the launch traced here: 188 us
  starting transfers between devices  109 us (57%)
  Pallas kernels  40.8 us (21%)
  waiting for transfers between devices  33 us (17%)
  other arithmetic  3.85 us (2%)
    ppermute x23, starting transfers between devices, shift(): lax.ppermute(value, axis, [(i, (i + by) % size) for i in range(size)])  104 us
    ppermute x23, waiting for transfers between devices, shift(): lax.ppermute(value, axis, [(i, (i + by) % size) for i in range(size)])  25.3 us
    pallas_call x2, Pallas kernels, attend_more(): pl.pallas_call(functools.partial(attend_more_body, chunks=len(pieces)), i...  12 us
    pallas_call x4, Pallas kernels, attend_last(): pl.pallas_call(functools.partial(attend_last_body, chunks=len(pieces), ti...  10.2 us
    ppermute x3, waiting for transfers between devices, on_device(): received = lax.ppermute(sent, 'z', [(i, i ^ bit) for i in range(NZ)])  7.66 us
    pallas_call x1, Pallas kernels, make_local(): pl.pallas_call(local_body, in_specs=[VMEM] * 10, out_specs=[VMEM] * 4, ou...  5.9 us
    ppermute x3, starting transfers between devices, on_device(): received = lax.ppermute(sent, 'z', [(i, i ^ bit) for i in range(NZ)])  4.74 us
    pallas_call x1, Pallas kernels, attend_first(): pl.pallas_call(attend_first_body, in_specs=[VMEM] * (NX + 1), out_specs=[...  4.09 us
  transfers between devices with their start and end apart: 26, of which 11 were waited for; matrix products, arithmetic and copies ran while one was open for 1% of the time, Pallas kernels for 17%

profile of v4, /device:TPU:1, one launch (start us, length us, event | category | flops | bytes accessed | tf_op | source)
XLA Modules:
  0.0 187.6 jit_solution(10690094192114389338)
XLA Ops:
  2.3 2.2 %collective-permute-start = (bf16[64,2048]{1,0:T(8,128)(2,1)S(1)}, bf16[64,2048]{1,0:T(8,128)(2,1)S(1)}, u32[]{:S(2)}, u32[]{:S(2)}) collective-permute-start(bf16[64,2048]{1,0:T(8,128)(2,1)S(1)} %get-tuple-element.60), channel_id=1, source_target_pairs={{0,2},{2,4},{4,6},{6,0},{1,3},{3,5},{5,7},{7,1},{8,10},{10,12},{12... | collective-permute-start | bytes 786440 | tf_op jit(solution)/shard_map/ppermute | solution.py:35
  4.5 1.5 collective-permute-start.1
  6.1 1.6 collective-permute-start.2
  11.2 4.4 %collective-permute-done.2 = bf16[32,2048]{1,0:T(8,128)(2,1)S(1)} collective-permute-done((bf16[32,2048]{1,0:T(8,128)(2,1)S(1)}, bf16[32,2048]{1,0:T(8,128)(2,1)S(1)}, u32[]{:S(2)}, u32[]{:S(2)}) %collective-permute-start.2) | collective-permute-done | bytes 131104 | tf_op jit(solution)/shard_map/ppermute | solution.py:35
  15.7 2.8 %collective-permute-done.3 = bf16[32,2048]{1,0:T(8,128)(2,1)S(1)} collective-permute-done((bf16[32,2048]{1,0:T(8,128)(2,1)S(1)}, bf16[32,2048]{1,0:T(8,128)(2,1)S(1)}, u32[]{:S(2)}, u32[]{:S(2)}) %collective-permute-start.3) | collective-permute-done | bytes 131104 | tf_op jit(solution)/shard_map/ppermute | solution.py:35
  18.5 1.6 collective-permute-start.4
  22.4 1.5 make_keys.1
  23.9 1.7 collective-permute-start.11
  25.6 4.0 %collective-permute-start.14 = (bf16[1024,128]{1,0:T(8,128)(2,1)S(1)}, bf16[1024,128]{1,0:T(8,128)(2,1)S(1)}, u32[]{:S(2)}, u32[]{:S(2)}) collective-permute-start(bf16[1024,128]{1,0:T(8,128)(2,1)S(1)} %get-tuple-element.43.refs_4_), channel_id=1, source_target_pairs={{0,224},{32,0},{64,32},{96,64},{128,96},{160,128},{192,160},{224,1... | collective-permute-start | bytes 786440 | tf_op jit(solution)/shard_map/ppermute | solution.py:35
  29.6 6.2 %collective-permute-done.11.refs_0_ = bf16[1024,128]{1,0:T(8,128)(2,1)S(1)} collective-permute-done((bf16[1024,128]{1,0:T(8,128)(2,1)S(1)}, bf16[1024,128]{1,0:T(8,128)(2,1)S(1)}, u32[]{:S(2)}, u32[]{:S(2)}) %collective-permute-start.11) | collective-permute-done | bytes 262176 | tf_op jit(solution)/shard_map/ppermute | solution.py:35
  36.1 5.9 %local.1 = (bf16[784,128]{1,0:T(8,128)(2,1)S(1)}, f32[512,128]{1,0:T(8,128)S(1)}, bf16[512,128]{1,0:T(8,128)(2,1)S(1)}, bf16[512,128]{1,0:T(8,128)(2,1)S(1)}) custom-call(bf16[512,2048]{1,0:T(8,128)(2,1)S(1)} %get-tuple-element.32.rows_ref, bf16[2048,128]{1,0:T(8,128)(2,1)S(1)} %copy-done.6, bf16[2048,128]{1,0:T(8,128)(2,1)S(1)} %copy-done.7, ...), custom_call_target="tpu_custom_call" | custom-call | flops 2147483648 | bytes 1048576 | tf_op jit(solution)/shard_map/local/pallas_call | solution.py:185
  43.4 2.5 %collective-permute-start.6 = (bf16[784,128]{1,0:T(8,128)(2,1)S(1)}, bf16[784,128]{1,0:T(8,128)(2,1)S(1)}, u32[]{:S(2)}, u32[]{:S(2)}) collective-permute-start(bf16[784,128]{1,0:T(8,128)(2,1)S(1)} %get-tuple-element.33.own_ref.refs_0_), channel_id=1, source_target_pairs={{0,16},{8,24},{16,0},{24,8},{1,17},{9,25},{17,1},{25,9},{2,18},{10... | collective-permute-start | bytes 602120 | tf_op jit(solution)/shard_map/ppermute | solution.py:35
  47.0 2.7 %collective-permute-start.15 = (bf16[1024,128]{1,0:T(8,128)(2,1)S(1)}, bf16[1024,128]{1,0:T(8,128)(2,1)S(1)}, u32[]{:S(2)}, u32[]{:S(2)}) collective-permute-start(bf16[1024,128]{1,0:T(8,128)(2,1)S(1)} %collective-permute-done.14.refs_1_), channel_id=1, source_target_pairs={{0,224},{32,0},{64,32},{96,64},{128,96},{160,128},{192,160},{224,1... | collective-permute-start | bytes 786440 | tf_op jit(solution)/shard_map/ppermute | solution.py:35
  49.7 4.6 %collective-permute-done.6.below2_ref.refs_3_ = bf16[784,128]{1,0:T(8,128)(2,1)S(1)} collective-permute-done((bf16[784,128]{1,0:T(8,128)(2,1)S(1)}, bf16[784,128]{1,0:T(8,128)(2,1)S(1)}, u32[]{:S(2)}, u32[]{:S(2)}) %collective-permute-start.6) | collective-permute-done | bytes 200736 | tf_op jit(solution)/shard_map/ppermute | solution.py:35
  54.3 4.1 %attend_first.1 = (bf16[4,128,512]{2,1,0:T(8,128)(2,1)S(1)}, f32[4,2,8,512]{3,2,1,0:T(8,128)S(1)}, f32[4,2,144,512]{3,2,1,0:T(8,128)S(1)}) custom-call(bf16[784,128]{1,0:T(8,128)(2,1)S(1)} %get-tuple-element.33.own_ref.refs_0_, bf16[784,128]{1,0:T(8,128)(2,1)S(1)} %collective-permute-done.5.below1_ref.refs_1_, ...), custom_call_target="tpu_custom_call" | custom-call | flops 805306368 | bytes 1048576 | tf_op jit(solution)/shard_map/attend_first/pallas_call | solution.py:479
  58.4 2.5 %collective-permute-start.16 = (bf16[1024,128]{1,0:T(8,128)(2,1)S(1)}, bf16[1024,128]{1,0:T(8,128)(2,1)S(1)}, u32[]{:S(2)}, u32[]{:S(2)}) collective-permute-start(bf16[1024,128]{1,0:T(8,128)(2,1)S(1)} %collective-permute-done.15.refs_1_), channel_id=1, source_target_pairs={{0,224},{32,0},{64,32},{96,64},{128,96},{160,128},{192,160},{224,1... | collective-permute-start | bytes 786440 | tf_op jit(solution)/shard_map/ppermute | solution.py:35
  60.9 6.0 %attend_more.2 = (f32[4,2,8,512]{3,2,1,0:T(8,128)S(1)}, f32[4,2,144,512]{3,2,1,0:T(8,128)S(1)}) custom-call(bf16[4,128,512]{2,1,0:T(8,128)(2,1)S(1)} %get-tuple-element.44.turned_ref, bf16[1024,128]{1,0:T(8,128)(2,1)S(1)} %collective-permute-done.11.refs_0_, bf16[1024,128]{1,0:T(8,128)(2,1)S(1)} %collective-permute-done.14.refs_1_, ...), custom_call_target="tpu_custom_call" | custom-call | flops 1610612736 | bytes 1048576 | tf_op jit(solution)/shard_map/attend_more/pallas_call | solution.py:491
  66.9 6.0 %attend_more.3 = (f32[4,2,8,512]{3,2,1,0:T(8,128)S(1)}, f32[4,2,144,512]{3,2,1,0:T(8,128)S(1)}) custom-call(bf16[4,128,512]{2,1,0:T(8,128)(2,1)S(1)} %get-tuple-element.44.turned_ref, bf16[1024,128]{1,0:T(8,128)(2,1)S(1)} %collective-permute-done.12.refs_0_, bf16[1024,128]{1,0:T(8,128)(2,1)S(1)} %collective-permute-done.15.refs_1_, ...), custom_call_target="tpu_custom_call" | custom-call | flops 1610612736 | bytes 1048576 | tf_op jit(solution)/shard_map/attend_more/pallas_call | solution.py:491
  72.9 2.5 %attend_last.6 = bf16[288,512]{1,0:T(8,128)(2,1)S(1)} custom-call(bf16[4,128,512]{2,1,0:T(8,128)(2,1)S(1)} %get-tuple-element.44.turned_ref, bf16[1024,128]{1,0:T(8,128)(2,1)S(1)} %collective-permute-done.13.refs_0_, bf16[1024,128]{1,0:T(8,128)(2,1)S(1)} %collective-permute-done.16.refs_1_, bf16[1024,128]{1,0:T(8,128)(2,1)S(1)} %collective-permute-done.17.refs_2_, ...), custom_call_target="tpu_custom_call" | custom-call | flops 603979776 | bytes 1048576 | tf_op jit(solution)/shard_map/attend_last/pallas_call | solution.py:504
  75.5 2.3 %collective-permute-start.19 = (bf16[288,512]{1,0:T(8,128)(2,1)S(1)}, bf16[288,512]{1,0:T(8,128)(2,1)S(1)}, u32[]{:S(2)}, u32[]{:S(2)}) collective-permute-start(bf16[288,512]{1,0:T(8,128)(2,1)S(1)} %attend_last.6), channel_id=1, source_target_pairs={{0,8},{8,16},{16,24},{24,0},{1,9},{9,17},{17,25},{25,1},{2,10},{10... | collective-permute-start | bytes 884744 | tf_op jit(solution)/shard_map/ppermute | solution.py:35
  77.7 2.5 %attend_last.5 = bf16[288,512]{1,0:T(8,128)(2,1)S(1)} custom-call(bf16[4,128,512]{2,1,0:T(8,128)(2,1)S(1)} %get-tuple-element.44.turned_ref, bf16[1024,128]{1,0:T(8,128)(2,1)S(1)} %collective-permute-done.13.refs_0_, bf16[1024,128]{1,0:T(8,128)(2,1)S(1)} %collective-permute-done.16.refs_1_, bf16[1024,128]{1,0:T(8,128)(2,1)S(1)} %collective-permute-done.17.refs_2_, ...), custom_call_target="tpu_custom_call" | custom-call | flops 603979776 | bytes 1048576 | tf_op jit(solution)/shard_map/attend_last/pallas_call | solution.py:504
  81.9 3.1 %collective-permute-done.8.received_ref = bf16[272,128]{1,0:T(8,128)(2,1)S(1)} collective-permute-done((bf16[272,128]{1,0:T(8,128)(2,1)S(1)}, bf16[272,128]{1,0:T(8,128)(2,1)S(1)}, u32[]{:S(2)}, u32[]{:S(2)}) %collective-permute-start.8) | collective-permute-done | bytes 69664 | tf_op jit(solution)/shard_map/ppermute | solution.py:659
  85.7 2.7 %collective-permute-start.9 = (bf16[272,128]{1,0:T(8,128)(2,1)S(1)}, bf16[272,128]{1,0:T(8,128)(2,1)S(1)}, u32[]{:S(2)}, u32[]{:S(2)}) collective-permute-start(bf16[272,128]{1,0:T(8,128)(2,1)S(1)} %get-tuple-element.37), channel_id=1, source_target_pairs={{0,64},{32,96},{64,0},{96,32},{128,192},{160,224},{192,128},{224,1... | collective-permute-start | bytes 208904 | tf_op jit(solution)/shard_map/ppermute | solution.py:659
  88.4 2.5 %attend_last.7 = (bf16[144,512]{1,0:T(8,128)(2,1)S(1)}, bf16[144,512]{1,0:T(8,128)(2,1)S(1)}) custom-call(bf16[4,128,512]{2,1,0:T(8,128)(2,1)S(1)} %get-tuple-element.44.turned_ref, bf16[1024,128]{1,0:T(8,128)(2,1)S(1)} %collective-permute-done.13.refs_0_, bf16[1024,128]{1,0:T(8,128)(2,1)S(1)} %collective-permute-done.16.refs_1_, ...), custom_call_target="tpu_custom_call" | custom-call | flops 603979776 | bytes 1048576 | tf_op jit(solution)/shard_map/attend_last/pallas_call | solution.py:504
  92.2 1.7 collective-permute-start.21
  94.6 2.0 %collective-permute-start.10 = (bf16[272,128]{1,0:T(8,128)(2,1)S(1)}, bf16[272,128]{1,0:T(8,128)(2,1)S(1)}, u32[]{:S(2)}, u32[]{:S(2)}) collective-permute-start(bf16[272,128]{1,0:T(8,128)(2,1)S(1)} %get-tuple-element.39), channel_id=1, source_target_pairs={{0,128},{32,160},{64,192},{96,224},{128,0},{160,32},{192,64},{224,... | collective-permute-start | bytes 208904 | tf_op jit(solution)/shard_map/ppermute | solution.py:659
  97.2 4.5 %collective-permute-done.10.received_ref = bf16[272,128]{1,0:T(8,128)(2,1)S(1)} collective-permute-done((bf16[272,128]{1,0:T(8,128)(2,1)S(1)}, bf16[272,128]{1,0:T(8,128)(2,1)S(1)}, u32[]{:S(2)}, u32[]{:S(2)}) %collective-permute-start.10) | collective-permute-done | bytes 69664 | tf_op jit(solution)/shard_map/ppermute | solution.py:659
  102.6 2.5 %attend_last.4.a_ref = bf16[288,512]{1,0:T(8,128)(2,1)S(1)} custom-call(bf16[4,128,512]{2,1,0:T(8,128)(2,1)S(1)} %get-tuple-element.44.turned_ref, bf16[1024,128]{1,0:T(8,128)(2,1)S(1)} %collective-permute-done.13.refs_0_, bf16[1024,128]{1,0:T(8,128)(2,1)S(1)} %collective-permute-done.16.refs_1_, bf16[1024,128]{1,0:T(8,128)(2,1)S(1)} %collective-permute-done.17.refs_2_, ...), custom_call_target="tpu_custom_call" | custom-call | flops 603979776 | bytes 1048576 | tf_op jit(solution)/shard_map/attend_last/pallas_call | solution.py:504
  106.2 70.6 %collective-permute-start.22 = (bf16[4,64,256]{2,1,0:T(8,128)(2,1)S(1)}, bf16[4,64,256]{2,1,0:T(8,128)(2,1)S(1)}, u32[]{:S(2)}, u32[]{:S(2)}) collective-permute-start(bf16[4,64,256]{2,1,0:T(8,128)(2,1)S(1)} %get-tuple-element.54), channel_id=1, source_target_pairs={{0,1},{1,0},{2,3},{3,2},{4,5},{5,4},{6,7},{7,6},{8,9},{9,8},{10,11... | collective-permute-start | bytes 393224 | tf_op jit(solution)/shard_map/ppermute | solution.py:35
  178.6 2.6 %collective-permute-start.25 = (bf16[64,512]{1,0:T(8,128)(2,1)S(1)}, bf16[64,512]{1,0:T(8,128)(2,1)S(1)}, u32[]{:S(2)}, u32[]{:S(2)}) collective-permute-start(bf16[64,512]{1,0:T(8,128)(2,1)S(1)} %get-tuple-element.58), channel_id=1, source_target_pairs={{0,6},{2,0},{4,2},{6,4},{1,7},{3,1},{5,3},{7,5},{8,14},{10,8},{12,... | collective-permute-start | bytes 196616 | tf_op jit(solution)/shard_map/ppermute | solution.py:35
  181.2 3.6 %collective-permute-done.23.refs_1_ = bf16[64,512]{1,0:T(8,128)(2,1)S(1)} collective-permute-done((bf16[64,512]{1,0:T(8,128)(2,1)S(1)}, bf16[64,512]{1,0:T(8,128)(2,1)S(1)}, u32[]{:S(2)}, u32[]{:S(2)}) %collective-permute-start.23) | collective-permute-done | bytes 65568 | tf_op jit(solution)/shard_map/ppermute | solution.py:35
  184.7 2.8 %project.1 = bf16[64,2048]{1,0:T(8,128)(2,1)} custom-call(s32[4]{0:T(128)S(1)} %pad_add_fusion.place_ref, bf16[64,512]{1,0:T(8,128)(2,1)S(1)} %get-tuple-element.55.refs_0_, bf16[64,512]{1,0:T(8,128)(2,1)S(1)} %collective-permute-done.23.refs_1_, bf16[64,512]{1,0:T(8,128)(2,1)S(1)} %collective-permute-done.24.refs_2_, ...), custom_call_target="tpu_custom_call" | custom-call | flops 536870912 | bytes 1048576 | tf_op jit(solution)/shard_map/project/pallas_call | solution.py:605
  (77 shorter events, 18.7 us)
Async XLA Ops:
  1.1 21.3 %copy-start.2 = (bf16[2048,128]{1,0:T(8,128)(2,1)S(1)}, bf16[2048,128]{1,0:T(8,128)(2,1)}, u32[]{:S(2)}) copy-start(bf16[2048,128]{1,0:T(8,128)(2,1)} %key_ref.1) | copy-start | bytes 1572868
  1.1 21.3 %copy-start.3 = (bf16[2048,128]{1,0:T(8,128)(2,1)S(1)}, bf16[2048,128]{1,0:T(8,128)(2,1)}, u32[]{:S(2)}) copy-start(bf16[2048,128]{1,0:T(8,128)(2,1)} %value_ref.1) | copy-start | bytes 1572868
  2.3 7.7 %collective-permute-start = (bf16[64,2048]{1,0:T(8,128)(2,1)S(1)}, bf16[64,2048]{1,0:T(8,128)(2,1)S(1)}, u32[]{:S(2)}, u32[]{:S(2)}) collective-permute-start(bf16[64,2048]{1,0:T(8,128)(2,1)S(1)} %get-tuple-element.60), channel_id=1, source_target_pairs={{0,2},{2,4},{4,6},{6,0},{1,3},{3,5},{5,7},{7,1},{8,10},{10,12},{12... | collective-permute-start | bytes 786440 | tf_op jit(solution)/shard_map/ppermute | solution.py:35
  4.5 6.7 %collective-permute-start.1 = (bf16[64,2048]{1,0:T(8,128)(2,1)S(1)}, bf16[64,2048]{1,0:T(8,128)(2,1)S(1)}, u32[]{:S(2)}, u32[]{:S(2)}) collective-permute-start(bf16[64,2048]{1,0:T(8,128)(2,1)S(1)} %get-tuple-element.60), channel_id=1, source_target_pairs={{0,6},{2,0},{4,2},{6,4},{1,7},{3,1},{5,3},{7,5},{8,14},{10,8},{12,... | collective-permute-start | bytes 786440 | tf_op jit(solution)/shard_map/ppermute | solution.py:35
  6.1 9.6 %collective-permute-start.2 = (bf16[32,2048]{1,0:T(8,128)(2,1)S(1)}, bf16[32,2048]{1,0:T(8,128)(2,1)S(1)}, u32[]{:S(2)}, u32[]{:S(2)}) collective-permute-start(bf16[32,2048]{1,0:T(8,128)(2,1)S(1)} %get-tuple-element.62), channel_id=1, source_target_pairs={{0,4},{2,6},{4,0},{6,2},{1,5},{3,7},{5,1},{7,3},{8,12},{10,14},{12... | collective-permute-start | bytes 393224 | tf_op jit(solution)/shard_map/ppermute | solution.py:35
  7.7 10.8 %collective-permute-start.3 = (bf16[32,2048]{1,0:T(8,128)(2,1)S(1)}, bf16[32,2048]{1,0:T(8,128)(2,1)S(1)}, u32[]{:S(2)}, u32[]{:S(2)}) collective-permute-start(bf16[32,2048]{1,0:T(8,128)(2,1)S(1)} %get-tuple-element.61), channel_id=1, source_target_pairs={{0,4},{2,6},{4,0},{6,2},{1,5},{3,7},{5,1},{7,3},{8,12},{10,14},{12... | collective-permute-start | bytes 393224 | tf_op jit(solution)/shard_map/ppermute | solution.py:35
  18.5 3.9 %collective-permute-start.4 = (bf16[256,2048]{1,0:T(8,128)(2,1)S(1)}, bf16[256,2048]{1,0:T(8,128)(2,1)S(1)}, u32[]{:S(2)}, u32[]{:S(2)}) collective-permute-start(bf16[256,2048]{1,0:T(8,128)(2,1)S(1)} %constant_dynamic-update-slice_fusion.mine_ref), channel_id=1, source_target_pairs={{0,1},{1,0},{2,3},{3,2},{4,5},{5,4},{6,7},{7,6},{8,9},{9,8},{10,11... | collective-permute-start | bytes 3145736 | tf_op jit(solution)/shard_map/ppermute | solution.py:35
  21.2 14.6 %copy-start.12 = (f32[2,512,1]{1,2,0:T(1,128)S(1)}, f32[2,512,1]{1,2,0:T(1,128)}, u32[]{:S(2)}) copy-start(f32[2,512,1]{1,2,0:T(1,128)} %param.23) | copy-start | bytes 12292
  23.9 12.0 %collective-permute-start.11 = (bf16[1024,128]{1,0:T(8,128)(2,1)S(1)}, bf16[1024,128]{1,0:T(8,128)(2,1)S(1)}, u32[]{:S(2)}, u32[]{:S(2)}) collective-permute-start(bf16[1024,128]{1,0:T(8,128)(2,1)S(1)} %get-tuple-element.43.refs_4_), channel_id=1, source_target_pairs={{0,32},{32,64},{64,96},{96,128},{128,160},{160,192},{192,224},{224... | collective-permute-start | bytes 786440 | tf_op jit(solution)/shard_map/ppermute | solution.py:35
  25.6 21.4 %collective-permute-start.14 = (bf16[1024,128]{1,0:T(8,128)(2,1)S(1)}, bf16[1024,128]{1,0:T(8,128)(2,1)S(1)}, u32[]{:S(2)}, u32[]{:S(2)}) collective-permute-start(bf16[1024,128]{1,0:T(8,128)(2,1)S(1)} %get-tuple-element.43.refs_4_), channel_id=1, source_target_pairs={{0,224},{32,0},{64,32},{96,64},{128,96},{160,128},{192,160},{224,1... | collective-permute-start | bytes 786440 | tf_op jit(solution)/shard_map/ppermute | solution.py:35
  35.8 13.8 %collective-permute-start.12 = (bf16[1024,128]{1,0:T(8,128)(2,1)S(1)}, bf16[1024,128]{1,0:T(8,128)(2,1)S(1)}, u32[]{:S(2)}, u32[]{:S(2)}) collective-permute-start(bf16[1024,128]{1,0:T(8,128)(2,1)S(1)} %collective-permute-done.11.refs_0_), channel_id=1, source_target_pairs={{0,32},{32,64},{64,96},{96,128},{128,160},{160,192},{192,224},{224... | collective-permute-start | bytes 786440 | tf_op jit(solution)/shard_map/ppermute | solution.py:35
  42.0 7.7 %collective-permute-start.5 = (bf16[784,128]{1,0:T(8,128)(2,1)S(1)}, bf16[784,128]{1,0:T(8,128)(2,1)S(1)}, u32[]{:S(2)}, u32[]{:S(2)}) collective-permute-start(bf16[784,128]{1,0:T(8,128)(2,1)S(1)} %get-tuple-element.33.own_ref.refs_0_), channel_id=1, source_target_pairs={{0,8},{8,16},{16,24},{24,0},{1,9},{9,17},{17,25},{25,1},{2,10},{10... | collective-permute-start | bytes 602120 | tf_op jit(solution)/shard_map/ppermute | solution.py:35
  43.4 10.9 %collective-permute-start.6 = (bf16[784,128]{1,0:T(8,128)(2,1)S(1)}, bf16[784,128]{1,0:T(8,128)(2,1)S(1)}, u32[]{:S(2)}, u32[]{:S(2)}) collective-permute-start(bf16[784,128]{1,0:T(8,128)(2,1)S(1)} %get-tuple-element.33.own_ref.refs_0_), channel_id=1, source_target_pairs={{0,16},{8,24},{16,0},{24,8},{1,17},{9,25},{17,1},{25,9},{2,18},{10... | collective-permute-start | bytes 602120 | tf_op jit(solution)/shard_map/ppermute | solution.py:35
  45.8 8.4 %collective-permute-start.7 = (bf16[784,128]{1,0:T(8,128)(2,1)S(1)}, bf16[784,128]{1,0:T(8,128)(2,1)S(1)}, u32[]{:S(2)}, u32[]{:S(2)}) collective-permute-start(bf16[784,128]{1,0:T(8,128)(2,1)S(1)} %get-tuple-element.33.own_ref.refs_0_), channel_id=1, source_target_pairs={{0,24},{8,0},{16,8},{24,16},{1,25},{9,1},{17,9},{25,17},{2,26},{10... | collective-permute-start | bytes 602120 | tf_op jit(solution)/shard_map/ppermute | solution.py:35
  47.0 11.4 %collective-permute-start.15 = (bf16[1024,128]{1,0:T(8,128)(2,1)S(1)}, bf16[1024,128]{1,0:T(8,128)(2,1)S(1)}, u32[]{:S(2)}, u32[]{:S(2)}) collective-permute-start(bf16[1024,128]{1,0:T(8,128)(2,1)S(1)} %collective-permute-done.14.refs_1_), channel_id=1, source_target_pairs={{0,224},{32,0},{64,32},{96,64},{128,96},{160,128},{192,160},{224,1... | collective-permute-start | bytes 786440 | tf_op jit(solution)/shard_map/ppermute | solution.py:35
  49.7 11.2 %collective-permute-start.13 = (bf16[1024,128]{1,0:T(8,128)(2,1)S(1)}, bf16[1024,128]{1,0:T(8,128)(2,1)S(1)}, u32[]{:S(2)}, u32[]{:S(2)}) collective-permute-start(bf16[1024,128]{1,0:T(8,128)(2,1)S(1)} %collective-permute-done.12.refs_0_), channel_id=1, source_target_pairs={{0,32},{32,64},{64,96},{96,128},{128,160},{160,192},{192,224},{224... | collective-permute-start | bytes 786440 | tf_op jit(solution)/shard_map/ppermute | solution.py:35
  58.4 14.5 %collective-permute-start.16 = (bf16[1024,128]{1,0:T(8,128)(2,1)S(1)}, bf16[1024,128]{1,0:T(8,128)(2,1)S(1)}, u32[]{:S(2)}, u32[]{:S(2)}) collective-permute-start(bf16[1024,128]{1,0:T(8,128)(2,1)S(1)} %collective-permute-done.15.refs_1_), channel_id=1, source_target_pairs={{0,224},{32,0},{64,32},{96,64},{128,96},{160,128},{192,160},{224,1... | collective-permute-start | bytes 786440 | tf_op jit(solution)/shard_map/ppermute | solution.py:35
  60.9 12.0 %collective-permute-start.17 = (bf16[1024,128]{1,0:T(8,128)(2,1)S(1)}, bf16[1024,128]{1,0:T(8,128)(2,1)S(1)}, u32[]{:S(2)}, u32[]{:S(2)}) collective-permute-start(bf16[1024,128]{1,0:T(8,128)(2,1)S(1)} %collective-permute-done.13.refs_0_), channel_id=1, source_target_pairs={{0,32},{32,64},{64,96},{96,128},{128,160},{160,192},{192,224},{224... | collective-permute-start | bytes 786440 | tf_op jit(solution)/shard_map/ppermute | solution.py:35
  75.5 29.7 %collective-permute-start.19 = (bf16[288,512]{1,0:T(8,128)(2,1)S(1)}, bf16[288,512]{1,0:T(8,128)(2,1)S(1)}, u32[]{:S(2)}, u32[]{:S(2)}) collective-permute-start(bf16[288,512]{1,0:T(8,128)(2,1)S(1)} %attend_last.6), channel_id=1, source_target_pairs={{0,8},{8,16},{16,24},{24,0},{1,9},{9,17},{17,25},{25,1},{2,10},{10... | collective-permute-start | bytes 884744 | tf_op jit(solution)/shard_map/ppermute | solution.py:35
  80.3 24.9 %collective-permute-start.18 = (bf16[288,512]{1,0:T(8,128)(2,1)S(1)}, bf16[288,512]{1,0:T(8,128)(2,1)S(1)}, u32[]{:S(2)}, u32[]{:S(2)}) collective-permute-start(bf16[288,512]{1,0:T(8,128)(2,1)S(1)} %attend_last.5), channel_id=1, source_target_pairs={{0,24},{8,0},{16,8},{24,16},{1,25},{9,1},{17,9},{25,17},{2,26},{10... | collective-permute-start | bytes 884744 | tf_op jit(solution)/shard_map/ppermute | solution.py:35
  81.8 19.9 %copy-start.4 = (f32[128]{0:T(128)S(1)}, f32[128]{0:T(128)}, u32[]{:S(2)}) copy-start(f32[128]{0:T(128)} %param.24) | copy-start | bytes 1540
  81.8 3.2 %collective-permute-start.8 = (bf16[272,128]{1,0:T(8,128)(2,1)S(1)}, bf16[272,128]{1,0:T(8,128)(2,1)S(1)}, u32[]{:S(2)}, u32[]{:S(2)}) collective-permute-start(bf16[272,128]{1,0:T(8,128)(2,1)S(1)} %get-tuple-element.35), channel_id=1, source_target_pairs={{0,32},{32,0},{64,96},{96,64},{128,160},{160,128},{192,224},{224,1... | collective-permute-start | bytes 208904 | tf_op jit(solution)/shard_map/ppermute | solution.py:659
  85.7 8.3 %collective-permute-start.9 = (bf16[272,128]{1,0:T(8,128)(2,1)S(1)}, bf16[272,128]{1,0:T(8,128)(2,1)S(1)}, u32[]{:S(2)}, u32[]{:S(2)}) collective-permute-start(bf16[272,128]{1,0:T(8,128)(2,1)S(1)} %get-tuple-element.37), channel_id=1, source_target_pairs={{0,64},{32,96},{64,0},{96,32},{128,192},{160,224},{192,128},{224,1... | collective-permute-start | bytes 208904 | tf_op jit(solution)/shard_map/ppermute | solution.py:659
  88.4 96.4 %copy-start.1 = (bf16[1024,2048]{1,0:T(8,128)(2,1)S(1)}, bf16[1024,2048]{1,0:T(8,128)(2,1)}, u32[]{:S(2)}) copy-start(bf16[1024,2048]{1,0:T(8,128)(2,1)} %refs_5_.1) | copy-start | bytes 12582916
  90.9 14.3 %collective-permute-start.20 = (bf16[144,512]{1,0:T(8,128)(2,1)S(1)}, bf16[144,512]{1,0:T(8,128)(2,1)S(1)}, u32[]{:S(2)}, u32[]{:S(2)}) collective-permute-start(bf16[144,512]{1,0:T(8,128)(2,1)S(1)} %get-tuple-element.51), channel_id=1, source_target_pairs={{0,16},{8,24},{16,0},{24,8},{1,17},{9,25},{17,1},{25,9},{2,18},{10... | collective-permute-start | bytes 442376 | tf_op jit(solution)/shard_map/ppermute | solution.py:35
  92.2 12.9 %collective-permute-start.21 = (bf16[144,512]{1,0:T(8,128)(2,1)S(1)}, bf16[144,512]{1,0:T(8,128)(2,1)S(1)}, u32[]{:S(2)}, u32[]{:S(2)}) collective-permute-start(bf16[144,512]{1,0:T(8,128)(2,1)S(1)} %get-tuple-element.52), channel_id=1, source_target_pairs={{0,16},{8,24},{16,0},{24,8},{1,17},{9,25},{17,1},{25,9},{2,18},{10... | collective-permute-start | bytes 442376 | tf_op jit(solution)/shard_map/ppermute | solution.py:35
  94.6 7.2 %collective-permute-start.10 = (bf16[272,128]{1,0:T(8,128)(2,1)S(1)}, bf16[272,128]{1,0:T(8,128)(2,1)S(1)}, u32[]{:S(2)}, u32[]{:S(2)}) collective-permute-start(bf16[272,128]{1,0:T(8,128)(2,1)S(1)} %get-tuple-element.39), channel_id=1, source_target_pairs={{0,128},{32,160},{64,192},{96,224},{128,0},{160,32},{192,64},{224,... | collective-permute-start | bytes 208904 | tf_op jit(solution)/shard_map/ppermute | solution.py:659
  102.6 82.1 %copy-start = (bf16[1024,2048]{1,0:T(8,128)(2,1)S(1)}, bf16[1024,2048]{1,0:T(8,128)(2,1)}, u32[]{:S(2)}) copy-start(bf16[1024,2048]{1,0:T(8,128)(2,1)} %refs_4_.1) | copy-start | bytes 12582916
  106.2 71.6 %collective-permute-start.22 = (bf16[4,64,256]{2,1,0:T(8,128)(2,1)S(1)}, bf16[4,64,256]{2,1,0:T(8,128)(2,1)S(1)}, u32[]{:S(2)}, u32[]{:S(2)}) collective-permute-start(bf16[4,64,256]{2,1,0:T(8,128)(2,1)S(1)} %get-tuple-element.54), channel_id=1, source_target_pairs={{0,1},{1,0},{2,3},{3,2},{4,5},{5,4},{6,7},{7,6},{8,9},{9,8},{10,11... | collective-permute-start | bytes 393224 | tf_op jit(solution)/shard_map/ppermute | solution.py:35
  178.4 6.3 %collective-permute-start.23 = (bf16[64,512]{1,0:T(8,128)(2,1)S(1)}, bf16[64,512]{1,0:T(8,128)(2,1)S(1)}, u32[]{:S(2)}, u32[]{:S(2)}) collective-permute-start(bf16[64,512]{1,0:T(8,128)(2,1)S(1)} %get-tuple-element.56), channel_id=1, source_target_pairs={{0,2},{2,4},{4,6},{6,0},{1,3},{3,5},{5,7},{7,1},{8,10},{10,12},{12... | collective-permute-start | bytes 196616 | tf_op jit(solution)/shard_map/ppermute | solution.py:35
  178.5 6.2 %collective-permute-start.24 = (bf16[64,512]{1,0:T(8,128)(2,1)S(1)}, bf16[64,512]{1,0:T(8,128)(2,1)S(1)}, u32[]{:S(2)}, u32[]{:S(2)}) collective-permute-start(bf16[64,512]{1,0:T(8,128)(2,1)S(1)} %get-tuple-element.57), channel_id=1, source_target_pairs={{0,4},{2,6},{4,0},{6,2},{1,5},{3,7},{5,1},{7,3},{8,12},{10,14},{12... | collective-permute-start | bytes 196616 | tf_op jit(solution)/shard_map/ppermute | solution.py:35
  178.6 6.1 %collective-permute-start.25 = (bf16[64,512]{1,0:T(8,128)(2,1)S(1)}, bf16[64,512]{1,0:T(8,128)(2,1)S(1)}, u32[]{:S(2)}, u32[]{:S(2)}) collective-permute-start(bf16[64,512]{1,0:T(8,128)(2,1)S(1)} %get-tuple-element.58), channel_id=1, source_target_pairs={{0,6},{2,0},{4,2},{6,4},{1,7},{3,1},{5,3},{7,5},{8,14},{10,8},{12,... | collective-permute-start | bytes 196616 | tf_op jit(solution)/shard_map/ppermute | solution.py:35
  (7 other events, 89.5 us)

commit v5 on v4

--- a/solution.py
+++ b/solution.py
@@ -29,6 +29,9 @@
 EPS = 1e-06
 THETA = 500000.0
 RISE = 40.0
+LOW = -1e30
+PEERS = NX - 1
+FAR = 384
 
 
 def shift(value, axis, by, size):
@@ -114,7 +117,7 @@
 
 def local_body(
     rows_ref, aq_ref, q_ref, f_ref, b_ref, v_ref, leak_ref, decay_ref, cos_ref, sin_ref,
-    pack_ref, out_ref, read_f_ref, read_b_ref,
+    pack_ref, far_a_ref, far_b_ref, out_ref, read_f_ref, read_b_ref,
 ):
     def project(*weights):
         joined = jnp.concatenate([w[...] for w in weights], axis=1)
@@ -179,15 +182,19 @@
     pack_ref[TOK + 2 * HV :, :] = jnp.concatenate(
         [*totals, jnp.zeros((PACK - TOK - 2 * HV - 2, HK), F32)]
     ).astype(BF16)
+    far_a_ref[...] = pack_ref[:FAR, :]
+    far_b_ref[...] = pack_ref[FAR:, :]
 
 
 def make_local(rows, weights, leak, decays, cosine, sine):
     return pl.pallas_call(
         local_body,
         in_specs=[VMEM] * 10,
-        out_specs=[VMEM] * 4,
+        out_specs=[VMEM] * 6,
         out_shape=[
             jax.ShapeDtypeStruct((PACK, 128), BF16),
+            jax.ShapeDtypeStruct((FAR, 128), BF16),
+            jax.ShapeDtypeStruct((PACK - FAR, 128), BF16),
             jax.ShapeDtypeStruct((TOK, 128), F32),
             jax.ShapeDtypeStruct((TOK, 128), BF16),
             jax.ShapeDtypeStruct((TOK, 128), BF16),
@@ -231,7 +238,12 @@
 
 def fold_body(place_ref, own_ref, below1_ref, below2_ref, below3_ref, kept_ref, sent_ref):
     place = place_ref[1]
-    entries = [read_sent(ref, TOK) for ref in (own_ref, below1_ref, below2_ref, below3_ref)]
+    entries = [
+        read_sent(own_ref, TOK),
+        read_sent(below1_ref, TOK),
+        read_sent(below2_ref, TOK - FAR),
+        read_sent(below3_ref, TOK),
+    ]
     none = (jnp.ones((1, HK), F32), jnp.zeros((HV, HK), F32))
 
     def fold(way, below, order):
@@ -324,7 +336,7 @@
     )(place, kept, received, out, read_f, read_b, gain.reshape(1, HV))
 
 
-def attend_tile(maps, kv_refs, peaks, accs, first):
+def attend_tile(maps, kv_refs, peaks, accs):
     ones = jnp.ones((ACC_ROWS - AV, TOK), BF16)
     values = [
         jnp.concatenate(
@@ -346,37 +358,40 @@
     scores = scores_of(units[0])
     for at, (m, n) in enumerate(units):
         upcoming = scores_of(units[at + 1]) if at + 1 < len(units) else None
-        if first:
+        found = peaks[m] is None
+        if found:
             peaks[m] = jnp.max(scores, axis=0, keepdims=True)
         above = scores - peaks[m]
-        if not first:
+        if not found:
             rises.append(jnp.max(above.reshape(-1, 8, above.shape[1]), axis=0))
         added = jnp.dot(values[n], jnp.exp(above).astype(BF16), preferred_element_type=F32)
-        accs[m] = added if first else accs[m] + added
+        accs[m] = added if accs[m] is None else accs[m] + added
         scores = upcoming
-    return accs, peaks, None if first else jnp.max(functools.reduce(jnp.maximum, rises))
+    return accs, peaks, jnp.max(functools.reduce(jnp.maximum, rises)) if rises else None
 
 
 def attend_again(maps_ref, kv_refs, peaks_ref, accs_ref):
     ones = jnp.ones((ACC_ROWS - AV, 128), BF16)
+    steps = TOK // 128
     for kv in kv_refs:
 
         def absorb(i, unused):
-            m, n = i // (TOK // 128), i % (TOK // 128)
+            m, w, n = i // (steps * steps), (i // steps) % steps, i % steps
             keys = kv[pl.ds(pl.multiple_of(n * 128, 128), 128), :]
             values = kv[pl.ds(pl.multiple_of(TOK + n * 128, 128), 128), :]
-            scores = jnp.dot(keys, maps_ref[m], preferred_element_type=F32)
-            old = peaks_ref[m, 0:1, :]
+            cols = pl.ds(pl.multiple_of(w * 128, 128), 128)
+            scores = jnp.dot(keys, maps_ref[m, :, cols], preferred_element_type=F32)
+            old = peaks_ref[m, 0:1, cols]
             new = jnp.maximum(old, jnp.max(scores, axis=0, keepdims=True))
-            accs_ref[m] = accs_ref[m] * jnp.exp(old - new) + jnp.dot(
+            accs_ref[m, :, cols] = accs_ref[m, :, cols] * jnp.exp(old - new) + jnp.dot(
                 jnp.concatenate([values, ones]),
                 jnp.exp(scores - new).astype(BF16),
                 preferred_element_type=F32,
             )
-            peaks_ref[m, 0:1, :] = new
+            peaks_ref[m, 0:1, cols] = new
             return 0
 
-        lax.fori_loop(0, 2 * TOK // 128, absorb, 0)
+        lax.fori_loop(0, 2 * steps * steps, absorb, 0)
 
 
 def both_maps(turned):
@@ -385,21 +400,19 @@
     return jnp.where(upper, turned, zero), jnp.where(upper, zero, turned)
 
 
-def attend_first_body(*refs):
-    q_refs, (kv_ref, turned_ref, peaks_ref, accs_ref) = refs[:NX], refs[NX:]
-    for n, ref in enumerate(q_refs):
-        turned_ref[n] = ref[:TOK, :].T
+def attend_first_body(below_ref, above_ref, far_a_ref, far_b_ref, kv_ref, turned_ref, peaks_ref, accs_ref):
+    turned_ref[0] = below_ref[:TOK, :].T
+    turned_ref[1] = above_ref[:TOK, :].T
+    turned_ref[2] = jnp.concatenate([far_a_ref[...], far_b_ref[: TOK - FAR, :]]).T
 
     def tile(t, unused):
-        accs, peaks, _ = attend_tile(
-            both_maps(turned_ref[t]), [kv_ref], [None] * 2, [None] * 2, True
-        )
+        accs, peaks, _ = attend_tile(both_maps(turned_ref[t]), [kv_ref], [None] * 2, [None] * 2)
         for m in range(2):
             accs_ref[t, m] = accs[m]
             peaks_ref[t, m] = jnp.broadcast_to(peaks[m], (8, TOK))
         return 0
 
-    lax.fori_loop(0, NX, tile, 0)
+    lax.fori_loop(0, PEERS, tile, 0)
 
 
 def attend_more_body(turned_ref, *refs, chunks):
@@ -409,7 +422,7 @@
     def tile(t, unused):
         maps = both_maps(turned_ref[t])
         peaks = [peaks_in[t, m, 0:1, :] for m in range(2)]
-        accs, _, rise = attend_tile(maps, kv_refs, peaks, [accs_in[t, m] for m in range(2)], False)
+        accs, _, rise = attend_tile(maps, kv_refs, peaks, [accs_in[t, m] for m in range(2)])
         for m in range(2):
             accs_ref[t, m] = accs[m]
 
@@ -421,31 +434,10 @@
 
         return 0
 
-    lax.fori_loop(0, NX, tile, 0)
-
-
-def attend_last_body(turned_ref, *refs, chunks, tile):
-    kv_refs, rest = refs[:chunks], refs[chunks:]
-    peaks_in, accs_in, *send_refs, peaks_ref, accs_ref, maps_ref, rise_ref = rest
-    maps_ref[0], maps_ref[1] = both_maps(turned_ref[tile])
-    peaks_ref[...] = peaks_in[tile]
-    rise_ref[0] = 0.0
-
-    def one_map(m, unused):
-        accs, _, rise = attend_tile(
-            [maps_ref[m]], kv_refs, [peaks_in[tile, m, 0:1, :]], [accs_in[tile, m]], False
-        )
-        accs_ref[m] = accs[0]
-        rise_ref[0] = jnp.maximum(rise_ref[0], rise)
-        return 0
-
-    lax.fori_loop(0, 2, one_map, 0)
-
-    @pl.when(rise_ref[0] > RISE)
-    def _():
-        accs_ref[...] = accs_in[tile]
-        attend_again(maps_ref, kv_refs, peaks_ref, accs_ref)
-
+    lax.fori_loop(0, PEERS, tile, 0)
+
+
+def write_partial(send_refs, peaks_ref, accs_ref):
     for m in range(2):
         acc = accs_ref[m]
         total = acc[AV : AV + 1, :]
@@ -464,10 +456,77 @@
         ref[at + AV : at + MAP_ROWS, :] = levels
 
 
+def attend_last_body(turned_ref, *refs, chunks, tiles):
+    kv_refs, rest = refs[:chunks], refs[chunks:]
+    peaks_in, accs_in, *send_refs, peaks_ref, accs_ref, maps_ref, rise_ref = rest
+    start, count = tiles
+    for t in range(count):
+        maps_ref[t, 0], maps_ref[t, 1] = both_maps(turned_ref[start + t])
+        rise_ref[t] = 0.0
+
+    def one_map(i, unused):
+        t, m = i // 2, i % 2
+        peaks = peaks_in[start + t, m]
+        accs, _, rise = attend_tile(
+            [maps_ref[t, m]], kv_refs, [peaks[0:1]], [accs_in[start + t, m]]
+        )
+        peaks_ref[t, m] = peaks
+        accs_ref[t, m] = accs[0]
+        rise_ref[t] = jnp.maximum(rise_ref[t], rise)
+        return 0
+
+    lax.fori_loop(0, 2 * count, one_map, 0)
+
+    def check(t, unused):
+        @pl.when(rise_ref[t] > RISE)
+        def _():
+            accs_ref[t] = accs_in[start + t]
+            attend_again(maps_ref.at[t], kv_refs, peaks_ref.at[t], accs_ref.at[t])
+
+        return 0
+
+    lax.fori_loop(0, count, check, 0)
+    parts = len(send_refs) // count
+    for t in range(count):
+        write_partial(send_refs[t * parts : (t + 1) * parts], peaks_ref.at[t], accs_ref.at[t])
+
+
+def attend_own_body(pack_ref, *refs, chunks):
+    kv_refs, (own_ref, peaks_ref, accs_ref, maps_ref, rise_ref) = refs[:chunks], refs[chunks:]
+    maps_ref[0, 0], maps_ref[0, 1] = both_maps(pack_ref[:TOK, :].T)
+    rise_ref[0] = 0.0
+
+    def one_map(m, unused):
+        accs, peaks, rise = attend_tile([maps_ref[0, m]], kv_refs, [None], [None])
+        accs_ref[0, m] = accs[0]
+        peaks_ref[0, m] = jnp.broadcast_to(peaks[0], (8, TOK))
+        rise_ref[0] = jnp.maximum(rise_ref[0], rise)
+        return 0
+
+    lax.fori_loop(0, 2, one_map, 0)
+
+    @pl.when(rise_ref[0] > RISE)
+    def _():
+        peaks_ref[...] = jnp.full(peaks_ref.shape, LOW, F32)
+        accs_ref[...] = jnp.zeros(accs_ref.shape, F32)
+        attend_again(maps_ref.at[0], kv_refs, peaks_ref.at[0], accs_ref.at[0])
+
+    write_partial([own_ref], peaks_ref.at[0], accs_ref.at[0])
+
+
 STATE = [
-    jax.ShapeDtypeStruct((NX, 2, 8, TOK), F32),
-    jax.ShapeDtypeStruct((NX, 2, ACC_ROWS, TOK), F32),
+    jax.ShapeDtypeStruct((PEERS, 2, 8, TOK), F32),
+    jax.ShapeDtypeStruct((PEERS, 2, ACC_ROWS, TOK), F32),
 ]
+
+
+def tile_scratch(count):
+    return [
+        pltpu.VMEM((count, 2, 8, TOK), F32),
+        pltpu.VMEM((count, 2, ACC_ROWS, TOK), F32),
+        pltpu.VMEM((count, 2, 2 * AK, TOK), BF16),
+        pltpu.SMEM((count,), F32),
+    ]
 
 
 def attend_cost(tiles, chunks):
@@ -475,16 +534,16 @@
     return cost(work * 2 * (AK + AV), work)
 
 
-def attend_first(packs, kv):
+def attend_first(*operands):
     return pl.pallas_call(
         attend_first_body,
-        in_specs=[VMEM] * (NX + 1),
+        in_specs=[VMEM] * 5,
         out_specs=[VMEM] * 3,
-        out_shape=[jax.ShapeDtypeStruct((NX, 2 * AK, TOK), BF16), *STATE],
-        cost_estimate=attend_cost(NX, 1),
+        out_shape=[jax.ShapeDtypeStruct((PEERS, 2 * AK, TOK), BF16), *STATE],
+        cost_estimate=attend_cost(PEERS, 1),
         compiler_params=limit(14),
         name="attend_first",
-    )(*packs, kv)
+    )(*operands)
 
 
 def attend_more(turned, pieces, state):
@@ -494,28 +553,37 @@
         out_specs=[VMEM] * 2,
         out_shape=STATE,
         scratch_shapes=[pltpu.VMEM((2, 2 * AK, TOK), BF16)],
-        cost_estimate=attend_cost(NX, len(pieces)),
+        cost_estimate=attend_cost(PEERS, len(pieces)),
         compiler_params=limit(14),
         name="attend_more",
     )(turned, *pieces, *state)
 
 
-def attend_last(turned, pieces, state, tile, parts):
-    return pl.pallas_call(
-        functools.partial(attend_last_body, chunks=len(pieces), tile=tile),
+def attend_last(turned, pieces, state, tiles, parts):
+    count = tiles[1]
+    return pl.pallas_call(
+        functools.partial(attend_last_body, chunks=len(pieces), tiles=tiles),
         in_specs=[VMEM] * (len(pieces) + 3),
-        out_specs=[VMEM] * parts,
-        out_shape=[jax.ShapeDtypeStruct((SEND_ROWS // parts, TOK), BF16)] * parts,
-        scratch_shapes=[
-            pltpu.VMEM((2, 8, TOK), F32),
-            pltpu.VMEM((2, ACC_ROWS, TOK), F32),
-            pltpu.VMEM((2, 2 * AK, TOK), BF16),
-            pltpu.SMEM((1,), F32),
-        ],
-        cost_estimate=attend_cost(1, len(pieces)),
+        out_specs=[VMEM] * (parts * count),
+        out_shape=[jax.ShapeDtypeStruct((SEND_ROWS // parts, TOK), BF16)] * (parts * count),
+        scratch_shapes=tile_scratch(count),
+        cost_estimate=attend_cost(count, len(pieces)),
         compiler_params=limit(14),
         name="attend_last",
     )(turned, *pieces, *state)
+
+
+def attend_own(pack, pieces):
+    return pl.pallas_call(
+        functools.partial(attend_own_body, chunks=len(pieces)),
+        in_specs=[VMEM] * (len(pieces) + 1),
+        out_specs=VMEM,
+        out_shape=jax.ShapeDtypeStruct((SEND_ROWS, TOK), BF16),
+        scratch_shapes=tile_scratch(1),
+        cost_estimate=attend_cost(1, len(pieces)),
+        compiler_params=limit(14),
+        name="attend_own",
+    )(pack, *pieces)
 
 
 SWAP = TOK // (NY * NC)
@@ -587,17 +655,13 @@
 
 
 def project_body(place_ref, *refs):
-    sources, (rec_ref, att_ref, out_ref) = refs[:NY], refs[NY:]
-    total = None
-    for weights_ref, width, start in ((rec_ref, 2 * HV, 0), (att_ref, 2 * AV, 2 * HV)):
-        for k, ref in enumerate(sources):
-            at = pl.multiple_of(((place_ref[2] + NY - k) % NY) * width, width)
-            term = jnp.dot(
-                ref[:, start : start + width],
-                weights_ref[pl.ds(at, width), :],
-                preferred_element_type=F32,
-            )
-            total = term if total is None else total + term
+    sources, (rec_ref, att_ref, out_ref, rows_ref) = refs[:NY], refs[NY:]
+    for k, ref in enumerate(sources):
+        at = pl.multiple_of(((place_ref[2] + NY - k) % NY) * 2 * HV, 2 * HV)
+        for n in range(2):
+            rows_ref[n, :, pl.ds(at, 2 * HV)] = ref[:, n * 2 * HV : (n + 1) * 2 * HV]
+    total = jnp.dot(rows_ref[0], rec_ref[...], preferred_element_type=F32)
+    total = total + jnp.dot(rows_ref[1], att_ref[...], preferred_element_type=F32)
     out_ref[...] = total.astype(BF16)
 
 
@@ -607,6 +671,7 @@
         in_specs=[SMEM] + [VMEM] * (NY + 2),
         out_specs=VMEM,
         out_shape=jax.ShapeDtypeStruct((SWAP, out_rec.shape[1]), BF16),
+        scratch_shapes=[pltpu.VMEM((2, SWAP, 2 * NY * HV), BF16)],
         cost_estimate=cost(1 << 29),
         compiler_params=limit(6),
         name="project",
@@ -642,7 +707,7 @@
         ups.append(shift(ups[-1], "z", 1, NZ))
         if step < NZ // 2:
             downs.append(shift(downs[-1], "z", -1, NZ))
-    pack, out_local, read_f, read_b = make_local(
+    pack, far_a, far_b, out_local, read_f, read_b = make_local(
         rows,
         (att_query, rec_query, fwd_gate, bwd_gate, rec_value),
         gate_leak,
@@ -650,11 +715,12 @@
         cosine,
         sine,
     )
-    packs = [pack]
-    for by in (1, 2, -1):
-        packs.append(shift(pack, "x", by, NX))
-    kept, sent = fold_x(place, packs)
-    turned, *state = attend_first([packs[0], packs[1], packs[3], packs[2]], own_kv)
+    far_a = shift(far_a, "x", 2, NX)
+    far_b = shift(far_b, "x", -2, NX)
+    below = shift(pack, "x", 1, NX)
+    above = shift(pack, "x", -1, NX)
+    kept, sent = fold_x(place, [pack, below, far_b, above])
+    turned, *state = attend_first(below, above, far_a, far_b, own_kv)
     for bit in (1, 2, 4):
         received = lax.ppermute(sent, "z", [(i, i ^ bit) for i in range(NZ)])
         if bit < 4:
@@ -662,14 +728,13 @@
     state = attend_more(turned, [ups[1], downs[1]], state)
     state = attend_more(turned, [ups[2], downs[2]], state)
     ends = [ups[3], downs[3], ups[4]]
-    low, high = attend_last(turned, ends, state, 3, 2)
+    low, high = attend_last(turned, ends, state, (2, 1), 2)
     far_low = shift(low, "x", 2, NX)
     far_high = shift(high, "x", -2, NX)
-    (send,) = attend_last(turned, ends, state, 1, 1)
-    from_above = shift(send, "x", -1, NX)
-    (send,) = attend_last(turned, ends, state, 2, 1)
-    from_below = shift(send, "x", 1, NX)
-    (own,) = attend_last(turned, ends, state, 0, 1)
+    to_below, to_above = attend_last(turned, ends, state, (0, 2), 1)
+    from_above = shift(to_below, "x", -1, NX)
+    from_below = shift(to_above, "x", 1, NX)
+    own = attend_own(pack, [own_kv, *ups[1:], *downs[1:]])
     rec_rows = finish(place, bit, kept, received, out_local, read_f, read_b, rec_gain)
     partials = [own, from_above, from_below, far_low, far_high]
     keep, give = mix(place, rec_rows, partials, lambdas, att_gain)

time: 190 us -> 353 us (1.86)
  starting transfers between devices: 109 us -> 271 us
    ppermute x23 -> x24, starting transfers between devices: 104 us -> 265 us  [shift(): lax.ppermute(value, axis, [(i, (i + by) % size) for i in range(size)])]
    ppermute x23 -> x24, waiting for transfers between devices: 25.3 us -> 30.8 us  [shift(): lax.ppermute(value, axis, [(i, (i + by) % size) for i in range(size)])]
    pallas_call x2 -> x3, Pallas kernels: 9.99 us -> 14.6 us  [the longest x1 5.92 us: make_local(): pl.pallas_call(local_body, in_specs=[VMEM] * 10, out_specs=[VMEM] * 6, ou...]
    pallas_call x4 -> x2, Pallas kernels: 10.2 us -> 7.76 us  [attend_last(): pl.pallas_call(functools.partial(attend_last_body, chunks=len(pieces), ti...]
  transfers between devices with their start and end apart: 26 -> 27, of which waited for: 11 -> 11; matrix products, arithmetic and copies ran while one was open for 1% -> 1% of each run, Pallas kernels for 17% -> 10%
where the time goes in v5:
time: 353 us; the launch traced here: 351 us
  starting transfers between devices  271 us (77%)
  Pallas kernels  40.2 us (11%)
  waiting for transfers between devices  35.3 us (10%)
  other arithmetic  3.78 us (1%)
    ppermute x24, starting transfers between devices, shift(): lax.ppermute(value, axis, [(i, (i + by) % size) for i in range(size)])  265 us
    ppermute x24, waiting for transfers between devices, shift(): lax.ppermute(value, axis, [(i, (i + by) % size) for i in range(size)])  30.8 us
    pallas_call x2, Pallas kernels, attend_more(): pl.pallas_call(functools.partial(attend_more_body, chunks=len(pieces)), i...  9.22 us
    pallas_call x2, Pallas kernels, attend_last(): pl.pallas_call(functools.partial(attend_last_body, chunks=len(pieces), ti...  7.76 us
  transfers between devices with their start and end apart: 27, of which 11 were waited for; matrix products, arithmetic and copies ran while one was open for 1% of the time, Pallas kernels for 10%

profile of v5, /device:TPU:1, one launch (start us, length us, event | category | flops | bytes accessed | tf_op | source)
XLA Modules:
  0.0 351.2 jit_solution(12914087268958603555)
XLA Ops:
  2.3 2.2 collective-permute-start
  4.4 1.5 collective-permute-start.1
  6.0 1.6 collective-permute-start.2
  11.2 4.4 %collective-permute-done.2 = bf16[32,2048]{1,0:T(8,128)(2,1)S(1)} collective-permute-done((bf16[32,2048]{1,0:T(8,128)(2,1)S(1)}, bf16[32,2048]{1,0:T(8,128)(2,1)S(1)}, u32[]{:S(2)}, u32[]{:S(2)}) %collective-permute-start.2) | collective-permute-done | bytes 131104 | tf_op jit(solution)/shard_map/ppermute | solution.py:38
  15.6 2.8 collective-permute-done.3
  18.4 1.6 collective-permute-start.4
  22.4 1.5 make_keys.1
  23.9 1.7 collective-permute-start.11
  25.6 4.0 %collective-permute-start.15 = (bf16[1024,128]{1,0:T(8,128)(2,1)S(1)}, bf16[1024,128]{1,0:T(8,128)(2,1)S(1)}, u32[]{:S(2)}, u32[]{:S(2)}) collective-permute-start(bf16[1024,128]{1,0:T(8,128)(2,1)S(1)} %get-tuple-element.48.refs_0_.kv_ref), channel_id=1, source_target_pairs={{0,224},{32,0},{64,32},{96,64},{128,96},{160,128},{192,160},{224,1... | collective-permute-start | bytes 786440 | tf_op jit(solution)/shard_map/ppermute | solution.py:38
  29.6 6.2 %collective-permute-done.11.refs_1_.refs_0_ = bf16[1024,128]{1,0:T(8,128)(2,1)S(1)} collective-permute-done((bf16[1024,128]{1,0:T(8,128)(2,1)S(1)}, bf16[1024,128]{1,0:T(8,128)(2,1)S(1)}, u32[]{:S(2)}, u32[]{:S(2)}) %collective-permute-start.11) | collective-permute-done | bytes 262176 | tf_op jit(solution)/shard_map/ppermute | solution.py:38
  35.9 2.7 collective-permute-start.16
  38.6 5.4 %collective-permute-done.12.refs_2_.refs_0_ = bf16[1024,128]{1,0:T(8,128)(2,1)S(1)} collective-permute-done((bf16[1024,128]{1,0:T(8,128)(2,1)S(1)}, bf16[1024,128]{1,0:T(8,128)(2,1)S(1)}, u32[]{:S(2)}, u32[]{:S(2)}) %collective-permute-start.12) | collective-permute-done | bytes 262176 | tf_op jit(solution)/shard_map/ppermute | solution.py:38
  44.2 5.9 %local.1 = (bf16[784,128]{1,0:T(8,128)(2,1)S(1)}, bf16[384,128]{1,0:T(8,128)(2,1)S(1)}, bf16[400,128]{1,0:T(8,128)(2,1)S(1)}, f32[512,128]{1,0:T(8,128)S(1)}, bf...) custom-call(bf16[512,2048]{1,0:T(8,128)(2,1)S(1)} %get-tuple-element.36.rows_ref, ...), custom_call_target="tpu_custom_call" | custom-call | flops 2147483648 | bytes 1048576 | tf_op jit(solution)/shard_map/local/pallas_call | solution.py:190
  51.3 1.5 collective-permute-start.7
  52.8 1.5 collective-permute-start.6
  54.3 4.6 %collective-permute-done.6.below2_ref.far_b_ref = bf16[400,128]{1,0:T(8,128)(2,1)S(1)} collective-permute-done((bf16[400,128]{1,0:T(8,128)(2,1)S(1)}, bf16[400,128]{1,0:T(8,128)(2,1)S(1)}, u32[]{:S(2)}, u32[]{:S(2)}) %collective-permute-start.6) | collective-permute-done | bytes 102432 | tf_op jit(solution)/shard_map/ppermute | solution.py:38
  59.0 1.5 collective-permute-start.18
  61.2 2.8 collective-permute-start.17
  64.0 3.1 attend_first.1
  67.1 4.6 %attend_more.2 = (f32[3,2,8,512]{3,2,1,0:T(8,128)S(1)}, f32[3,2,144,512]{3,2,1,0:T(8,128)S(1)}) custom-call(bf16[3,128,512]{2,1,0:T(8,128)(2,1)S(1)} %get-tuple-element.50.turned_ref, bf16[1024,128]{1,0:T(8,128)(2,1)S(1)} %collective-permute-done.11.refs_1_.refs_0_, bf16[1024,128]{1,0:T(8,128)(2,1)S(1)} %collective-permute-done.15.refs_5_.refs_1_, ...), custom_call_target="tpu_custom_call" | custom-call | flops 1207959552 | bytes 1048576 | tf_op jit(solution)/shard_map/attend_more/pallas_call | solution.py:550
  72.3 3.0 collective-permute-start.9
  75.3 4.6 %attend_more.3 = (f32[3,2,8,512]{3,2,1,0:T(8,128)S(1)}, f32[3,2,144,512]{3,2,1,0:T(8,128)S(1)}) custom-call(bf16[3,128,512]{2,1,0:T(8,128)(2,1)S(1)} %get-tuple-element.50.turned_ref, bf16[1024,128]{1,0:T(8,128)(2,1)S(1)} %collective-permute-done.12.refs_2_.refs_0_, bf16[1024,128]{1,0:T(8,128)(2,1)S(1)} %collective-permute-done.16.refs_6_.refs_1_, ...), custom_call_target="tpu_custom_call" | custom-call | flops 1207959552 | bytes 1048576 | tf_op jit(solution)/shard_map/attend_more/pallas_call | solution.py:550
  80.0 5.2 %attend_last.2 = (bf16[288,512]{1,0:T(8,128)(2,1)S(1)}, bf16[288,512]{1,0:T(8,128)(2,1)S(1)}) custom-call(bf16[3,128,512]{2,1,0:T(8,128)(2,1)S(1)} %get-tuple-element.50.turned_ref, bf16[1024,128]{1,0:T(8,128)(2,1)S(1)} %collective-permute-done.13.refs_3_.refs_0_, bf16[1024,128]{1,0:T(8,128)(2,1)S(1)} %collective-permute-done.17.refs_7_.refs_1_, ...), custom_call_target="tpu_custom_call" | custom-call | flops 1207959552 | bytes 1048576 | tf_op jit(solution)/shard_map/attend_last/pallas_call | solution.py:564
  87.3 2.0 collective-permute-start.10
  90.0 4.5 %collective-permute-done.10.received_ref = bf16[272,128]{1,0:T(8,128)(2,1)S(1)} collective-permute-done((bf16[272,128]{1,0:T(8,128)(2,1)S(1)}, bf16[272,128]{1,0:T(8,128)(2,1)S(1)}, u32[]{:S(2)}, u32[]{:S(2)}) %collective-permute-start.10) | collective-permute-done | bytes 69664 | tf_op jit(solution)/shard_map/ppermute | solution.py:725
  95.3 2.6 attend_last.3
  98.9 2.1 collective-permute-start.22
  101.0 5.6 %attend_own.1.a_ref = bf16[288,512]{1,0:T(8,128)(2,1)S(1)} custom-call(bf16[784,128]{1,0:T(8,128)(2,1)S(1)} %get-tuple-element.37.own_ref.pack_ref, bf16[1024,128]{1,0:T(8,128)(2,1)S(1)} %get-tuple-element.48.refs_0_.kv_ref, bf16[1024,128]{1,0:T(8,128)(2,1)S(1)} %collective-permute-done.11.refs_1_.refs_0_, ...), custom_call_target="tpu_custom_call" | custom-call | flops 1610612736 | bytes 1048576 | tf_op jit(solution)/shard_map/attend_own/pallas_call | solution.py:577
  107.6 232.5 %collective-permute-start.23 = (bf16[4,64,256]{2,1,0:T(8,128)(2,1)S(1)}, bf16[4,64,256]{2,1,0:T(8,128)(2,1)S(1)}, u32[]{:S(2)}, u32[]{:S(2)}) collective-permute-start(bf16[4,64,256]{2,1,0:T(8,128)(2,1)S(1)} %get-tuple-element.62), channel_id=1, source_target_pairs={{0,1},{1,0},{2,3},{3,2},{4,5},{5,4},{6,7},{7,6},{8,9},{9,8},{10,11... | collective-permute-start | bytes 393224 | tf_op jit(solution)/shard_map/ppermute | solution.py:38
  342.2 2.6 collective-permute-start.26
  344.8 3.6 %collective-permute-done.24.refs_1_ = bf16[64,512]{1,0:T(8,128)(2,1)S(1)} collective-permute-done((bf16[64,512]{1,0:T(8,128)(2,1)S(1)}, bf16[64,512]{1,0:T(8,128)(2,1)S(1)}, u32[]{:S(2)}, u32[]{:S(2)}) %collective-permute-start.24) | collective-permute-done | bytes 65568 | tf_op jit(solution)/shard_map/ppermute | solution.py:38
  348.3 2.8 project.1
  (78 shorter events, 17.9 us)
Async XLA Ops:
  2.3 7.7 %collective-permute-start = (bf16[64,2048]{1,0:T(8,128)(2,1)S(1)}, bf16[64,2048]{1,0:T(8,128)(2,1)S(1)}, u32[]{:S(2)}, u32[]{:S(2)}) collective-permute-start(bf16[64,2048]{1,0:T(8,128)(2,1)S(1)} %get-tuple-element.68), channel_id=1, source_target_pairs={{0,2},{2,4},{4,6},{6,0},{1,3},{3,5},{5,7},{7,1},{8,10},{10,12},{12... | collective-permute-start | bytes 786440 | tf_op jit(solution)/shard_map/ppermute | solution.py:38
  4.4 6.7 %collective-permute-start.1 = (bf16[64,2048]{1,0:T(8,128)(2,1)S(1)}, bf16[64,2048]{1,0:T(8,128)(2,1)S(1)}, u32[]{:S(2)}, u32[]{:S(2)}) collective-permute-start(bf16[64,2048]{1,0:T(8,128)(2,1)S(1)} %get-tuple-element.68), channel_id=1, source_target_pairs={{0,6},{2,0},{4,2},{6,4},{1,7},{3,1},{5,3},{7,5},{8,14},{10,8},{12,... | collective-permute-start | bytes 786440 | tf_op jit(solution)/shard_map/ppermute | solution.py:38
  6.0 9.6 %collective-permute-start.2 = (bf16[32,2048]{1,0:T(8,128)(2,1)S(1)}, bf16[32,2048]{1,0:T(8,128)(2,1)S(1)}, u32[]{:S(2)}, u32[]{:S(2)}) collective-permute-start(bf16[32,2048]{1,0:T(8,128)(2,1)S(1)} %get-tuple-element.70), channel_id=1, source_target_pairs={{0,4},{2,6},{4,0},{6,2},{1,5},{3,7},{5,1},{7,3},{8,12},{10,14},{12... | collective-permute-start | bytes 393224 | tf_op jit(solution)/shard_map/ppermute | solution.py:38
  7.6 10.8 %collective-permute-start.3 = (bf16[32,2048]{1,0:T(8,128)(2,1)S(1)}, bf16[32,2048]{1,0:T(8,128)(2,1)S(1)}, u32[]{:S(2)}, u32[]{:S(2)}) collective-permute-start(bf16[32,2048]{1,0:T(8,128)(2,1)S(1)} %get-tuple-element.69), channel_id=1, source_target_pairs={{0,4},{2,6},{4,0},{6,2},{1,5},{3,7},{5,1},{7,3},{8,12},{10,14},{12... | collective-permute-start | bytes 393224 | tf_op jit(solution)/shard_map/ppermute | solution.py:38
  18.4 3.9 %collective-permute-start.4 = (bf16[256,2048]{1,0:T(8,128)(2,1)S(1)}, bf16[256,2048]{1,0:T(8,128)(2,1)S(1)}, u32[]{:S(2)}, u32[]{:S(2)}) collective-permute-start(bf16[256,2048]{1,0:T(8,128)(2,1)S(1)} %constant_dynamic-update-slice_fusion.mine_ref), channel_id=1, source_target_pairs={{0,1},{1,0},{2,3},{3,2},{4,5},{5,4},{6,7},{7,6},{8,9},{9,8},{10,11... | collective-permute-start | bytes 3145736 | tf_op jit(solution)/shard_map/ppermute | solution.py:38
  22.3 21.8 %copy-start.8 = (bf16[2048,128]{1,0:T(8,128)(2,1)S(1)}, bf16[2048,128]{1,0:T(8,128)(2,1)}, u32[]{:S(2)}) copy-start(bf16[2048,128]{1,0:T(8,128)(2,1)} %f_ref.1) | copy-start | bytes 1572868
  22.3 21.8 %copy-start.9 = (bf16[2048,128]{1,0:T(8,128)(2,1)S(1)}, bf16[2048,128]{1,0:T(8,128)(2,1)}, u32[]{:S(2)}) copy-start(bf16[2048,128]{1,0:T(8,128)(2,1)} %b_ref.1) | copy-start | bytes 1572868
  22.4 21.8 %copy-start.10 = (bf16[2048,128]{1,0:T(8,128)(2,1)S(1)}, bf16[2048,128]{1,0:T(8,128)(2,1)}, u32[]{:S(2)}) copy-start(bf16[2048,128]{1,0:T(8,128)(2,1)} %v_ref.1) | copy-start | bytes 1572868
  23.9 12.0 %collective-permute-start.11 = (bf16[1024,128]{1,0:T(8,128)(2,1)S(1)}, bf16[1024,128]{1,0:T(8,128)(2,1)S(1)}, u32[]{:S(2)}, u32[]{:S(2)}) collective-permute-start(bf16[1024,128]{1,0:T(8,128)(2,1)S(1)} %get-tuple-element.48.refs_0_.kv_ref), channel_id=1, source_target_pairs={{0,32},{32,64},{64,96},{96,128},{128,160},{160,192},{192,224},{224... | collective-permute-start | bytes 786440 | tf_op jit(solution)/shard_map/ppermute | solution.py:38
  25.6 10.3 %collective-permute-start.15 = (bf16[1024,128]{1,0:T(8,128)(2,1)S(1)}, bf16[1024,128]{1,0:T(8,128)(2,1)S(1)}, u32[]{:S(2)}, u32[]{:S(2)}) collective-permute-start(bf16[1024,128]{1,0:T(8,128)(2,1)S(1)} %get-tuple-element.48.refs_0_.kv_ref), channel_id=1, source_target_pairs={{0,224},{32,0},{64,32},{96,64},{128,96},{160,128},{192,160},{224,1... | collective-permute-start | bytes 786440 | tf_op jit(solution)/shard_map/ppermute | solution.py:38
  35.8 8.1 %collective-permute-start.12 = (bf16[1024,128]{1,0:T(8,128)(2,1)S(1)}, bf16[1024,128]{1,0:T(8,128)(2,1)S(1)}, u32[]{:S(2)}, u32[]{:S(2)}) collective-permute-start(bf16[1024,128]{1,0:T(8,128)(2,1)S(1)} %collective-permute-done.11.refs_1_.refs_0_), channel_id=1, source_target_pairs={{0,32},{32,64},{64,96},{96,128},{128,160},{160,192},{192,224},{224... | collective-permute-start | bytes 786440 | tf_op jit(solution)/shard_map/ppermute | solution.py:38
  35.9 25.4 %collective-permute-start.16 = (bf16[1024,128]{1,0:T(8,128)(2,1)S(1)}, bf16[1024,128]{1,0:T(8,128)(2,1)S(1)}, u32[]{:S(2)}, u32[]{:S(2)}) collective-permute-start(bf16[1024,128]{1,0:T(8,128)(2,1)S(1)} %collective-permute-done.15.refs_5_.refs_1_), channel_id=1, source_target_pairs={{0,224},{32,0},{64,32},{96,64},{128,96},{160,128},{192,160},{224,1... | collective-permute-start | bytes 786440 | tf_op jit(solution)/shard_map/ppermute | solution.py:38
  44.0 20.0 %collective-permute-start.13 = (bf16[1024,128]{1,0:T(8,128)(2,1)S(1)}, bf16[1024,128]{1,0:T(8,128)(2,1)S(1)}, u32[]{:S(2)}, u32[]{:S(2)}) collective-permute-start(bf16[1024,128]{1,0:T(8,128)(2,1)S(1)} %collective-permute-done.12.refs_2_.refs_0_), channel_id=1, source_target_pairs={{0,32},{32,64},{64,96},{96,128},{128,160},{160,192},{192,224},{224... | collective-permute-start | bytes 786440 | tf_op jit(solution)/shard_map/ppermute | solution.py:38
  50.1 10.3 %collective-permute-start.5 = (bf16[784,128]{1,0:T(8,128)(2,1)S(1)}, bf16[784,128]{1,0:T(8,128)(2,1)S(1)}, u32[]{:S(2)}, u32[]{:S(2)}) collective-permute-start(bf16[784,128]{1,0:T(8,128)(2,1)S(1)} %get-tuple-element.37.own_ref.pack_ref), channel_id=1, source_target_pairs={{0,8},{8,16},{16,24},{24,0},{1,9},{9,17},{17,25},{25,1},{2,10},{10... | collective-permute-start | bytes 602120 | tf_op jit(solution)/shard_map/ppermute | solution.py:38
  51.3 9.1 %collective-permute-start.7 = (bf16[784,128]{1,0:T(8,128)(2,1)S(1)}, bf16[784,128]{1,0:T(8,128)(2,1)S(1)}, u32[]{:S(2)}, u32[]{:S(2)}) collective-permute-start(bf16[784,128]{1,0:T(8,128)(2,1)S(1)} %get-tuple-element.37.own_ref.pack_ref), channel_id=1, source_target_pairs={{0,24},{8,0},{16,8},{24,16},{1,25},{9,1},{17,9},{25,17},{2,26},{10... | collective-permute-start | bytes 602120 | tf_op jit(solution)/shard_map/ppermute | solution.py:38
  52.8 6.2 %collective-permute-start.6 = (bf16[400,128]{1,0:T(8,128)(2,1)S(1)}, bf16[400,128]{1,0:T(8,128)(2,1)S(1)}, u32[]{:S(2)}, u32[]{:S(2)}) collective-permute-start(bf16[400,128]{1,0:T(8,128)(2,1)S(1)} %get-tuple-element.38), channel_id=1, source_target_pairs={{0,16},{8,24},{16,0},{24,8},{1,17},{9,25},{17,1},{25,9},{2,18},{10... | collective-permute-start | bytes 307208 | tf_op jit(solution)/shard_map/ppermute | solution.py:38
  59.0 5.0 %collective-permute-start.18 = (bf16[384,128]{1,0:T(8,128)(2,1)S(1)}, bf16[384,128]{1,0:T(8,128)(2,1)S(1)}, u32[]{:S(2)}, u32[]{:S(2)}) collective-permute-start(bf16[384,128]{1,0:T(8,128)(2,1)S(1)} %get-tuple-element.49), channel_id=1, source_target_pairs={{0,16},{8,24},{16,0},{24,8},{1,17},{9,25},{17,1},{25,9},{2,18},{10... | collective-permute-start | bytes 294920 | tf_op jit(solution)/shard_map/ppermute | solution.py:38
  61.1 10.6 %collective-permute-start.8 = (bf16[272,128]{1,0:T(8,128)(2,1)S(1)}, bf16[272,128]{1,0:T(8,128)(2,1)S(1)}, u32[]{:S(2)}, u32[]{:S(2)}) collective-permute-start(bf16[272,128]{1,0:T(8,128)(2,1)S(1)} %get-tuple-element.40), channel_id=1, source_target_pairs={{0,32},{32,0},{64,96},{96,64},{128,160},{160,128},{192,224},{224,1... | collective-permute-start | bytes 208904 | tf_op jit(solution)/shard_map/ppermute | solution.py:725
  61.2 18.7 %collective-permute-start.17 = (bf16[1024,128]{1,0:T(8,128)(2,1)S(1)}, bf16[1024,128]{1,0:T(8,128)(2,1)S(1)}, u32[]{:S(2)}, u32[]{:S(2)}) collective-permute-start(bf16[1024,128]{1,0:T(8,128)(2,1)S(1)} %collective-permute-done.16.refs_6_.refs_1_), channel_id=1, source_target_pairs={{0,224},{32,0},{64,32},{96,64},{128,96},{160,128},{192,160},{224,1... | collective-permute-start | bytes 786440 | tf_op jit(solution)/shard_map/ppermute | solution.py:38
  64.0 16.0 %collective-permute-start.14 = (bf16[1024,128]{1,0:T(8,128)(2,1)S(1)}, bf16[1024,128]{1,0:T(8,128)(2,1)S(1)}, u32[]{:S(2)}, u32[]{:S(2)}) collective-permute-start(bf16[1024,128]{1,0:T(8,128)(2,1)S(1)} %collective-permute-done.13.refs_3_.refs_0_), channel_id=1, source_target_pairs={{0,32},{32,64},{64,96},{96,128},{128,160},{160,192},{192,224},{224... | collective-permute-start | bytes 786440 | tf_op jit(solution)/shard_map/ppermute | solution.py:38
  72.3 14.4 %collective-permute-start.9 = (bf16[272,128]{1,0:T(8,128)(2,1)S(1)}, bf16[272,128]{1,0:T(8,128)(2,1)S(1)}, u32[]{:S(2)}, u32[]{:S(2)}) collective-permute-start(bf16[272,128]{1,0:T(8,128)(2,1)S(1)} %get-tuple-element.42), channel_id=1, source_target_pairs={{0,64},{32,96},{64,0},{96,32},{128,192},{160,224},{192,128},{224,1... | collective-permute-start | bytes 208904 | tf_op jit(solution)/shard_map/ppermute | solution.py:725
  85.1 21.4 %collective-permute-start.19 = (bf16[288,512]{1,0:T(8,128)(2,1)S(1)}, bf16[288,512]{1,0:T(8,128)(2,1)S(1)}, u32[]{:S(2)}, u32[]{:S(2)}) collective-permute-start(bf16[288,512]{1,0:T(8,128)(2,1)S(1)} %get-tuple-element.57), channel_id=1, source_target_pairs={{0,24},{8,0},{16,8},{24,16},{1,25},{9,1},{17,9},{25,17},{2,26},{10... | collective-permute-start | bytes 884744 | tf_op jit(solution)/shard_map/ppermute | solution.py:38
  86.1 20.5 %collective-permute-start.20 = (bf16[288,512]{1,0:T(8,128)(2,1)S(1)}, bf16[288,512]{1,0:T(8,128)(2,1)S(1)}, u32[]{:S(2)}, u32[]{:S(2)}) collective-permute-start(bf16[288,512]{1,0:T(8,128)(2,1)S(1)} %get-tuple-element.58), channel_id=1, source_target_pairs={{0,8},{8,16},{16,24},{24,0},{1,9},{9,17},{17,25},{25,1},{2,10},{10... | collective-permute-start | bytes 884744 | tf_op jit(solution)/shard_map/ppermute | solution.py:38
  87.3 7.2 %collective-permute-start.10 = (bf16[272,128]{1,0:T(8,128)(2,1)S(1)}, bf16[272,128]{1,0:T(8,128)(2,1)S(1)}, u32[]{:S(2)}, u32[]{:S(2)}) collective-permute-start(bf16[272,128]{1,0:T(8,128)(2,1)S(1)} %get-tuple-element.44), channel_id=1, source_target_pairs={{0,128},{32,160},{64,192},{96,224},{128,0},{160,32},{192,64},{224,... | collective-permute-start | bytes 208904 | tf_op jit(solution)/shard_map/ppermute | solution.py:725
  97.9 8.6 %collective-permute-start.21 = (bf16[144,512]{1,0:T(8,128)(2,1)S(1)}, bf16[144,512]{1,0:T(8,128)(2,1)S(1)}, u32[]{:S(2)}, u32[]{:S(2)}) collective-permute-start(bf16[144,512]{1,0:T(8,128)(2,1)S(1)} %get-tuple-element.59), channel_id=1, source_target_pairs={{0,16},{8,24},{16,0},{24,8},{1,17},{9,25},{17,1},{25,9},{2,18},{10... | collective-permute-start | bytes 442376 | tf_op jit(solution)/shard_map/ppermute | solution.py:38
  98.9 7.7 %collective-permute-start.22 = (bf16[144,512]{1,0:T(8,128)(2,1)S(1)}, bf16[144,512]{1,0:T(8,128)(2,1)S(1)}, u32[]{:S(2)}, u32[]{:S(2)}) collective-permute-start(bf16[144,512]{1,0:T(8,128)(2,1)S(1)} %get-tuple-element.60), channel_id=1, source_target_pairs={{0,16},{8,24},{16,0},{24,8},{1,17},{9,25},{17,1},{25,9},{2,18},{10... | collective-permute-start | bytes 442376 | tf_op jit(solution)/shard_map/ppermute | solution.py:38
  101.0 247.4 %copy-start = (bf16[1024,2048]{1,0:T(8,128)(2,1)S(1)}, bf16[1024,2048]{1,0:T(8,128)(2,1)}, u32[]{:S(2)}) copy-start(bf16[1024,2048]{1,0:T(8,128)(2,1)} %refs_4_.1) | copy-start | bytes 12582916
  101.0 247.4 %copy-start.1 = (bf16[1024,2048]{1,0:T(8,128)(2,1)S(1)}, bf16[1024,2048]{1,0:T(8,128)(2,1)}, u32[]{:S(2)}) copy-start(bf16[1024,2048]{1,0:T(8,128)(2,1)} %refs_5_.1) | copy-start | bytes 12582916
  107.6 233.5 %collective-permute-start.23 = (bf16[4,64,256]{2,1,0:T(8,128)(2,1)S(1)}, bf16[4,64,256]{2,1,0:T(8,128)(2,1)S(1)}, u32[]{:S(2)}, u32[]{:S(2)}) collective-permute-start(bf16[4,64,256]{2,1,0:T(8,128)(2,1)S(1)} %get-tuple-element.62), channel_id=1, source_target_pairs={{0,1},{1,0},{2,3},{3,2},{4,5},{5,4},{6,7},{7,6},{8,9},{9,8},{10,11... | collective-permute-start | bytes 393224 | tf_op jit(solution)/shard_map/ppermute | solution.py:38
  341.7 6.6 %collective-permute-start.24 = (bf16[64,512]{1,0:T(8,128)(2,1)S(1)}, bf16[64,512]{1,0:T(8,128)(2,1)S(1)}, u32[]{:S(2)}, u32[]{:S(2)}) collective-permute-start(bf16[64,512]{1,0:T(8,128)(2,1)S(1)} %get-tuple-element.64), channel_id=1, source_target_pairs={{0,2},{2,4},{4,6},{6,0},{1,3},{3,5},{5,7},{7,1},{8,10},{10,12},{12... | collective-permute-start | bytes 196616 | tf_op jit(solution)/shard_map/ppermute | solution.py:38
  342.1 6.2 %collective-permute-start.25 = (bf16[64,512]{1,0:T(8,128)(2,1)S(1)}, bf16[64,512]{1,0:T(8,128)(2,1)S(1)}, u32[]{:S(2)}, u32[]{:S(2)}) collective-permute-start(bf16[64,512]{1,0:T(8,128)(2,1)S(1)} %get-tuple-element.65), channel_id=1, source_target_pairs={{0,4},{2,6},{4,0},{6,2},{1,5},{3,7},{5,1},{7,3},{8,12},{10,14},{12... | collective-permute-start | bytes 196616 | tf_op jit(solution)/shard_map/ppermute | solution.py:38
  342.2 6.1 %collective-permute-start.26 = (bf16[64,512]{1,0:T(8,128)(2,1)S(1)}, bf16[64,512]{1,0:T(8,128)(2,1)S(1)}, u32[]{:S(2)}, u32[]{:S(2)}) collective-permute-start(bf16[64,512]{1,0:T(8,128)(2,1)S(1)} %get-tuple-element.66), channel_id=1, source_target_pairs={{0,6},{2,0},{4,2},{6,4},{1,7},{3,1},{5,3},{7,5},{8,14},{10,8},{12,... | collective-permute-start | bytes 196616 | tf_op jit(solution)/shard_map/ppermute | solution.py:38
  (8 other events, 142.1 us)

commit v6 on v5

--- a/solution.py
+++ b/solution.py
@@ -133,52 +133,57 @@
     queries = raw / (1.0 + jnp.exp(-raw))
     row = lax.broadcasted_iota(jnp.int32, (BLOCK, BLOCK), 0)
     col = lax.broadcasted_iota(jnp.int32, (BLOCK, BLOCK), 1)
-    totals = []
-    for way, read_ref in enumerate((read_f_ref, read_b_ref)):
+    blocks = TOK // BLOCK
+    all_keys, all_logs = [], []
+    for way in range(2):
         gates = raw_f_b[:, way * HK : (way + 1) * HK].astype(F32)
         keys = leak_ref[way : way + 1, :] / (1.0 + jnp.exp(gates))
-        logs = jnp.log1p(-keys) + decay_ref[way]
+        all_keys.append(keys)
+        all_logs.append(jnp.log1p(-keys) + decay_ref[way])
+    states = [jnp.zeros((HV, HK), F32)] * 2
+    befores = [jnp.zeros((1, HK), F32)] * 2
+    for step, way in [(step, way) for step in range(blocks) for way in range(2)]:
+        n = step if way == 0 else blocks - 1 - step
+        keys, logs, state, before = all_keys[way], all_logs[way], states[way], befores[way]
+        read_ref = (read_f_ref, read_b_ref)[way]
         reach = (row >= col) if way == 0 else (row <= col)
         sums = jnp.where(reach, 1.0, 0.0)
         middle_row, last_row = (BLOCK // 2 - 1, BLOCK - 1) if way == 0 else (BLOCK // 2, 0)
-        state = jnp.zeros((HV, HK), F32)
-        before = jnp.zeros((1, HK), F32)
-        blocks = range(TOK // BLOCK)
-        for n in blocks if way == 0 else reversed(blocks):
-            at = slice(n * BLOCK, (n + 1) * BLOCK)
-            cumulative = jnp.dot(
-                sums, logs[at], precision=lax.Precision.HIGHEST, preferred_element_type=F32
-            )
-            middle = cumulative[middle_row : middle_row + 1]
-            last = cumulative[last_row : last_row + 1]
-            scores = lax.dot_general(
-                (queries[at] * jnp.exp(cumulative - middle)).astype(BF16),
-                (keys[at] * jnp.exp(middle - cumulative)).astype(BF16),
-                (((1,), (1,)), ((), ())),
-                preferred_element_type=F32,
-            )
-            scores = jnp.where(reach, scores, 0.0).astype(BF16)
-            values = raw_q_v[at, 128:]
-            out = jnp.dot(scores, values, preferred_element_type=F32)
-            read = queries[at] * jnp.exp(cumulative)
-            out = out + lax.dot_general(
-                read.astype(BF16),
-                state.astype(BF16),
-                (((1,), (1,)), ((), ())),
-                preferred_element_type=F32,
-            )
-            out_ref[at, :] = out if way == 0 else out_ref[at, :] + out
-            read_ref[at, :] = (read * jnp.exp(before)).astype(BF16)
-            added = lax.dot_general(
-                values,
-                (keys[at] * jnp.exp(last - cumulative)).astype(BF16),
-                (((0,), (0,)), ((), ())),
-                preferred_element_type=F32,
-            )
-            state = state * jnp.exp(last) + added
-            before = before + last
-        pack_ref[TOK + way * HV : TOK + (way + 1) * HV, :] = state.astype(BF16)
-        totals.append(jnp.exp(before))
+        at = slice(n * BLOCK, (n + 1) * BLOCK)
+        cumulative = jnp.dot(
+            sums, logs[at], precision=lax.Precision.HIGHEST, preferred_element_type=F32
+        )
+        middle = cumulative[middle_row : middle_row + 1]
+        last = cumulative[last_row : last_row + 1]
+        scores = lax.dot_general(
+            (queries[at] * jnp.exp(cumulative - middle)).astype(BF16),
+            (keys[at] * jnp.exp(middle - cumulative)).astype(BF16),
+            (((1,), (1,)), ((), ())),
+            preferred_element_type=F32,
+        )
+        scores = jnp.where(reach, scores, 0.0).astype(BF16)
+        values = raw_q_v[at, 128:]
+        out = jnp.dot(scores, values, preferred_element_type=F32)
+        read = queries[at] * jnp.exp(cumulative)
+        out = out + lax.dot_general(
+            read.astype(BF16),
+            state.astype(BF16),
+            (((1,), (1,)), ((), ())),
+            preferred_element_type=F32,
+        )
+        out_ref[at, :] = out if step < blocks // 2 else out_ref[at, :] + out
+        read_ref[at, :] = (read * jnp.exp(before)).astype(BF16)
+        added = lax.dot_general(
+            values,
+            (keys[at] * jnp.exp(last - cumulative)).astype(BF16),
+            (((0,), (0,)), ((), ())),
+            preferred_element_type=F32,
+        )
+        states[way] = state * jnp.exp(last) + added
+        befores[way] = before + last
+    for way in range(2):
+        pack_ref[TOK + way * HV : TOK + (way + 1) * HV, :] = states[way].astype(BF16)
+    totals = [jnp.exp(before) for before in befores]
     pack_ref[TOK + 2 * HV :, :] = jnp.concatenate(
         [*totals, jnp.zeros((PACK - TOK - 2 * HV - 2, HK), F32)]
     ).astype(BF16)

time: 353 us -> 353 us (level)
  no operation moved by 1% of the time
where the time goes in v6:
time: 353 us; the launch traced here: 351 us
  starting transfers between devices  271 us (77%)
  Pallas kernels  40.2 us (11%)
  waiting for transfers between devices  35.3 us (10%)
  other arithmetic  3.78 us (1%)
    ppermute x24, starting transfers between devices, shift(): lax.ppermute(value, axis, [(i, (i + by) % size) for i in range(size)])  265 us
    ppermute x24, waiting for transfers between devices, shift(): lax.ppermute(value, axis, [(i, (i + by) % size) for i in range(size)])  30.8 us
    pallas_call x2, Pallas kernels, attend_more(): pl.pallas_call(functools.partial(attend_more_body, chunks=len(pieces)), i...  9.22 us
    pallas_call x2, Pallas kernels, attend_last(): pl.pallas_call(functools.partial(attend_last_body, chunks=len(pieces), ti...  7.76 us
  transfers between devices with their start and end apart: 27, of which 11 were waited for; matrix products, arithmetic and copies ran while one was open for 1% of the time, Pallas kernels for 10%

profile of v6, /device:TPU:1, one launch (start us, length us, event | category | flops | bytes accessed | tf_op | source)
XLA Modules:
  0.0 351.1 jit_solution(9410511636647682834)
XLA Ops:
  2.3 2.2 collective-permute-start
  4.4 1.5 collective-permute-start.1
  6.0 1.6 collective-permute-start.2
  11.2 4.4 %collective-permute-done.2 = bf16[32,2048]{1,0:T(8,128)(2,1)S(1)} collective-permute-done((bf16[32,2048]{1,0:T(8,128)(2,1)S(1)}, bf16[32,2048]{1,0:T(8,128)(2,1)S(1)}, u32[]{:S(2)}, u32[]{:S(2)}) %collective-permute-start.2) | collective-permute-done | bytes 131104 | tf_op jit(solution)/shard_map/ppermute | solution.py:38
  15.6 2.8 collective-permute-done.3
  18.4 1.6 collective-permute-start.4
  22.4 1.5 make_keys.1
  23.9 1.7 collective-permute-start.11
  25.6 4.0 %collective-permute-start.15 = (bf16[1024,128]{1,0:T(8,128)(2,1)S(1)}, bf16[1024,128]{1,0:T(8,128)(2,1)S(1)}, u32[]{:S(2)}, u32[]{:S(2)}) collective-permute-start(bf16[1024,128]{1,0:T(8,128)(2,1)S(1)} %get-tuple-element.48.refs_0_.kv_ref), channel_id=1, source_target_pairs={{0,224},{32,0},{64,32},{96,64},{128,96},{160,128},{192,160},{224,1... | collective-permute-start | bytes 786440 | tf_op jit(solution)/shard_map/ppermute | solution.py:38
  29.6 6.2 %collective-permute-done.11.refs_1_.refs_0_ = bf16[1024,128]{1,0:T(8,128)(2,1)S(1)} collective-permute-done((bf16[1024,128]{1,0:T(8,128)(2,1)S(1)}, bf16[1024,128]{1,0:T(8,128)(2,1)S(1)}, u32[]{:S(2)}, u32[]{:S(2)}) %collective-permute-start.11) | collective-permute-done | bytes 262176 | tf_op jit(solution)/shard_map/ppermute | solution.py:38
  35.9 2.7 collective-permute-start.16
  38.6 5.4 %collective-permute-done.12.refs_2_.refs_0_ = bf16[1024,128]{1,0:T(8,128)(2,1)S(1)} collective-permute-done((bf16[1024,128]{1,0:T(8,128)(2,1)S(1)}, bf16[1024,128]{1,0:T(8,128)(2,1)S(1)}, u32[]{:S(2)}, u32[]{:S(2)}) %collective-permute-start.12) | collective-permute-done | bytes 262176 | tf_op jit(solution)/shard_map/ppermute | solution.py:38
  44.2 5.9 %local.1 = (bf16[784,128]{1,0:T(8,128)(2,1)S(1)}, bf16[384,128]{1,0:T(8,128)(2,1)S(1)}, bf16[400,128]{1,0:T(8,128)(2,1)S(1)}, f32[512,128]{1,0:T(8,128)S(1)}, bf...) custom-call(bf16[512,2048]{1,0:T(8,128)(2,1)S(1)} %get-tuple-element.36.rows_ref, ...), custom_call_target="tpu_custom_call" | custom-call | flops 2147483648 | bytes 1048576 | tf_op jit(solution)/shard_map/local/pallas_call | solution.py:195
  51.3 1.5 collective-permute-start.7
  52.8 1.5 collective-permute-start.6
  54.3 4.6 %collective-permute-done.6.below2_ref.far_b_ref = bf16[400,128]{1,0:T(8,128)(2,1)S(1)} collective-permute-done((bf16[400,128]{1,0:T(8,128)(2,1)S(1)}, bf16[400,128]{1,0:T(8,128)(2,1)S(1)}, u32[]{:S(2)}, u32[]{:S(2)}) %collective-permute-start.6) | collective-permute-done | bytes 102432 | tf_op jit(solution)/shard_map/ppermute | solution.py:38
  59.0 1.5 collective-permute-start.18
  61.2 2.7 collective-permute-start.17
  64.0 3.1 attend_first.1
  67.1 4.6 %attend_more.2 = (f32[3,2,8,512]{3,2,1,0:T(8,128)S(1)}, f32[3,2,144,512]{3,2,1,0:T(8,128)S(1)}) custom-call(bf16[3,128,512]{2,1,0:T(8,128)(2,1)S(1)} %get-tuple-element.50.turned_ref, bf16[1024,128]{1,0:T(8,128)(2,1)S(1)} %collective-permute-done.11.refs_1_.refs_0_, bf16[1024,128]{1,0:T(8,128)(2,1)S(1)} %collective-permute-done.15.refs_5_.refs_1_, ...), custom_call_target="tpu_custom_call" | custom-call | flops 1207959552 | bytes 1048576 | tf_op jit(solution)/shard_map/attend_more/pallas_call | solution.py:555
  72.3 3.0 collective-permute-start.9
  75.3 4.6 %attend_more.3 = (f32[3,2,8,512]{3,2,1,0:T(8,128)S(1)}, f32[3,2,144,512]{3,2,1,0:T(8,128)S(1)}) custom-call(bf16[3,128,512]{2,1,0:T(8,128)(2,1)S(1)} %get-tuple-element.50.turned_ref, bf16[1024,128]{1,0:T(8,128)(2,1)S(1)} %collective-permute-done.12.refs_2_.refs_0_, bf16[1024,128]{1,0:T(8,128)(2,1)S(1)} %collective-permute-done.16.refs_6_.refs_1_, ...), custom_call_target="tpu_custom_call" | custom-call | flops 1207959552 | bytes 1048576 | tf_op jit(solution)/shard_map/attend_more/pallas_call | solution.py:555
  80.0 5.2 %attend_last.2 = (bf16[288,512]{1,0:T(8,128)(2,1)S(1)}, bf16[288,512]{1,0:T(8,128)(2,1)S(1)}) custom-call(bf16[3,128,512]{2,1,0:T(8,128)(2,1)S(1)} %get-tuple-element.50.turned_ref, bf16[1024,128]{1,0:T(8,128)(2,1)S(1)} %collective-permute-done.13.refs_3_.refs_0_, bf16[1024,128]{1,0:T(8,128)(2,1)S(1)} %collective-permute-done.17.refs_7_.refs_1_, ...), custom_call_target="tpu_custom_call" | custom-call | flops 1207959552 | bytes 1048576 | tf_op jit(solution)/shard_map/attend_last/pallas_call | solution.py:569
  87.3 2.0 collective-permute-start.10
  89.9 4.5 %collective-permute-done.10.received_ref = bf16[272,128]{1,0:T(8,128)(2,1)S(1)} collective-permute-done((bf16[272,128]{1,0:T(8,128)(2,1)S(1)}, bf16[272,128]{1,0:T(8,128)(2,1)S(1)}, u32[]{:S(2)}, u32[]{:S(2)}) %collective-permute-start.10) | collective-permute-done | bytes 69664 | tf_op jit(solution)/shard_map/ppermute | solution.py:730
  95.3 2.6 attend_last.3
  98.9 2.1 collective-permute-start.22
  101.0 5.6 %attend_own.1.a_ref = bf16[288,512]{1,0:T(8,128)(2,1)S(1)} custom-call(bf16[784,128]{1,0:T(8,128)(2,1)S(1)} %get-tuple-element.37.own_ref.pack_ref, bf16[1024,128]{1,0:T(8,128)(2,1)S(1)} %get-tuple-element.48.refs_0_.kv_ref, bf16[1024,128]{1,0:T(8,128)(2,1)S(1)} %collective-permute-done.11.refs_1_.refs_0_, ...), custom_call_target="tpu_custom_call" | custom-call | flops 1610612736 | bytes 1048576 | tf_op jit(solution)/shard_map/attend_own/pallas_call | solution.py:582
  107.6 232.5 %collective-permute-start.23 = (bf16[4,64,256]{2,1,0:T(8,128)(2,1)S(1)}, bf16[4,64,256]{2,1,0:T(8,128)(2,1)S(1)}, u32[]{:S(2)}, u32[]{:S(2)}) collective-permute-start(bf16[4,64,256]{2,1,0:T(8,128)(2,1)S(1)} %get-tuple-element.62), channel_id=1, source_target_pairs={{0,1},{1,0},{2,3},{3,2},{4,5},{5,4},{6,7},{7,6},{8,9},{9,8},{10,11... | collective-permute-start | bytes 393224 | tf_op jit(solution)/shard_map/ppermute | solution.py:38
  342.2 2.6 collective-permute-start.26
  344.8 3.6 %collective-permute-done.24.refs_1_ = bf16[64,512]{1,0:T(8,128)(2,1)S(1)} collective-permute-done((bf16[64,512]{1,0:T(8,128)(2,1)S(1)}, bf16[64,512]{1,0:T(8,128)(2,1)S(1)}, u32[]{:S(2)}, u32[]{:S(2)}) %collective-permute-start.24) | collective-permute-done | bytes 65568 | tf_op jit(solution)/shard_map/ppermute | solution.py:38
  348.3 2.8 project.1
  (78 shorter events, 17.9 us)
Async XLA Ops:
  2.3 7.7 %collective-permute-start = (bf16[64,2048]{1,0:T(8,128)(2,1)S(1)}, bf16[64,2048]{1,0:T(8,128)(2,1)S(1)}, u32[]{:S(2)}, u32[]{:S(2)}) collective-permute-start(bf16[64,2048]{1,0:T(8,128)(2,1)S(1)} %get-tuple-element.68), channel_id=1, source_target_pairs={{0,2},{2,4},{4,6},{6,0},{1,3},{3,5},{5,7},{7,1},{8,10},{10,12},{12... | collective-permute-start | bytes 786440 | tf_op jit(solution)/shard_map/ppermute | solution.py:38
  4.4 6.7 %collective-permute-start.1 = (bf16[64,2048]{1,0:T(8,128)(2,1)S(1)}, bf16[64,2048]{1,0:T(8,128)(2,1)S(1)}, u32[]{:S(2)}, u32[]{:S(2)}) collective-permute-start(bf16[64,2048]{1,0:T(8,128)(2,1)S(1)} %get-tuple-element.68), channel_id=1, source_target_pairs={{0,6},{2,0},{4,2},{6,4},{1,7},{3,1},{5,3},{7,5},{8,14},{10,8},{12,... | collective-permute-start | bytes 786440 | tf_op jit(solution)/shard_map/ppermute | solution.py:38
  6.0 9.6 %collective-permute-start.2 = (bf16[32,2048]{1,0:T(8,128)(2,1)S(1)}, bf16[32,2048]{1,0:T(8,128)(2,1)S(1)}, u32[]{:S(2)}, u32[]{:S(2)}) collective-permute-start(bf16[32,2048]{1,0:T(8,128)(2,1)S(1)} %get-tuple-element.70), channel_id=1, source_target_pairs={{0,4},{2,6},{4,0},{6,2},{1,5},{3,7},{5,1},{7,3},{8,12},{10,14},{12... | collective-permute-start | bytes 393224 | tf_op jit(solution)/shard_map/ppermute | solution.py:38
  7.6 10.8 %collective-permute-start.3 = (bf16[32,2048]{1,0:T(8,128)(2,1)S(1)}, bf16[32,2048]{1,0:T(8,128)(2,1)S(1)}, u32[]{:S(2)}, u32[]{:S(2)}) collective-permute-start(bf16[32,2048]{1,0:T(8,128)(2,1)S(1)} %get-tuple-element.69), channel_id=1, source_target_pairs={{0,4},{2,6},{4,0},{6,2},{1,5},{3,7},{5,1},{7,3},{8,12},{10,14},{12... | collective-permute-start | bytes 393224 | tf_op jit(solution)/shard_map/ppermute | solution.py:38
  18.4 3.9 %collective-permute-start.4 = (bf16[256,2048]{1,0:T(8,128)(2,1)S(1)}, bf16[256,2048]{1,0:T(8,128)(2,1)S(1)}, u32[]{:S(2)}, u32[]{:S(2)}) collective-permute-start(bf16[256,2048]{1,0:T(8,128)(2,1)S(1)} %constant_dynamic-update-slice_fusion.mine_ref), channel_id=1, source_target_pairs={{0,1},{1,0},{2,3},{3,2},{4,5},{5,4},{6,7},{7,6},{8,9},{9,8},{10,11... | collective-permute-start | bytes 3145736 | tf_op jit(solution)/shard_map/ppermute | solution.py:38
  22.3 21.8 %copy-start.8 = (bf16[2048,128]{1,0:T(8,128)(2,1)S(1)}, bf16[2048,128]{1,0:T(8,128)(2,1)}, u32[]{:S(2)}) copy-start(bf16[2048,128]{1,0:T(8,128)(2,1)} %f_ref.1) | copy-start | bytes 1572868
  22.3 21.8 %copy-start.9 = (bf16[2048,128]{1,0:T(8,128)(2,1)S(1)}, bf16[2048,128]{1,0:T(8,128)(2,1)}, u32[]{:S(2)}) copy-start(bf16[2048,128]{1,0:T(8,128)(2,1)} %b_ref.1) | copy-start | bytes 1572868
  22.4 21.8 %copy-start.10 = (bf16[2048,128]{1,0:T(8,128)(2,1)S(1)}, bf16[2048,128]{1,0:T(8,128)(2,1)}, u32[]{:S(2)}) copy-start(bf16[2048,128]{1,0:T(8,128)(2,1)} %v_ref.1) | copy-start | bytes 1572868
  23.9 12.0 %collective-permute-start.11 = (bf16[1024,128]{1,0:T(8,128)(2,1)S(1)}, bf16[1024,128]{1,0:T(8,128)(2,1)S(1)}, u32[]{:S(2)}, u32[]{:S(2)}) collective-permute-start(bf16[1024,128]{1,0:T(8,128)(2,1)S(1)} %get-tuple-element.48.refs_0_.kv_ref), channel_id=1, source_target_pairs={{0,32},{32,64},{64,96},{96,128},{128,160},{160,192},{192,224},{224... | collective-permute-start | bytes 786440 | tf_op jit(solution)/shard_map/ppermute | solution.py:38
  25.6 10.3 %collective-permute-start.15 = (bf16[1024,128]{1,0:T(8,128)(2,1)S(1)}, bf16[1024,128]{1,0:T(8,128)(2,1)S(1)}, u32[]{:S(2)}, u32[]{:S(2)}) collective-permute-start(bf16[1024,128]{1,0:T(8,128)(2,1)S(1)} %get-tuple-element.48.refs_0_.kv_ref), channel_id=1, source_target_pairs={{0,224},{32,0},{64,32},{96,64},{128,96},{160,128},{192,160},{224,1... | collective-permute-start | bytes 786440 | tf_op jit(solution)/shard_map/ppermute | solution.py:38
  35.8 8.1 %collective-permute-start.12 = (bf16[1024,128]{1,0:T(8,128)(2,1)S(1)}, bf16[1024,128]{1,0:T(8,128)(2,1)S(1)}, u32[]{:S(2)}, u32[]{:S(2)}) collective-permute-start(bf16[1024,128]{1,0:T(8,128)(2,1)S(1)} %collective-permute-done.11.refs_1_.refs_0_), channel_id=1, source_target_pairs={{0,32},{32,64},{64,96},{96,128},{128,160},{160,192},{192,224},{224... | collective-permute-start | bytes 786440 | tf_op jit(solution)/shard_map/ppermute | solution.py:38
  35.9 25.4 %collective-permute-start.16 = (bf16[1024,128]{1,0:T(8,128)(2,1)S(1)}, bf16[1024,128]{1,0:T(8,128)(2,1)S(1)}, u32[]{:S(2)}, u32[]{:S(2)}) collective-permute-start(bf16[1024,128]{1,0:T(8,128)(2,1)S(1)} %collective-permute-done.15.refs_5_.refs_1_), channel_id=1, source_target_pairs={{0,224},{32,0},{64,32},{96,64},{128,96},{160,128},{192,160},{224,1... | collective-permute-start | bytes 786440 | tf_op jit(solution)/shard_map/ppermute | solution.py:38
  44.0 20.0 %collective-permute-start.13 = (bf16[1024,128]{1,0:T(8,128)(2,1)S(1)}, bf16[1024,128]{1,0:T(8,128)(2,1)S(1)}, u32[]{:S(2)}, u32[]{:S(2)}) collective-permute-start(bf16[1024,128]{1,0:T(8,128)(2,1)S(1)} %collective-permute-done.12.refs_2_.refs_0_), channel_id=1, source_target_pairs={{0,32},{32,64},{64,96},{96,128},{128,160},{160,192},{192,224},{224... | collective-permute-start | bytes 786440 | tf_op jit(solution)/shard_map/ppermute | solution.py:38
  50.1 10.3 %collective-permute-start.5 = (bf16[784,128]{1,0:T(8,128)(2,1)S(1)}, bf16[784,128]{1,0:T(8,128)(2,1)S(1)}, u32[]{:S(2)}, u32[]{:S(2)}) collective-permute-start(bf16[784,128]{1,0:T(8,128)(2,1)S(1)} %get-tuple-element.37.own_ref.pack_ref), channel_id=1, source_target_pairs={{0,8},{8,16},{16,24},{24,0},{1,9},{9,17},{17,25},{25,1},{2,10},{10... | collective-permute-start | bytes 602120 | tf_op jit(solution)/shard_map/ppermute | solution.py:38
  51.3 9.1 %collective-permute-start.7 = (bf16[784,128]{1,0:T(8,128)(2,1)S(1)}, bf16[784,128]{1,0:T(8,128)(2,1)S(1)}, u32[]{:S(2)}, u32[]{:S(2)}) collective-permute-start(bf16[784,128]{1,0:T(8,128)(2,1)S(1)} %get-tuple-element.37.own_ref.pack_ref), channel_id=1, source_target_pairs={{0,24},{8,0},{16,8},{24,16},{1,25},{9,1},{17,9},{25,17},{2,26},{10... | collective-permute-start | bytes 602120 | tf_op jit(solution)/shard_map/ppermute | solution.py:38
  52.8 6.1 %collective-permute-start.6 = (bf16[400,128]{1,0:T(8,128)(2,1)S(1)}, bf16[400,128]{1,0:T(8,128)(2,1)S(1)}, u32[]{:S(2)}, u32[]{:S(2)}) collective-permute-start(bf16[400,128]{1,0:T(8,128)(2,1)S(1)} %get-tuple-element.38), channel_id=1, source_target_pairs={{0,16},{8,24},{16,0},{24,8},{1,17},{9,25},{17,1},{25,9},{2,18},{10... | collective-permute-start | bytes 307208 | tf_op jit(solution)/shard_map/ppermute | solution.py:38
  59.0 5.0 %collective-permute-start.18 = (bf16[384,128]{1,0:T(8,128)(2,1)S(1)}, bf16[384,128]{1,0:T(8,128)(2,1)S(1)}, u32[]{:S(2)}, u32[]{:S(2)}) collective-permute-start(bf16[384,128]{1,0:T(8,128)(2,1)S(1)} %get-tuple-element.49), channel_id=1, source_target_pairs={{0,16},{8,24},{16,0},{24,8},{1,17},{9,25},{17,1},{25,9},{2,18},{10... | collective-permute-start | bytes 294920 | tf_op jit(solution)/shard_map/ppermute | solution.py:38
  61.1 10.6 %collective-permute-start.8 = (bf16[272,128]{1,0:T(8,128)(2,1)S(1)}, bf16[272,128]{1,0:T(8,128)(2,1)S(1)}, u32[]{:S(2)}, u32[]{:S(2)}) collective-permute-start(bf16[272,128]{1,0:T(8,128)(2,1)S(1)} %get-tuple-element.40), channel_id=1, source_target_pairs={{0,32},{32,0},{64,96},{96,64},{128,160},{160,128},{192,224},{224,1... | collective-permute-start | bytes 208904 | tf_op jit(solution)/shard_map/ppermute | solution.py:730
  61.2 18.7 %collective-permute-start.17 = (bf16[1024,128]{1,0:T(8,128)(2,1)S(1)}, bf16[1024,128]{1,0:T(8,128)(2,1)S(1)}, u32[]{:S(2)}, u32[]{:S(2)}) collective-permute-start(bf16[1024,128]{1,0:T(8,128)(2,1)S(1)} %collective-permute-done.16.refs_6_.refs_1_), channel_id=1, source_target_pairs={{0,224},{32,0},{64,32},{96,64},{128,96},{160,128},{192,160},{224,1... | collective-permute-start | bytes 786440 | tf_op jit(solution)/shard_map/ppermute | solution.py:38
  64.0 16.0 %collective-permute-start.14 = (bf16[1024,128]{1,0:T(8,128)(2,1)S(1)}, bf16[1024,128]{1,0:T(8,128)(2,1)S(1)}, u32[]{:S(2)}, u32[]{:S(2)}) collective-permute-start(bf16[1024,128]{1,0:T(8,128)(2,1)S(1)} %collective-permute-done.13.refs_3_.refs_0_), channel_id=1, source_target_pairs={{0,32},{32,64},{64,96},{96,128},{128,160},{160,192},{192,224},{224... | collective-permute-start | bytes 786440 | tf_op jit(solution)/shard_map/ppermute | solution.py:38
  72.3 14.4 %collective-permute-start.9 = (bf16[272,128]{1,0:T(8,128)(2,1)S(1)}, bf16[272,128]{1,0:T(8,128)(2,1)S(1)}, u32[]{:S(2)}, u32[]{:S(2)}) collective-permute-start(bf16[272,128]{1,0:T(8,128)(2,1)S(1)} %get-tuple-element.42), channel_id=1, source_target_pairs={{0,64},{32,96},{64,0},{96,32},{128,192},{160,224},{192,128},{224,1... | collective-permute-start | bytes 208904 | tf_op jit(solution)/shard_map/ppermute | solution.py:730
  85.1 21.4 %collective-permute-start.19 = (bf16[288,512]{1,0:T(8,128)(2,1)S(1)}, bf16[288,512]{1,0:T(8,128)(2,1)S(1)}, u32[]{:S(2)}, u32[]{:S(2)}) collective-permute-start(bf16[288,512]{1,0:T(8,128)(2,1)S(1)} %get-tuple-element.57), channel_id=1, source_target_pairs={{0,24},{8,0},{16,8},{24,16},{1,25},{9,1},{17,9},{25,17},{2,26},{10... | collective-permute-start | bytes 884744 | tf_op jit(solution)/shard_map/ppermute | solution.py:38
  86.1 20.5 %collective-permute-start.20 = (bf16[288,512]{1,0:T(8,128)(2,1)S(1)}, bf16[288,512]{1,0:T(8,128)(2,1)S(1)}, u32[]{:S(2)}, u32[]{:S(2)}) collective-permute-start(bf16[288,512]{1,0:T(8,128)(2,1)S(1)} %get-tuple-element.58), channel_id=1, source_target_pairs={{0,8},{8,16},{16,24},{24,0},{1,9},{9,17},{17,25},{25,1},{2,10},{10... | collective-permute-start | bytes 884744 | tf_op jit(solution)/shard_map/ppermute | solution.py:38
  87.3 7.2 %collective-permute-start.10 = (bf16[272,128]{1,0:T(8,128)(2,1)S(1)}, bf16[272,128]{1,0:T(8,128)(2,1)S(1)}, u32[]{:S(2)}, u32[]{:S(2)}) collective-permute-start(bf16[272,128]{1,0:T(8,128)(2,1)S(1)} %get-tuple-element.44), channel_id=1, source_target_pairs={{0,128},{32,160},{64,192},{96,224},{128,0},{160,32},{192,64},{224,... | collective-permute-start | bytes 208904 | tf_op jit(solution)/shard_map/ppermute | solution.py:730
  97.9 8.6 %collective-permute-start.21 = (bf16[144,512]{1,0:T(8,128)(2,1)S(1)}, bf16[144,512]{1,0:T(8,128)(2,1)S(1)}, u32[]{:S(2)}, u32[]{:S(2)}) collective-permute-start(bf16[144,512]{1,0:T(8,128)(2,1)S(1)} %get-tuple-element.59), channel_id=1, source_target_pairs={{0,16},{8,24},{16,0},{24,8},{1,17},{9,25},{17,1},{25,9},{2,18},{10... | collective-permute-start | bytes 442376 | tf_op jit(solution)/shard_map/ppermute | solution.py:38
  98.9 7.7 %collective-permute-start.22 = (bf16[144,512]{1,0:T(8,128)(2,1)S(1)}, bf16[144,512]{1,0:T(8,128)(2,1)S(1)}, u32[]{:S(2)}, u32[]{:S(2)}) collective-permute-start(bf16[144,512]{1,0:T(8,128)(2,1)S(1)} %get-tuple-element.60), channel_id=1, source_target_pairs={{0,16},{8,24},{16,0},{24,8},{1,17},{9,25},{17,1},{25,9},{2,18},{10... | collective-permute-start | bytes 442376 | tf_op jit(solution)/shard_map/ppermute | solution.py:38
  101.0 247.4 %copy-start = (bf16[1024,2048]{1,0:T(8,128)(2,1)S(1)}, bf16[1024,2048]{1,0:T(8,128)(2,1)}, u32[]{:S(2)}) copy-start(bf16[1024,2048]{1,0:T(8,128)(2,1)} %refs_4_.1) | copy-start | bytes 12582916
  101.0 247.4 %copy-start.1 = (bf16[1024,2048]{1,0:T(8,128)(2,1)S(1)}, bf16[1024,2048]{1,0:T(8,128)(2,1)}, u32[]{:S(2)}) copy-start(bf16[1024,2048]{1,0:T(8,128)(2,1)} %refs_5_.1) | copy-start | bytes 12582916
  107.6 233.5 %collective-permute-start.23 = (bf16[4,64,256]{2,1,0:T(8,128)(2,1)S(1)}, bf16[4,64,256]{2,1,0:T(8,128)(2,1)S(1)}, u32[]{:S(2)}, u32[]{:S(2)}) collective-permute-start(bf16[4,64,256]{2,1,0:T(8,128)(2,1)S(1)} %get-tuple-element.62), channel_id=1, source_target_pairs={{0,1},{1,0},{2,3},{3,2},{4,5},{5,4},{6,7},{7,6},{8,9},{9,8},{10,11... | collective-permute-start | bytes 393224 | tf_op jit(solution)/shard_map/ppermute | solution.py:38
  341.7 6.6 %collective-permute-start.24 = (bf16[64,512]{1,0:T(8,128)(2,1)S(1)}, bf16[64,512]{1,0:T(8,128)(2,1)S(1)}, u32[]{:S(2)}, u32[]{:S(2)}) collective-permute-start(bf16[64,512]{1,0:T(8,128)(2,1)S(1)} %get-tuple-element.64), channel_id=1, source_target_pairs={{0,2},{2,4},{4,6},{6,0},{1,3},{3,5},{5,7},{7,1},{8,10},{10,12},{12... | collective-permute-start | bytes 196616 | tf_op jit(solution)/shard_map/ppermute | solution.py:38
  342.1 6.2 %collective-permute-start.25 = (bf16[64,512]{1,0:T(8,128)(2,1)S(1)}, bf16[64,512]{1,0:T(8,128)(2,1)S(1)}, u32[]{:S(2)}, u32[]{:S(2)}) collective-permute-start(bf16[64,512]{1,0:T(8,128)(2,1)S(1)} %get-tuple-element.65), channel_id=1, source_target_pairs={{0,4},{2,6},{4,0},{6,2},{1,5},{3,7},{5,1},{7,3},{8,12},{10,14},{12... | collective-permute-start | bytes 196616 | tf_op jit(solution)/shard_map/ppermute | solution.py:38
  342.2 6.1 %collective-permute-start.26 = (bf16[64,512]{1,0:T(8,128)(2,1)S(1)}, bf16[64,512]{1,0:T(8,128)(2,1)S(1)}, u32[]{:S(2)}, u32[]{:S(2)}) collective-permute-start(bf16[64,512]{1,0:T(8,128)(2,1)S(1)} %get-tuple-element.66), channel_id=1, source_target_pairs={{0,6},{2,0},{4,2},{6,4},{1,7},{3,1},{5,3},{7,5},{8,14},{10,8},{12,... | collective-permute-start | bytes 196616 | tf_op jit(solution)/shard_map/ppermute | solution.py:38
  (8 other events, 142.1 us)
